TPU v7x, 256 devices: a whole 4x4x8 slice. The times are simulated.
256 devices in a mesh: ep: 16 (over y, x), tp: 16 (over z, core).
Axes of the slice: x: 4, y: 4, z: 8, core: 2. Of those that a mesh axis runs over, the one named last changes fastest.
Arguments:
- mixer_in: bfloat16 [32768, 2048], P(('ep', 'tp')), may hold values from -6 to 6
- expert_in: bfloat16 [32768, 2048], P(('ep', 'tp')), may hold values from -6 to 6
- mixer_gain: float32 [2048], replicated, may hold values from 0.1 to 1.9
- w_outer: bfloat16 [2048, 2048], P(None, 'tp'), may hold values from -0.125 to 0.125
- w_inner: bfloat16 [2048, 2048], P(None, 'tp'), may hold values from -0.125 to 0.125
- w_value: bfloat16 [2048, 2048], P(None, 'tp'), may hold values from -0.125 to 0.125
- conv_taps: float32 [3, 2048], P(None, 'tp'), may hold values from -3 to 3
- w_mix_out: bfloat16 [2048, 2048], P('tp'), may hold values from -0.125 to 0.125
- expert_gain: float32 [2048], replicated, may hold values from 0.1 to 1.9
- w_gate: bfloat16 [32, 2048, 2048], P('ep', None, 'tp'), may hold values from -0.375 to 0.375
- w_up: bfloat16 [32, 2048, 2048], P('ep', None, 'tp'), may hold values from -0.375 to 0.375
- w_down: bfloat16 [32, 2048, 2048], P('ep', 'tp'), may hold values from -0.02734375 to 0.02734375
- route_ids: int32 [32768, 2], P(('ep', 'tp')), may hold values from 0 to 31, all different within a row; in each aligned block of 128 rows (0 to 127, 128 to 255, ...) at most 10 rows name the same one
- route_weights: float32 [32768, 2], P(('ep', 'tp')), may hold values from 0.2 to 1
Outputs:
- mixer_out: bfloat16 [32768, 2048], P(('ep', 'tp'))
- expert_out: bfloat16 [32768, 2048], P(('ep', 'tp'))
Inputs may be any that keep to these rules, and one draw needn't show every extreme that they name: `route_ids`: each row names 2 different experts. Among the 128 rows of one device no expert is named more than 10 times, and in every draw some device names some expert exactly 10 times.
All inputs are finite; a program needn't handle non-finite values.
Results may differ from a plain program's by a relative error of at most 0.019.
Values may be sent and summed in bfloat16 or wider, within the bound.
A program may use at most 128 MiB of HBM per device.

v0:
```python
import jax
import jax.numpy as jnp
from jax import lax
from jax.sharding import Mesh
from jax.sharding import PartitionSpec as P

EXPERTS = 32
CAP = 10
TP = ("tp_0", "tp_1")
EP_TP = ("ep", "tp_0", "tp_1")


norm_eps = 1e-06
clamp_limit = 7.0
gate_alpha = 1.702


def from_behind(block, axis, distance):
    devices = range(lax.axis_size(axis))
    route = [(i - distance, i) for i in devices if i - distance in devices]
    return lax.ppermute(block, axis, route)


def cut_along(shard, dim, peers):
    before, after = (shard.shape[:dim], shard.shape[dim + 1 :])
    return jnp.moveaxis(shard.reshape(*before, peers, -1, *after), dim, 0)


def summed_rows_2(shard, chips, core, dim):
    sizes = (lax.axis_size(chips), lax.axis_size(core))
    pieces = cut_along(shard, dim, sizes[0] * sizes[1])
    inside = pieces.shape[1:]
    pieces = pieces.reshape(*sizes, *inside).swapaxes(0, 1).reshape(-1, *inside)
    pieces = lax.psum_scatter(pieces, core, scatter_dimension=0, tiled=True)
    return lax.psum_scatter(pieces, chips, scatter_dimension=0, tiled=True)[0]


def rms_scale(tok_rows, gain_vec):
    values = tok_rows.astype(jnp.float32)
    scaled = values * lax.rsqrt(jnp.mean(values * values, axis=-1, keepdims=True) + norm_eps)
    return (scaled * gain_vec).astype(jnp.bfloat16)


def project_rows(block_rows, w_outer, w_inner, w_value):
    outer_gate = jnp.dot(block_rows, w_outer, preferred_element_type=jnp.float32)
    inner_left = jnp.dot(block_rows, w_inner, preferred_element_type=jnp.float32)
    inner_right = jnp.dot(block_rows, w_value, preferred_element_type=jnp.float32)
    return jnp.concatenate((outer_gate, inner_left * inner_right), axis=1)


def gated_conv(projected, conv_taps):
    channels = conv_taps.shape[1]
    outer_gate = projected[:, :channels]
    inner_prod = projected[:, channels:]
    length = inner_prod.shape[0]
    prior_rows = from_behind(inner_prod[length - 2 :], "ep", 1)
    extended = jnp.concatenate((prior_rows, inner_prod), axis=0)
    conv_out = (
        conv_taps[2] * inner_prod
        + conv_taps[1] * extended[1 : length + 1]
        + conv_taps[0] * extended[:length]
    )
    return (outer_gate * conv_out).astype(jnp.bfloat16)


def expert_hidden(slot_rows, w_gate, w_up):
    gate_pre = jnp.einsum("nxcd,xdf->nxcf", slot_rows, w_gate, preferred_element_type=jnp.float32)
    up_pre = jnp.einsum("nxcd,xdf->nxcf", slot_rows, w_up, preferred_element_type=jnp.float32)
    gate_pre = jnp.minimum(gate_pre, clamp_limit)
    up_pre = jnp.clip(up_pre, -clamp_limit, clamp_limit)
    return ((up_pre + 1.0) * gate_pre * jax.nn.sigmoid(gate_alpha * gate_pre)).astype(jnp.bfloat16)


def down_rows(hidden_rows, w_down):
    return jnp.einsum("nxcf,xfd->nxcd", hidden_rows, w_down, preferred_element_type=jnp.float32)


def slot_index(route_ids, experts, capacity):
    flat_ids = route_ids.reshape(-1)
    member = (flat_ids[:, None] == jnp.arange(experts, dtype=jnp.int32)[None, :]).astype(jnp.int32)
    earlier = jnp.cumsum(member, axis=0) - member
    return flat_ids * capacity + jnp.sum(earlier * member, axis=1)


def per_device(
    mixer_in,
    expert_in,
    mixer_gain,
    w_outer,
    w_inner,
    w_value,
    conv_taps,
    w_mix_out,
    expert_gain,
    w_gate,
    w_up,
    w_down,
    route_ids,
    route_weights,
):
    ep_count = lax.axis_size("ep")
    tok_count, model_width = expert_in.shape
    local_experts = w_gate.shape[0]
    top_count = route_ids.shape[1]
    slot_total = EXPERTS * CAP
    normed_mix = rms_scale(mixer_in, mixer_gain)
    normed_exp = rms_scale(expert_in, expert_gain)
    slot_ids = slot_index(route_ids, EXPERTS, CAP)
    placing = slot_ids[None, :] == jnp.arange(slot_total, dtype=jnp.int32)[:, None]
    placing = jnp.sum(placing.reshape(slot_total, tok_count, top_count).astype(jnp.int32), axis=2)
    packed = jnp.dot(placing.astype(jnp.bfloat16), normed_exp, preferred_element_type=jnp.float32)
    packed = packed.astype(jnp.bfloat16).reshape(ep_count, slot_total // ep_count, model_width)
    arrived = lax.all_to_all(packed, "ep", split_axis=0, concat_axis=0, tiled=True)
    arrived = arrived.reshape(ep_count, local_experts, CAP, model_width)
    projected = project_rows(
        lax.all_gather(normed_mix, TP, axis=0, tiled=True), w_outer, w_inner, w_value
    )
    gated_rows = gated_conv(projected, conv_taps)
    mixer_sum = summed_rows_2(
        jnp.dot(gated_rows, w_mix_out, preferred_element_type=jnp.float32).astype(jnp.bfloat16),
        "tp_0",
        "tp_1",
        0,
    ).astype(jnp.float32)
    hidden_all = expert_hidden(lax.all_gather(arrived, TP, axis=0, tiled=True), w_gate, w_up)
    expert_sum = lax.psum_scatter(
        down_rows(hidden_all, w_down).astype(jnp.bfloat16), TP, scatter_dimension=0, tiled=True
    )
    mixer_out = mixer_sum.astype(jnp.bfloat16)
    expert_value = expert_sum.reshape(ep_count, slot_total // ep_count, model_width)
    returned = lax.all_to_all(expert_value, "ep", split_axis=0, concat_axis=0, tiled=True).reshape(
        slot_total, model_width
    )
    picked = jnp.take(returned, slot_ids.reshape(tok_count, top_count), axis=0)
    expert_out = jnp.sum(picked.astype(jnp.float32) * route_weights[:, :, None], axis=1).astype(
        jnp.bfloat16
    )
    return (mixer_out, expert_out)


def solution(mesh):
    finer = Mesh(mesh.devices.reshape(mesh.shape["ep"], 8, 2), ("ep", "tp_0", "tp_1"))
    return jax.shard_map(
        per_device,
        mesh=finer,
        in_specs=(
            P(EP_TP, None),
            P(EP_TP, None),
            P(),
            P(None, TP),
            P(None, TP),
            P(None, TP),
            P(None, TP),
            P(TP, None),
            P(),
            P("ep", None, TP),
            P("ep", None, TP),
            P("ep", TP, None),
            P(EP_TP, None),
            P(EP_TP, None),
        ),
        out_specs=(P(EP_TP, None), P(EP_TP, None)),
        check_vma=False,
    )
```

profile of v0, /device:TPU:1, one launch (start us, length us, event | category | flops | bytes accessed | tf_op | source)
XLA Modules:
  0.0 401.9 jit_solution(1218993182549316100)
XLA Ops:
  7.2 0.0 all-gather.3.cloned.1.call-start
  7.2 1.3 fusion.7
  8.6 2.0 fusion.9
  10.6 0.0 all-gather.3.cloned.1.call-update
  10.6 0.0 all-gather.5.cloned.1.call-start
  10.7 0.8 copy.42
  11.5 0.1 eq.43
  11.6 0.1 eq.39
  11.8 0.6 reduce-window.6
  12.4 0.2 slice_reduce_fusion
  12.6 0.1 fusion.28
  12.7 0.1 reduce_sum.49
  12.9 0.1 copy.45
  12.9 0.7 compare_and_fusion
  13.7 0.2 fusion.10
  13.9 1.7 convolution_convert_fusion.1
  15.5 2.2 reshape.82
  17.8 29.0 %all_to_all.10 = bf16[16,20,2048]{2,1,0:T(8,128)(2,1)S(1)} all-to-all(bf16[16,20,2048]{2,1,0:T(8,128)(2,1)S(1)} %reshape.82), channel_id=1, replica_groups=mesh['ep'=16,'tp_0'=8,'tp_1'=2] {'ep'}, dimensions={0} | all-to-all | bytes 2621440 | tf_op jit(solution)/shard_map/all_to_all | solution.py:113
  46.8 1.8 copy.47
  48.6 0.0 reduce-scatter.4.cloned.1.call-start
  48.7 22.2 %all-gather.3.cloned.1.call-done = bf16[2048,2048]{1,0:T(8,128)(2,1)} async-done(((bf16[128,2048]{1,0:T(8,128)(2,1)}), bf16[2048,2048]{1,0:T(8,128)(2,1)}) %all-gather.3.cloned.1.call-update) | async-done | bytes 8388624 | tf_op jit(solution)/shard_map/all_gather | solution.py:116
  70.8 5.9 %fusion.33 = f32[2048,128]{1,0:T(8,128)S(1)} fusion(bf16[2048,2048]{1,0:T(8,128)(2,1)} %all-gather.3.cloned.1.call-done, bf16[2048,128]{1,0:T(8,128)(2,1)S(1)} %copy-done.10), kind=kOutput, calls=%fused_computation.61 | convolution fusion | flops 1073741824 | bytes 9961472 | tf_op jit(solution)/shard_map/dot_general | solution.py:46
  76.8 2.4 convolution_multiply_fusion
  79.2 3.1 collective-permute-start
  82.4 0.7 collective-permute-done
  83.0 13.1 %convolution_convert_fusion = bf16[2048,2048]{1,0:T(8,128)(2,1)} fusion(bf16[128,2048]{1,0:T(8,128)(2,1)S(1)} %copy-done.4, f32[2,128]{1,0:T(2,128)S(1)} %collective-permute-done, f32[2048,128]{1,0:T(8,128)S(1)} %convolution_multiply_fusion, f32[128]{0:T(128)S(1)} %get-tuple-element.5, f32[128]{0:T(128)S(1)} %get-tuple-element.6, ...), kind=kOutput, calls=%fused_computation.2 | convolution fusion | flops 2154037248 | bytes 18876928 | tf_op jit(solution)/shard_map/dot_general | solution.py:120
  96.2 8.5 %copy.41 = bf16[2,8,128,2048]{3,2,1,0:T(8,128)(2,1)} copy(bf16[2,8,128,2048]{3,2,0,1:T(8,128)(2,1)} %bitcast.62) | data formatting | bytes 16777216 | tf_op jit(solution)/shard_map/transpose | solution.py:33
  104.7 0.2 reduce-scatter.8.cloned.1.call-start
  105.0 81.4 %all-gather.5.cloned.1.call-done = bf16[256,2,10,2048]{3,0,2,1:T(8,128)(2,1)} async-done(((bf16[16,2,10,2048]{3,0,2,1:T(8,128)(2,1)}), bf16[256,2,10,2048]{3,0,2,1:T(8,128)(2,1)}) %all-gather.5.cloned.1.call-update) | async-done | bytes 20971536 | tf_op jit(solution)/shard_map/all_gather | solution.py:125
  186.4 9.9 %fusion.16 = f32[2,256,10,128]{3,1,2,0:T(8,128)S(1)} fusion(bf16[256,2,10,2048]{3,0,2,1:T(8,128)(2,1)} %all-gather.5.cloned.1.call-done, bf16[2,2048,128]{2,1,0:T(8,128)(2,1)S(1)} %copy-done.8), kind=kOutput, calls=%fused_computation.31 | convolution fusion | flops 2684354560 | bytes 24641536 | tf_op jit(solution)/shard_map/nxcd,xdf->nxcf/dot_general | solution.py:68
  196.3 13.1 %fusion = bf16[256,2,10,128]{3,0,2,1:T(8,128)(2,1)S(1)} fusion(bf16[256,2,10,2048]{3,0,2,1:T(8,128)(2,1)} %all-gather.5.cloned.1.call-done, f32[2,256,10,128]{3,1,2,0:T(8,128)S(1)} %fusion.16, bf16[2,2048,128]{2,1,0:T(8,128)(2,1)S(1)} %copy-done.9), kind=kOutput, calls=%fused_computation.8 | convolution fusion | flops 2690908160 | bytes 25952256 | tf_op jit(solution)/shard_map/nxcd,xdf->nxcf/dot_general | solution.py:67
  209.5 9.9 %convert_bitcast_fusion = bf16[256,2,10,2048]{3,0,2,1:T(8,128)(2,1)} fusion(bf16[256,2,10,128]{3,0,2,1:T(8,128)(2,1)S(1)} %fusion, bf16[2,128,2048]{2,1,0:T(8,128)(2,1)S(1)} %copy-done), kind=kOutput, calls=%fused_computation.1 | convolution fusion | flops 2694840320 | bytes 23330816 | tf_op jit(solution)/shard_map/nxcf,xfd->nxcd/dot_general | solution.py:75
  219.4 0.0 reduce-scatter.6.cloned.1.call-start
  219.4 0.0 reduce-scatter.4.cloned.1.call-done
  219.5 0.5 reduce-scatter.6.cloned.1.call-update
  220.0 117.5 %reduce-scatter.8.cloned.1.call-done = bf16[16,2,10,2048]{3,0,2,1:T(8,128)(2,1)} async-done(((bf16[256,2,10,2048]{3,0,2,1:T(8,128)(2,1)}), bf16[16,2,10,2048]{3,0,2,1:T(8,128)(2,1)}) %reduce-scatter.8.cloned.1.call-update) | async-done | bytes 1310736 | tf_op jit(solution)/shard_map/reduce_scatter | solution.py:126
  337.5 3.2 copy.48
  340.7 6.6 %all-to-all-start.1 = ((bf16[16,20,2048]{2,1,0:T(8,128)(2,1)}), bf16[16,20,2048]{2,1,0:T(8,128)(2,1)}, u32[]{:S(2)}, u32[]{:S(2)}) async-start(bf16[16,20,2048]{2,1,0:T(8,128)(2,1)} %copy.48), calls=%async_computation.4 | async-start | bytes 3145728 | tf_op jit(solution)/shard_map/all_to_all | solution.py:131
  347.3 0.1 copy.49
  347.4 0.1 reshape.88
  347.6 0.1 copy.46
  347.7 0.1 copy.50
  347.8 20.1 %all-to-all-done.1 = bf16[16,20,2048]{2,1,0:T(8,128)(2,1)} async-done(((bf16[16,20,2048]{2,1,0:T(8,128)(2,1)}), bf16[16,20,2048]{2,1,0:T(8,128)(2,1)}, u32[]{:S(2)}, u32[]{:S(2)}) %all-to-all-start.1) | async-done | bytes 1310752 | tf_op jit(solution)/shard_map/all_to_all | solution.py:131
  368.0 2.3 reshape.85
  370.3 1.4 gather_fusion
  371.6 0.7 reshape.87
  372.3 4.9 %multiply_reduce_fusion = bf16[128,2048]{1,0:T(8,128)(2,1)} fusion(bf16[128,2,2048]{2,1,0:T(2,128)(2,1)S(1)} %reshape.87, pred[128,2]{1,0:T(8,128)(4,1)S(1)} %copy.46, f32[128,2]{1,0:T(8,128)S(1)} %copy.50), kind=kLoop, calls=%fused_computation.6 | loop fusion | flops 1835008 | bytes 1574144 | tf_op jit(solution)/shard_map/reduce_sum | solution.py:135
  377.3 18.1 %reduce-scatter.6.cloned.1.call-done = bf16[1,128,2048]{2,1,0:T(8,128)(2,1)} async-done(((bf16[8,128,2048]{2,1,0:T(8,128)(2,1)}), bf16[1,128,2048]{2,1,0:T(8,128)(2,1)}) %reduce-scatter.6.cloned.1.call-update) | async-done | bytes 524304 | tf_op jit(solution)/shard_map/reduce_scatter | solution.py:35
  (35 shorter events, 0.2 us)
Async XLA Ops:
  7.2 202.3 %copy-start = (bf16[2,128,2048]{2,1,0:T(8,128)(2,1)S(1)}, bf16[2,128,2048]{2,1,0:T(8,128)(2,1)}, u32[]{:S(2)}) copy-start(bf16[2,128,2048]{2,1,0:T(8,128)(2,1)} %param.25) | copy-start | bytes 3145732
  7.2 6.5 %copy-start.2 = (bf16[128,2048]{1,0:T(8,128)(2,1)S(1)}, bf16[128,2048]{1,0:T(8,128)(2,1)}, u32[]{:S(2)}) copy-start(bf16[128,2048]{1,0:T(8,128)(2,1)} %param.15) | copy-start | bytes 1572868
  7.2 6.7 %copy-start.5 = (f32[2048]{0:T(1024)S(1)}, f32[2048]{0:T(1024)}, u32[]{:S(2)}) copy-start(f32[2048]{0:T(1024)} %param.22) | copy-start | bytes 24580
  7.2 63.6 %all-gather.3.cloned.1.call-start = ((), (), s32[]{:S(2)}) async-start(), calls=%async_computation.5 | async-start | bytes 8912896 | tf_op jit(solution)/shard_map/all_gather | solution.py:116
  10.6 175.7 %all-gather.5.cloned.1.call-start = ((), (), s32[]{:S(2)}) async-start(), calls=%async_computation.8 | async-start | bytes 22282240 | tf_op jit(solution)/shard_map/all_gather | solution.py:125
  46.8 24.1 %copy-start.10 = (bf16[2048,128]{1,0:T(8,128)(2,1)S(1)}, bf16[2048,128]{1,0:T(8,128)(2,1)}, u32[]{:S(2)}) copy-start(bf16[2048,128]{1,0:T(8,128)(2,1)} %param.18) | copy-start | bytes 1572868
  48.6 28.2 %copy-start.3 = (bf16[2048,128]{1,0:T(8,128)(2,1)S(1)}, bf16[2048,128]{1,0:T(8,128)(2,1)}, u32[]{:S(2)}) copy-start(bf16[2048,128]{1,0:T(8,128)(2,1)} %param.19) | copy-start | bytes 1572868
  48.6 170.8 %reduce-scatter.4.cloned.1.call-start = ((), (), s32[]{:S(2)}) async-start(), calls=%async_computation.6 | async-start | bytes 12582912 | tf_op jit(solution)/shard_map/reduce_scatter | solution.py:34
  70.8 5.9 %copy-start.1 = (bf16[2048,2048]{1,0:T(8,128)(2,1)S(1)}, bf16[2048,2048]{1,0:T(8,128)(2,1)}, u32[]{:S(2)}) copy-start(bf16[2048,2048]{1,0:T(8,128)(2,1)} %all-gather.3.cloned.1.call-done) | copy-start | bytes 25165828
  76.8 5.6 %copy-start.6 = (f32[3,128]{1,0:T(4,128)S(1)}, f32[3,128]{1,0:T(4,128)}, u32[]{:S(2)}) copy-start(f32[3,128]{1,0:T(4,128)} %param.20) | copy-start | bytes 4612
  76.8 6.3 %copy-start.4 = (bf16[128,2048]{1,0:T(8,128)(2,1)S(1)}, bf16[128,2048]{1,0:T(8,128)(2,1)}, u32[]{:S(2)}) copy-start(bf16[128,2048]{1,0:T(8,128)(2,1)} %param.21) | copy-start | bytes 1572868
  79.2 3.8 collective-permute-start
  104.7 81.7 %copy-start.8 = (bf16[2,2048,128]{2,1,0:T(8,128)(2,1)S(1)}, bf16[2,2048,128]{2,1,0:T(8,128)(2,1)}, u32[]{:S(2)}) copy-start(bf16[2,2048,128]{2,1,0:T(8,128)(2,1)} %param.24) | copy-start | bytes 3145732
  104.7 91.6 %copy-start.9 = (bf16[2,2048,128]{2,1,0:T(8,128)(2,1)S(1)}, bf16[2,2048,128]{2,1,0:T(8,128)(2,1)}, u32[]{:S(2)}) copy-start(bf16[2,2048,128]{2,1,0:T(8,128)(2,1)} %param.23) | copy-start | bytes 3145732
  104.7 232.7 %reduce-scatter.8.cloned.1.call-start = ((), (), s32[]{:S(2)}) async-start(), calls=%async_computation.9 | async-start | bytes 22282240 | tf_op jit(solution)/shard_map/reduce_scatter | solution.py:126
  219.4 176.0 %reduce-scatter.6.cloned.1.call-start = ((), (), s32[]{:S(2)}) async-start(), calls=%async_computation.7 | async-start | bytes 4718592 | tf_op jit(solution)/shard_map/reduce_scatter | solution.py:35
  337.5 10.2 %copy-start.7 = (f32[128,2]{0,1:T(2,128)S(1)}, f32[128,2]{0,1:T(2,128)}, u32[]{:S(2)}) copy-start(f32[128,2]{0,1:T(2,128)} %param.27) | copy-start | bytes 3076
  340.7 27.2 %all-to-all-start.1 = ((bf16[16,20,2048]{2,1,0:T(8,128)(2,1)}), bf16[16,20,2048]{2,1,0:T(8,128)(2,1)}, u32[]{:S(2)}, u32[]{:S(2)}) async-start(bf16[16,20,2048]{2,1,0:T(8,128)(2,1)} %copy.48), calls=%async_computation.4 | async-start | bytes 3145728 | tf_op jit(solution)/shard_map/all_to_all | solution.py:131
Sparse Core Ops, SparseCore 0:
  10.8 60.0 all-gather.2
  72.7 113.6 all-gather.4
  188.9 20.5 reduce-scatter.3
  219.5 117.9 reduce-scatter.7
  340.4 54.8 reduce-scatter.5
where the time goes:
time: 402 us
  waiting for transfers between devices  261 us (65%)
  matrix products  56 us (14%)
  blocking collectives  29 us (7%)
  local copies, waits for them, and re-layouts  22.2 us (6%)
  between operations  14 us (3%)
  starting transfers between devices  10.1 us (3%)
  other arithmetic  9.98 us (2%)
    reduce_scatter x1, waiting for transfers between devices, per_device(): lax.psum_scatter(down_rows(hidden_all, w_down).astype(jnp.bfloat16), TP,...  118 us
    all_gather x1, waiting for transfers between devices, per_device(): lax.all_gather(arrived, TP, axis=0, tiled=True)  81.4 us
    all_to_all x1, blocking collectives, per_device(): lax.all_to_all(packed, 'ep', split_axis=0, concat_axis=0, tiled=True)  29 us
    all_gather x1, waiting for transfers between devices, per_device(): lax.all_gather(normed_mix, TP, axis=0, tiled=True)  22.2 us
    all_to_all x1, waiting for transfers between devices, per_device(): lax.all_to_all(expert_value, 'ep', split_axis=0, concat_axis=0, tiled=True)  20.1 us
    reduce_scatter x1, waiting for transfers between devices, summed_rows_2(): return lax.psum_scatter(pieces, chips, scatter_dimension=0, tiled=True)[0]  18.1 us
    dot_general x1, matrix products, per_device(): jnp.dot(gated_rows, w_mix_out, preferred_element_type=jnp.float32)  13.1 us
    dot_general x1, matrix products, expert_hidden(): jnp.einsum('nxcd,xdf->nxcf', slot_rows, w_gate, preferred_element_type=jn...  13.1 us
  transfers between devices with their start and end apart: 7, of which 6 were waited for; matrix products, arithmetic and copies ran while one was open for 21% of the time, Pallas kernels for 0%

commit v1 on v0

v1 whole, which is shorter than its diff:
```python
import functools

import jax
import jax.numpy as jnp
from jax import lax
from jax.experimental import pallas as pl
from jax.experimental.pallas import tpu as pltpu
from jax.sharding import Mesh
from jax.sharding import PartitionSpec as P

EXPERTS = 32
CAP = 10
PAD = 16
EP = 16
NZ = 8
LOCAL = 2
ROWS = EP * CAP
TP = ("tp_0", "tp_1")
EP_TP = ("ep", "tp_0", "tp_1")
MESH = pl.DeviceIdType.MESH
F32 = jnp.float32
BF16 = jnp.bfloat16

norm_eps = 1e-06
clamp_limit = 7.0
gate_alpha = 1.702


def rms_scale(tok_rows, gain_vec):
    values = tok_rows.astype(F32)
    scaled = values * lax.rsqrt(jnp.mean(values * values, axis=-1, keepdims=True) + norm_eps)
    return (scaled * gain_vec).astype(BF16)


def places():
    return lax.axis_index("ep"), lax.axis_index("tp_0"), lax.axis_index("tp_1")


def greet(ep, z, core):
    barrier = pltpu.get_barrier_semaphore()

    def one(k, _):
        pl.semaphore_signal(
            barrier, inc=1, device_id=(lax.rem(ep + k, EP), z, core), device_id_type=MESH
        )
        return 0

    lax.fori_loop(1, EP, one, 0)
    for step in (1, NZ - 1):
        pl.semaphore_signal(
            barrier, inc=1, device_id=(ep, lax.rem(z + step, NZ), core), device_id_type=MESH
        )
    pl.semaphore_signal(barrier, inc=1, device_id=(ep, z, 1 - core), device_id_type=MESH)
    pl.semaphore_wait(barrier, EP + 2)


def remote(src, dst, send, recv, where):
    return pltpu.make_async_remote_copy(
        src_ref=src, dst_ref=dst, send_sem=send, recv_sem=recv, device_id=where, device_id_type=MESH
    )


GATHER_D = (1, 1, 2, 2, 3, 3, 4)
GATHER_X = ((0, 1, 0, 1, 0, 1, 0), (0, 1, 0, 1, 0, 1, 1))
SCATTER_D = (4, 3, 3, 2, 2, 1, 1)
SCATTER_X = ((0, 1, 0, 1, 0, 1, 0), (1, 0, 1, 0, 1, 1, 0))
SCATTER_IN = ((None, None, 0, 1, 2, 3, 4), (None, None, 0, 1, 2, 4, 3))
LAST_IN = {1: (5, 5), 0: (6, 6)}
STEPS = 7


def gather_kernel(
    slots, w_gate, w_up, hid,
    units, landed, w_both,
    w_sem, a_send, a_recv, r_send, r_recv, c_send, c_recv,
):
    ep, z, core = places()
    loads = []
    for x in range(LOCAL):
        loads.append(pltpu.make_async_copy(w_gate.at[x], w_both.at[x, :, 0:128], w_sem.at[x, 0]))
        loads.append(pltpu.make_async_copy(w_up.at[x], w_both.at[x, :, 128:256], w_sem.at[x, 1]))
    for load in loads:
        load.start()
    greet(ep, z, core)

    def exchange(x, k):
        to = lax.rem(ep + k, EP)
        return remote(
            slots.at[x, to], landed.at[x, ep], a_send.at[x, k], a_recv.at[x, k], (to, z, core)
        )

    for x in range(LOCAL):

        def send_one(k, _, x=x):
            exchange(x, k).start()
            return 0

        lax.fori_loop(1, EP, send_one, 0)
    for load in loads:
        load.wait()
    for x in range(LOCAL):
        landed[x, ep] = slots[x, ep]

    row = lax.broadcasted_iota(jnp.int32, (ROWS, EP * PAD), 0)
    col = lax.broadcasted_iota(jnp.int32, (ROWS, EP * PAD), 1)
    picks = ((row // CAP) * PAD + row % CAP == col).astype(BF16)

    def compute(at_z, at_core, x):
        tok = units[at_z, at_core, x]
        both = jnp.dot(tok, w_both[x], preferred_element_type=F32)
        gate_pre = jnp.minimum(both[:, 0:128], clamp_limit)
        up_pre = jnp.clip(both[:, 128:256], -clamp_limit, clamp_limit)
        hid[at_z, at_core, x] = (
            (up_pre + 1.0) * gate_pre * jax.nn.sigmoid(gate_alpha * gate_pre)
        ).astype(BF16)

    steps = (NZ - 1, 1)

    def ring_copy(way, n):
        at = lax.rem(z + (GATHER_D[n] - 1) * steps[way], NZ)
        x = GATHER_X[way][n]
        there = lax.rem(z + (NZ - steps[way]), NZ)
        return remote(
            units.at[at, core, x], units.at[at, core, x],
            r_send.at[way, n], r_recv.at[way, n], (ep, there, core),
        )

    def across(way, n):
        at = z if n == STEPS else lax.rem(z + GATHER_D[n] * steps[way], NZ)
        x = way if n == STEPS else GATHER_X[way][n]
        ref = units.at[at, core, x]
        return remote(ref, ref, c_send.at[way, n], c_recv.at[way, n], (ep, z, 1 - core)), at, x

    for x in range(LOCAL):

        def wait_one(k, _, x=x):
            exchange(x, k).wait_recv()
            return 0

        lax.fori_loop(1, EP, wait_one, 0)

        def pack(j, _, x=x):
            cols = pl.ds(pl.multiple_of(j * 512, 512), 512)
            src = landed[x, :, :, cols].reshape(EP * PAD, 512)
            units[z, core, x, :, cols] = jnp.dot(picks, src, preferred_element_type=F32).astype(BF16)
            return 0

        lax.fori_loop(0, 4, pack, 0)
        for way in range(2):
            ring_copy(way, x).start()
        across(x, STEPS)[0].start()
    for x in range(LOCAL):
        compute(z, core, x)

    for n in range(STEPS):
        for way in range(2):
            ring_copy(way, n).wait_recv()
            nxt = 6 if (way, n) == (1, 5) else n + 2
            if nxt < STEPS and GATHER_X[way][nxt] == GATHER_X[way][n] and GATHER_D[nxt] == GATHER_D[n] + 1:
                ring_copy(way, nxt).start()
            across(way, n)[0].start()
        for way in range(2):
            at = lax.rem(z + GATHER_D[n] * steps[way], NZ)
            compute(at, core, GATHER_X[way][n])
        for way in range(2):
            copy, at, x = across(way, STEPS if n == 0 else n - 1)
            copy.wait_recv()
            compute(at, 1 - core, x)
    for way in range(2):
        copy, at, x = across(way, STEPS - 1)
        copy.wait_recv()
        compute(at, 1 - core, x)
    for way in range(2):
        for n in range(STEPS):
            ring_copy(way, n).wait_send()
            across(way, n)[0].wait_send()
        across(way, STEPS)[0].wait_send()
    for x in range(LOCAL):

        def done_one(k, _, x=x):
            exchange(x, k).wait_send()
            return 0

        lax.fori_loop(1, EP, done_one, 0)


def scatter_kernel(
    hid, w_down, back,
    c_out, c_in, r_out, r_in, b_out,
    c_send, c_recv, r_send, r_recv, a_send, a_recv,
):
    ep, z, core = places()
    greet(ep, z, core)
    steps = (1, NZ - 1)

    def place(way, m):
        if m == STEPS:
            return z, way
        return lax.rem(z + SCATTER_D[m] * steps[way], NZ), SCATTER_X[way][m]

    def across(way, m):
        return remote(
            c_out.at[way, m], c_in.at[way, m], c_send.at[way, m], c_recv.at[way, m],
            (ep, z, 1 - core),
        )

    def ring_copy(way, m):
        return remote(
            r_out.at[way, m], r_in.at[way, m], r_send.at[way, m], r_recv.at[way, m],
            (ep, lax.rem(z + steps[way], NZ), core),
        )

    def partial(at, at_core, x, add, out):
        def tile(j, _):
            cols = pl.ds(pl.multiple_of(j * 512, 512), 512)
            total = jnp.dot(hid[at, at_core, x], w_down[x, :, cols], preferred_element_type=F32)
            for ref in add:
                total = total + ref[:, cols].astype(F32)
            out[:, cols] = total.astype(BF16)
            return 0

        lax.fori_loop(0, 4, tile, 0)

    def help_other(m):
        for way in range(2):
            at, x = place(way, m)
            partial(at, 1 - core, x, (), c_out.at[way, m])
            across(way, m).start()

    help_other(0)
    help_other(1)
    for m in range(STEPS):
        for way in range(2):
            at, x = place(way, m)
            add = [c_in.at[way, m]]
            across(way, m).wait_recv()
            came = SCATTER_IN[way][m]
            if came is not None:
                ring_copy(way, came).wait_recv()
                add.append(r_in.at[way, came])
            partial(at, core, x, add, r_out.at[way, m])
            ring_copy(way, m).start()
        if m + 2 <= STEPS:
            help_other(m + 2)

    row = lax.broadcasted_iota(jnp.int32, (EP * PAD, ROWS), 0)
    col = lax.broadcasted_iota(jnp.int32, (EP * PAD, ROWS), 1)
    spread = ((row // PAD) * CAP + row % PAD == col) & (row % PAD < CAP)
    spread = spread.astype(BF16)

    def exchange(x, k):
        to = lax.rem(ep + k, EP)
        return remote(
            b_out.at[x, to], back.at[x, ep], a_send.at[x, k], a_recv.at[x, k], (to, z, core)
        )

    for x in (1, 0):
        across(x, STEPS).wait_recv()
        for way in range(2):
            ring_copy(way, LAST_IN[x][way]).wait_recv()

        def tile(j, _, x=x):
            cols = pl.ds(pl.multiple_of(j * 512, 512), 512)
            total = jnp.dot(hid[z, core, x], w_down[x, :, cols], preferred_element_type=F32)
            for ref in (c_in.at[x, STEPS], r_in.at[0, LAST_IN[x][0]], r_in.at[1, LAST_IN[x][1]]):
                total = total + ref[:, cols].astype(F32)
            wide = jnp.dot(spread, total.astype(BF16), preferred_element_type=F32).astype(BF16)
            b_out[x, :, :, cols] = wide.reshape(EP, PAD, 512)
            return 0

        lax.fori_loop(0, 4, tile, 0)

        def send_one(k, _, x=x):
            exchange(x, k).start()
            return 0

        lax.fori_loop(1, EP, send_one, 0)
        back[x, ep] = b_out[x, ep]
    for way in range(2):
        for m in range(STEPS):
            ring_copy(way, m).wait_send()
            across(way, m).wait_send()
        across(way, STEPS).wait_send()
    for x in (1, 0):

        def end_one(k, _, x=x):
            exchange(x, k).wait()
            return 0

        lax.fori_loop(1, EP, end_one, 0)


def mixer_kernel(tok, taps, blocks, out, total):
    step = pl.program_id(0)

    @pl.when(step == 0)
    def _():
        total[...] = jnp.zeros_like(total)

    rows = tok[...]
    outer, inner, value = (
        jnp.dot(rows, blocks[:, 0, 0, i].reshape(2048, 128), preferred_element_type=F32)
        for i in range(3)
    )
    prod = inner * value
    conv = taps[2:3] * prod[16:144] + taps[1:2] * prod[15:143] + taps[0:1] * prod[14:142]
    gated = (outer[16:144] * conv).astype(BF16)
    for e in range(EP):
        cols = slice(e * 128, (e + 1) * 128)
        total[:, cols] += jnp.dot(gated, blocks[e, 0, 0, 3], preferred_element_type=F32)

    @pl.when(step == pl.num_programs(0) - 1)
    def _():
        out[...] = total[...].astype(BF16)


def slot_index(route_ids, experts, capacity):
    flat_ids = route_ids.reshape(-1)
    member = (flat_ids[:, None] == jnp.arange(experts, dtype=jnp.int32)[None, :]).astype(jnp.int32)
    earlier = jnp.cumsum(member, axis=0) - member
    place = jnp.sum(earlier * member, axis=1)
    return (flat_ids % LOCAL) * (EP * PAD) + (flat_ids // LOCAL) * PAD + place


DMA = pltpu.SemaphoreType.DMA


def per_device(
    mixer_in, expert_in, mixer_gain, w_outer, w_inner, w_value, conv_taps, w_mix_out,
    expert_gain, w_gate, w_up, w_down, route_ids, route_weights,
):
    tok_count, width = expert_in.shape
    ep, z, core = places()

    part = jnp.stack(
        [lax.dynamic_slice_in_dim(w, ep * 128, 128, 0) for w in (w_outer, w_inner, w_value)]
        + [lax.dynamic_slice_in_dim(w_mix_out, ep * 128, 128, 1)]
    )
    part = lax.all_gather(part, "tp_0", axis=0, tiled=False)
    blocks = lax.all_gather(part, ("ep", "tp_1"), axis=0, tiled=False)
    blocks = blocks.reshape(EP, 2, NZ, 4, 128, 128)
    taps = lax.all_gather(conv_taps, TP, axis=0, tiled=False)

    normed_mix = rms_scale(mixer_in, mixer_gain)
    count = EP * NZ * 2
    before = lax.ppermute(normed_mix[tok_count - 16 :], EP_TP, [(i, i + 1) for i in range(count - 1)])
    mix_rows = jnp.concatenate((before, normed_mix), axis=0)

    normed_exp = rms_scale(expert_in, expert_gain)
    slot_ids = slot_index(route_ids, EXPERTS, CAP).reshape(tok_count, 2)
    wide = LOCAL * EP * PAD
    every = jnp.arange(wide, dtype=jnp.int32)
    placing = (every[:, None] == slot_ids[None, :, 0]) | (every[:, None] == slot_ids[None, :, 1])
    slots = jnp.dot(placing.astype(BF16), normed_exp, preferred_element_type=F32).astype(BF16)
    slots = slots.reshape(LOCAL, EP, PAD, width)

    vmem = pl.BlockSpec(memory_space=pltpu.VMEM)
    anywhere = pl.BlockSpec(memory_space=pl.ANY)
    hid = pl.pallas_call(
        gather_kernel,
        out_shape=jax.ShapeDtypeStruct((NZ, 2, LOCAL, ROWS, 128), BF16),
        in_specs=[vmem, anywhere, anywhere],
        out_specs=vmem,
        scratch_shapes=[
            pltpu.VMEM((NZ, 2, LOCAL, ROWS, width), BF16),
            pltpu.VMEM((LOCAL, EP, PAD, width), BF16),
            pltpu.VMEM((LOCAL, width, 256), BF16),
            DMA((LOCAL, 2)), DMA((LOCAL, EP)), DMA((LOCAL, EP)),
            DMA((2, STEPS)), DMA((2, STEPS)), DMA((2, STEPS + 1)), DMA((2, STEPS + 1)),
        ],
        cost_estimate=pl.CostEstimate(flops=6 * 10**9, bytes_accessed=3 * 10**8, transcendentals=0),
        compiler_params=pltpu.CompilerParams(
            collective_id=0, has_side_effects=True, vmem_limit_bytes=40 * 2**20
        ),
        name="gather_experts",
    )(slots, w_gate, w_up)
    back = pl.pallas_call(
        scatter_kernel,
        out_shape=jax.ShapeDtypeStruct((LOCAL, EP, PAD, width), BF16),
        in_specs=[vmem, vmem],
        out_specs=vmem,
        scratch_shapes=[
            pltpu.VMEM((2, STEPS + 1, ROWS, width), BF16),
            pltpu.VMEM((2, STEPS + 1, ROWS, width), BF16),
            pltpu.VMEM((2, STEPS, ROWS, width), BF16),
            pltpu.VMEM((2, STEPS, ROWS, width), BF16),
            pltpu.VMEM((LOCAL, EP, PAD, width), BF16),
            DMA((2, STEPS + 1)), DMA((2, STEPS + 1)), DMA((2, STEPS)), DMA((2, STEPS)),
            DMA((LOCAL, EP)), DMA((LOCAL, EP)),
        ],
        cost_estimate=pl.CostEstimate(flops=6 * 10**9, bytes_accessed=3 * 10**8, transcendentals=0),
        compiler_params=pltpu.CompilerParams(
            collective_id=1, has_side_effects=True, vmem_limit_bytes=56 * 2**20
        ),
        name="scatter_experts",
    )(hid, w_down)

    hit = [every[None, :] == slot_ids[:, k : k + 1] for k in range(2)]
    weights = sum(jnp.where(hit[k], route_weights[:, k : k + 1], 0.0) for k in range(2))
    high = lax.reduce_precision(weights, 8, 7)
    low = lax.reduce_precision(weights - high, 8, 7)
    both = jnp.concatenate((high, low), axis=0).astype(BF16)
    sums = jnp.dot(both, back.reshape(wide, width), preferred_element_type=F32)
    expert_out = (sums[:tok_count] + sums[tok_count:]).astype(BF16)

    mixer_out = pl.pallas_call(
        mixer_kernel,
        grid=(NZ * 2,),
        out_shape=jax.ShapeDtypeStruct((tok_count, width), BF16),
        in_specs=[
            pl.BlockSpec((tok_count + 16, width), lambda t: (0, 0)),
            pl.BlockSpec((None, 3, 128), lambda t: (t, 0, 0)),
            pl.BlockSpec((EP, 1, 1, 4, 128, 128), lambda t: (0, t % 2, t // 2, 0, 0, 0)),
        ],
        out_specs=pl.BlockSpec((tok_count, width), lambda t: (0, 0)),
        scratch_shapes=[pltpu.VMEM((tok_count, width), F32)],
        cost_estimate=pl.CostEstimate(flops=5 * 10**9, bytes_accessed=34 * 10**6, transcendentals=0),
        compiler_params=pltpu.CompilerParams(vmem_limit_bytes=24 * 2**20),
        name="mix_tokens",
    )(mix_rows, taps, blocks)
    return (mixer_out, expert_out)


def solution(mesh):
    finer = Mesh(mesh.devices.reshape(mesh.shape["ep"], 8, 2), EP_TP)
    return jax.shard_map(
        per_device,
        mesh=finer,
        in_specs=(
            P(EP_TP, None), P(EP_TP, None), P(), P(None, TP), P(None, TP), P(None, TP),
            P(None, TP), P(TP, None), P(), P("ep", None, TP), P("ep", None, TP),
            P("ep", TP, None), P(EP_TP, None), P(EP_TP, None),
        ),
        out_specs=(P(EP_TP, None), P(EP_TP, None)),
        check_vma=False,
    )
```

time: 402 us -> 379 us (0.943)
  Pallas kernels: 0 us -> 291 us
  waiting for transfers between devices: 261 us -> 38 us
  matrix products: 56 us -> 3.08 us
  local copies, waits for them, and re-layouts: 22.2 us -> 3.76 us
  blocking collectives: 29 us -> 17 us
  other arithmetic: 9.98 us -> 3.18 us
    pallas_call x0 -> x3, Pallas kernels: none -> 291 us  [the longest x1 139 us: per_device(): pl.pallas_call(gather_kernel, out_shape=jax.ShapeDtypeStruct((NZ, 2, LOCA...]
    reduce_scatter x3 -> x0, waiting for transfers between devices: 136 us -> none  [the longest x1 118 us: per_device(): lax.psum_scatter(down_rows(hidden_all, w_down).astype(jnp.bfloat16), TP,...]
    all_gather x2, waiting for transfers between devices: 104 us -> 37.9 us  [the longest x1 37.9 us: per_device(): part = lax.all_gather(part, 'tp_0', axis=0, tiled=False)]
    dot_general x7 -> x2, matrix products: 56 us -> 3.08 us  [the longest x1 2.3 us: per_device(): sums = jnp.dot(both, back.reshape(wide, width), preferred_element_type=F32)]
    all_to_all x1 -> x0, blocking collectives: 29 us -> none  [per_device(): lax.all_to_all(packed, 'ep', split_axis=0, concat_axis=0, tiled=True)]
    all_to_all x1 -> x0, waiting for transfers between devices: 20.1 us -> none  [per_device(): lax.all_to_all(expert_value, 'ep', split_axis=0, concat_axis=0, tiled=True)]
    all_gather x0 -> x1, blocking collectives: none -> 17 us  [per_device(): taps = lax.all_gather(conv_taps, TP, axis=0, tiled=False)]
    transpose x1 -> x0, local copies, waits for them, and re-layouts: 8.54 us -> none  [summed_rows_2(): pieces = pieces.reshape(*sizes, *inside).swapaxes(0, 1).reshape(-1, *inside)]
  transfers between devices with their start and end apart: 7 -> 3, of which waited for: 6 -> 1; matrix products, arithmetic and copies ran while one was open for 21% -> 2% of each run, Pallas kernels for 0% -> 71%
where the time goes in v1:
time: 379 us; the launch traced here: 378 us
  Pallas kernels  291 us (77%)
  waiting for transfers between devices  38 us (10%)
  blocking collectives  17 us (4%)
  between operations  14.3 us (4%)
  starting transfers between devices  8.23 us (2%)
    pallas_call x1, Pallas kernels, per_device(): pl.pallas_call(gather_kernel, out_shape=jax.ShapeDtypeStruct((NZ, 2, LOCA...  139 us
    pallas_call x1, Pallas kernels, per_device(): pl.pallas_call(scatter_kernel, out_shape=jax.ShapeDtypeStruct((LOCAL, EP,...  128 us
    all_gather x1, waiting for transfers between devices, per_device(): part = lax.all_gather(part, 'tp_0', axis=0, tiled=False)  37.9 us
    pallas_call x1, Pallas kernels, per_device(): pl.pallas_call(mixer_kernel, grid=(NZ * 2,), out_shape=jax.ShapeDtypeStru...  22.7 us
    all_gather x1, blocking collectives, per_device(): taps = lax.all_gather(conv_taps, TP, axis=0, tiled=False)  17 us
    ppermute x1, starting transfers between devices, per_device(): lax.ppermute(normed_mix[tok_count - 16:], EP_TP, [(i, i + 1) for i in ran...  8.15 us
  transfers between devices with their start and end apart: 3, of which 1 were waited for; matrix products, arithmetic and copies ran while one was open for 2% of the time, Pallas kernels for 71%

profile of v1, /device:TPU:1, one launch (start us, length us, event | category | flops | bytes accessed | tf_op | source)
XLA Modules:
  0.0 378.1 jit_solution(10759305911305948144)
XLA Ops:
  7.2 0.0 copy-start.3
  7.2 0.0 copy-start.5
  7.2 0.0 copy-start.8
  7.2 0.0 all-gather.7.cloned.1.call-start
  7.2 0.0 copy-start.4
  7.3 0.9 dynamic-slice_bitcast_fusion.2
  8.1 0.8 dynamic-slice_bitcast_fusion
  8.9 0.7 pad_maximum_fusion.1
  9.6 0.0 all-gather.7.cloned.1.call-update
  9.6 0.0 all-gather.9.cloned.1.call-start
  9.6 37.9 %all-gather.7.cloned.1.call-done = bf16[32,128,128]{2,1,0:T(8,128)(2,1)} async-done(((bf16[4,128,128]{2,1,0:T(8,128)(2,1)}), bf16[32,128,128]{2,1,0:T(8,128)(2,1)}) %all-gather.7.cloned.1.call-update) | async-done | bytes 1048592 | tf_op jit(solution)/shard_map/all_gather | solution.py:339
  47.6 0.0 all-gather.9.cloned.1.call-update
  47.6 0.0 copy-done.3
  47.6 0.2 fusion
  47.8 0.0 copy-done.5
  47.8 0.2 fusion.2
  48.0 8.2 %collective-permute-start = (bf16[16,2048]{1,0:T(8,128)(2,1)S(1)}, bf16[16,2048]{1,0:T(8,128)(2,1)S(1)}, u32[]{:S(2)}, u32[]{:S(2)}) collective-permute-start(bf16[16,2048]{1,0:T(8,128)(2,1)S(1)} %slice.38), channel_id=1, source_target_pairs={{0,1},{1,2},{2,3},{3,4},{4,5},{5,6},{6,7},{7,8},{8,9},{9,10},{10,1... | collective-permute-start | bytes 196616 | tf_op jit(solution)/shard_map/ppermute | solution.py:346
  56.2 0.0 copy-done.8
  56.2 0.1 copy.37
  56.3 0.0 copy-start.1
  56.3 0.1 eq.84
  56.5 0.1 eq.88
  56.6 0.1 copy.40
  56.8 0.6 reduce-window.6
  57.4 0.2 slice_reduce_fusion.2
  57.6 0.1 fusion.30
  57.7 0.1 reduce_sum.31
  57.8 0.1 fusion.22
  57.9 0.2 slice_reduce_fusion.1
  58.1 0.0 copy-done.4
  58.1 0.2 fusion.3
  58.3 0.0 copy-done.9
  58.3 0.2 reduce-precision_convert_fusion
  58.5 0.0 copy-done.6
  58.5 0.8 convolution_convert_fusion
  59.3 0.0 copy-done
  59.3 0.0 copy-done.1
  59.3 139.5 %gather_experts.1.hid = bf16[8,2,2,160,128]{4,3,2,1,0:T(8,128)(2,1)S(1)} custom-call(bf16[2,16,16,2048]{3,2,1,0:T(8,128)(2,1)S(1)} %bitcast.37, bf16[2,2048,128]{2,1,0:T(8,128)(2,1)S(1)} %copy-done, bf16[2,2048,128]{2,1,0:T(8,128)(2,1)S(1)} %copy-done.1), custom_call_target="tpu_custom_call" | custom-call | flops 6000000000 | bytes 300000000 | tf_op jit(solution)/shard_map/gather_experts/pallas_call | solution.py:359
  198.8 0.0 copy-start.2
  198.8 1.0 copy-done.2
  199.8 128.4 %scatter_experts.1 = bf16[2,16,16,2048]{3,2,1,0:T(8,128)(2,1)} custom-call(bf16[8,2,2,160,128]{4,3,2,1,0:T(8,128)(2,1)} %copy-done.2, bf16[2,128,2048]{2,1,0:T(8,128)(2,1)} %w_down.1), custom_call_target="tpu_custom_call" | custom-call | flops 6000000000 | bytes 300000000 | tf_op jit(solution)/shard_map/scatter_experts/pallas_call | solution.py:377
  328.2 2.3 fusion.12
  330.5 0.0 copy-start.7
  330.5 0.9 fusion.6
  331.4 17.0 %all-gather.3.taps = f32[16,3,128]{2,1,0:T(4,128)S(1)} all-gather(f32[1,3,128]{2,1,0:T(4,128)S(1)} %bitcast.41), channel_id=2, replica_groups=mesh['ep'=16,'tp_0'=8,'tp_1'=2] {'tp_0','tp_1'}, dimensions={0}, use_global_device_ids=true | all-gather | bytes 26112 | tf_op jit(solution)/shard_map/all_gather | solution.py:342
  348.4 0.0 collective-permute-done
  348.5 0.0 all-gather.9.cloned.1.call-done
  348.5 22.7 %mix_tokens.1 = bf16[128,2048]{1,0:T(8,128)(2,1)} custom-call(bf16[144,2048]{1,0:T(8,128)(2,1)S(1)} %pad_maximum_fusion.tok, f32[16,3,128]{2,1,0:T(4,128)S(1)} %all-gather.3.taps, bf16[16,2,8,4,128,128]{5,4,3,2,1,0:T(8,128)(2,1)} %bitcast.38), custom_call_target="tpu_custom_call" | custom-call | flops 5000000000 | bytes 34000000 | tf_op jit(solution)/shard_map/mix_tokens/pallas_call | solution.py:406
  (13 shorter events, 0.1 us)
Async XLA Ops:
  7.2 40.4 %copy-start.3 = (bf16[128,2048]{1,0:T(8,128)(2,1)S(1)}, bf16[128,2048]{1,0:T(8,128)(2,1)}, u32[]{:S(2)}) copy-start(bf16[128,2048]{1,0:T(8,128)(2,1)} %param.14) | copy-start | bytes 1572868
  7.2 40.6 %copy-start.5 = (f32[2048]{0:T(1024)S(1)}, f32[2048]{0:T(1024)}, u32[]{:S(2)}) copy-start(f32[2048]{0:T(1024)} %param.16) | copy-start | bytes 24580
  7.2 49.0 %copy-start.8 = (s32[128,2]{0,1:T(2,128)S(1)}, s32[128,2]{0,1:T(2,128)}, u32[]{:S(2)}) copy-start(s32[128,2]{0,1:T(2,128)} %param.26) | copy-start | bytes 3076
  7.2 40.4 %all-gather.7.cloned.1.call-start = ((), (), s32[]{:S(2)}) async-start(), calls=%async_computation | async-start | bytes 1179648 | tf_op jit(solution)/shard_map/all_gather | solution.py:339
  7.2 50.9 %copy-start.4 = (bf16[128,2048]{1,0:T(8,128)(2,1)S(1)}, bf16[128,2048]{1,0:T(8,128)(2,1)}, u32[]{:S(2)}) copy-start(bf16[128,2048]{1,0:T(8,128)(2,1)} %param.15) | copy-start | bytes 1572868
  9.6 48.7 %copy-start.9 = (f32[128,2]{0,1:T(2,128)S(1)}, f32[128,2]{0,1:T(2,128)}, u32[]{:S(2)}) copy-start(f32[128,2]{0,1:T(2,128)} %param.27) | copy-start | bytes 3076
  9.6 338.9 %all-gather.9.cloned.1.call-start = ((), (), s32[]{:S(2)}) async-start(), calls=%async_computation.1 | async-start | bytes 34603008 | tf_op jit(solution)/shard_map/all_gather | solution.py:340
  47.6 10.9 %copy-start.6 = (f32[2048]{0:T(1024)S(1)}, f32[2048]{0:T(1024)}, u32[]{:S(2)}) copy-start(f32[2048]{0:T(1024)} %param.22) | copy-start | bytes 24580
  48.0 300.4 %collective-permute-start = (bf16[16,2048]{1,0:T(8,128)(2,1)S(1)}, bf16[16,2048]{1,0:T(8,128)(2,1)S(1)}, u32[]{:S(2)}, u32[]{:S(2)}) collective-permute-start(bf16[16,2048]{1,0:T(8,128)(2,1)S(1)} %slice.38), channel_id=1, source_target_pairs={{0,1},{1,2},{2,3},{3,4},{4,5},{5,6},{6,7},{7,8},{8,9},{9,10},{10,1... | collective-permute-start | bytes 196616 | tf_op jit(solution)/shard_map/ppermute | solution.py:346
  56.3 3.0 copy-start
  56.3 3.0 copy-start.1
  198.8 1.0 copy-start.2
  330.5 0.9 copy-start.7
Sparse Core Ops, SparseCore 0:
  10.4 37.1 all-gather.6
  50.1 137.7 all-gather.8

commit v2 on v1

v2 whole, which is shorter than its diff:
```python
import functools

import jax
import jax.numpy as jnp
from jax import lax
from jax.experimental import pallas as pl
from jax.experimental.pallas import tpu as pltpu
from jax.sharding import Mesh
from jax.sharding import PartitionSpec as P

EXPERTS = 32
CAP = 10
QUADS = 80
EIGHTS = 80
EP = 16
NZ = 8
LOCAL = 2
ROWS = EP * CAP
TP = ("tp_0", "tp_1")
EP_TP = ("ep", "tp_0", "tp_1")
MESH = pl.DeviceIdType.MESH
F32 = jnp.float32
BF16 = jnp.bfloat16

norm_eps = 1e-06
clamp_limit = 7.0
gate_alpha = 1.702


def rms_scale(tok_rows, gain_vec):
    values = tok_rows.astype(F32)
    scaled = values * lax.rsqrt(jnp.mean(values * values, axis=-1, keepdims=True) + norm_eps)
    return (scaled * gain_vec).astype(BF16)


def places():
    return lax.axis_index("ep"), lax.axis_index("tp_0"), lax.axis_index("tp_1")


def signal(where):
    pl.semaphore_signal(
        pltpu.get_barrier_semaphore(), inc=1, device_id=where, device_id_type=MESH
    )


def signal_all(count, where):
    def one(k, _):
        signal(where(k))
        return 0

    lax.fori_loop(1, count, one, 0)


def signal_ring(ep, z, core):
    for step in (1, NZ - 1):
        signal((ep, lax.rem(z + step, NZ), core))
    signal((ep, z, 1 - core))


def remote(src, dst, send, recv, where):
    return pltpu.make_async_remote_copy(
        src_ref=src, dst_ref=dst, send_sem=send, recv_sem=recv, device_id=where, device_id_type=MESH
    )


def each(count, act):
    def one(k, _):
        act(k)
        return 0

    lax.fori_loop(1, count, one, 0)


GATHER_D = (1, 1, 2, 2, 3, 3, 4)
GATHER_X = ((0, 1, 0, 1, 0, 1, 0), (0, 1, 0, 1, 0, 1, 1))
SCATTER_D = (4, 3, 3, 2, 2, 1, 1)
SCATTER_X = ((0, 1, 0, 1, 0, 1, 0), (1, 0, 1, 0, 1, 1, 0))
SCATTER_IN = ((None, None, 0, 1, 2, 3, 4), (None, None, 0, 1, 2, 4, 3))
LAST_IN = {1: (5, 5), 0: (6, 6)}
STEPS = 7


def forwards(way, n):
    nxt = 6 if (way, n) == (1, 5) else n + 2
    if nxt < STEPS and GATHER_X[way][nxt] == GATHER_X[way][n] and GATHER_D[nxt] == GATHER_D[n] + 1:
        return nxt
    return None


def exchange_kernel(
    slots, tail, taps, w_outer, w_inner, w_value, w_mix,
    unit, w_three, w_one, taps_all, halo,
    landed, part,
    w_sem, a_send, a_recv, r_send, r_recv, t_send, t_recv, h_sem,
):
    ep, z, core = places()
    own = pl.ds(pl.multiple_of(ep * 128, 128), 128)
    loads = [
        pltpu.make_async_copy(w.at[own], part.at[i], w_sem.at[i])
        for i, w in enumerate((w_inner, w_value, w_outer))
    ]
    loads.append(pltpu.make_async_copy(w_mix.at[:, own], part.at[3], w_sem.at[3]))
    for load in loads:
        load.start()
    spot = z * 2 + core

    def tp_peer(k):
        to = lax.rem(spot + k, NZ * 2)
        return ep, to // 2, lax.rem(to, 2)

    def in_order(step):
        to = lax.rem(ep * (NZ * 2) + spot + step, EP * NZ * 2)
        return to // (NZ * 2), lax.rem(to // 2, NZ), lax.rem(to, 2)

    def ep_peer(k):
        return lax.rem(ep + k, EP), z, core

    signal_all(EP, ep_peer)
    signal_all(NZ * 2, tp_peer)
    signal(in_order(1))
    signal(in_order(EP * NZ * 2 - 1))
    pl.semaphore_wait(pltpu.get_barrier_semaphore(), EP + NZ * 2)

    def exchange(k):
        where = ep_peer(k)
        return remote(slots.at[where[0]], landed.at[ep], a_send.at[k], a_recv.at[k], where)

    def tell_taps(k):
        return remote(taps, taps_all.at[spot], t_send.at[k], t_recv.at[k], tp_peer(k))

    def tell_tail():
        return remote(tail, halo, h_sem.at[0], h_sem.at[1], in_order(1))

    steps = (NZ - 1, 1)

    def ring_copies(way, n):
        away = GATHER_D[n] - 1
        at = lax.rem(z + away * steps[way], NZ)
        there = (ep, lax.rem(z + (NZ - steps[way]), NZ), core)
        if GATHER_X[way][n] == 0:
            pairs = [(part.at[0:2] if away == 0 else w_three.at[at, 0:2], w_three.at[at, 0:2])]
        else:
            pairs = [
                (part.at[2] if away == 0 else w_three.at[at, 2], w_three.at[at, 2]),
                (part.at[3] if away == 0 else w_one.at[at], w_one.at[at]),
            ]
        return [
            remote(src, dst, r_send.at[way, n, i], r_recv.at[way, n, i], there)
            for i, (src, dst) in enumerate(pairs)
        ]

    for load in loads:
        load.wait()
    for n in range(LOCAL):
        for way in range(2):
            for copy in ring_copies(way, n):
                copy.start()
    each(EP, lambda k: exchange(k).start())
    each(NZ * 2, lambda k: tell_taps(k).start())
    tell_tail().start()
    w_three[z] = part[0:3]
    w_one[z] = part[3]
    taps_all[spot] = taps[...]
    landed[ep] = slots[ep]
    row = lax.broadcasted_iota(jnp.int32, (LOCAL * ROWS, EP * QUADS), 0)
    col = lax.broadcasted_iota(jnp.int32, (LOCAL * ROWS, EP * QUADS), 1)
    x, src, slot = row // ROWS, (row % ROWS) // CAP, row % CAP
    first = src * QUADS + x * CAP + slot
    for n in range(STEPS):
        for way in range(2):
            for copy in ring_copies(way, n):
                copy.wait_recv()
            nxt = forwards(way, n)
            if nxt is not None:
                for copy in ring_copies(way, nxt):
                    copy.start()
    each(EP, lambda k: exchange(k).wait_recv())
    for block in range(4):
        picks = (first + block * (LOCAL * CAP) == col).astype(BF16)
        out = jnp.dot(picks, landed[...].reshape(EP * QUADS, 512), preferred_element_type=F32)
        unit[:, :, block * 512 : (block + 1) * 512] = out.astype(BF16).reshape(LOCAL, ROWS, 512)
    each(NZ * 2, lambda k: tell_taps(k).wait())
    tell_tail().wait()
    each(EP, lambda k: exchange(k).wait_send())
    for way in range(2):
        for n in range(STEPS):
            for copy in ring_copies(way, n):
                copy.wait_send()


def gather_kernel(
    unit, w_gate, w_up, hid,
    units, w_both,
    w_sem, r_send, r_recv, c_send, c_recv,
):
    ep, z, core = places()
    loads = []
    for x in range(LOCAL):
        loads.append(pltpu.make_async_copy(w_gate.at[x], w_both.at[x, :, 0:128], w_sem.at[x, 0]))
        loads.append(pltpu.make_async_copy(w_up.at[x], w_both.at[x, :, 128:256], w_sem.at[x, 1]))
    for load in loads:
        load.start()
    signal_ring(ep, z, core)
    pl.semaphore_wait(pltpu.get_barrier_semaphore(), 3)

    def compute(tok, at_z, at_core, x):
        both = jnp.dot(tok, w_both[x], preferred_element_type=F32)
        gate_pre = jnp.minimum(both[:, 0:128], clamp_limit)
        up_pre = jnp.clip(both[:, 128:256], -clamp_limit, clamp_limit)
        hid[at_z, at_core, x] = (
            (up_pre + 1.0) * gate_pre * jax.nn.sigmoid(gate_alpha * gate_pre)
        ).astype(BF16)

    steps = (NZ - 1, 1)

    def ring_copy(way, n):
        away = GATHER_D[n] - 1
        at = lax.rem(z + away * steps[way], NZ)
        x = GATHER_X[way][n]
        there = lax.rem(z + (NZ - steps[way]), NZ)
        return remote(
            unit.at[x] if away == 0 else units.at[at, core, x], units.at[at, core, x],
            r_send.at[way, n], r_recv.at[way, n], (ep, there, core),
        )

    def across(way, n):
        own = n == STEPS
        at = z if own else lax.rem(z + GATHER_D[n] * steps[way], NZ)
        x = way if own else GATHER_X[way][n]
        ref = units.at[at, core, x]
        copy = remote(
            unit.at[x] if own else ref, ref, c_send.at[way, n], c_recv.at[way, n], (ep, z, 1 - core)
        )
        return copy, at, x

    for n in range(LOCAL):
        for way in range(2):
            ring_copy(way, n).start()
    for way in range(2):
        across(way, STEPS)[0].start()
    for load in loads:
        load.wait()
    for x in range(LOCAL):
        compute(unit[x], z, core, x)

    for n in range(STEPS):
        for way in range(2):
            ring_copy(way, n).wait_recv()
            nxt = forwards(way, n)
            if nxt is not None:
                ring_copy(way, nxt).start()
            across(way, n)[0].start()
        for way in range(2):
            at = lax.rem(z + GATHER_D[n] * steps[way], NZ)
            x = GATHER_X[way][n]
            compute(units[at, core, x], at, core, x)
        for way in range(2):
            copy, at, x = across(way, STEPS if n == 0 else n - 1)
            copy.wait_recv()
            compute(units[at, 1 - core, x], at, 1 - core, x)
    for way in range(2):
        copy, at, x = across(way, STEPS - 1)
        copy.wait_recv()
        compute(units[at, 1 - core, x], at, 1 - core, x)
    for way in range(2):
        for n in range(STEPS):
            ring_copy(way, n).wait_send()
            across(way, n)[0].wait_send()
        across(way, STEPS)[0].wait_send()


def scatter_kernel(
    hid, w_down, tok, taps, w_three,
    back, gated,
    c_out, c_in, r_out, r_in, b_in, b_out, spread, w_slots,
    c_send, c_recv, r_send, r_recv, a_send, a_recv, w_sem,
):
    ep, z, core = places()

    def fetch(t):
        return pltpu.make_async_copy(
            w_three.at[:, lax.rem(t, 2), t // 2], w_slots.at[lax.rem(t, 2)], w_sem.at[lax.rem(t, 2)]
        )

    fetch(0).start()
    fetch(1).start()
    signal_all(EP, lambda k: (lax.rem(ep + k, EP), z, core))
    signal_ring(ep, z, core)
    pl.semaphore_wait(pltpu.get_barrier_semaphore(), EP + 2)

    def mix(t, _):
        fetch(t).wait()
        at = lax.rem(t, 2)
        rows = tok[...]
        pair = jnp.concatenate([w_slots[at, :, i].reshape(2048, 128) for i in range(2)], axis=1)
        pair = jnp.dot(rows, pair, preferred_element_type=F32)
        prod = pair[:, 0:128] * pair[:, 128:256]
        outer = jnp.dot(
            rows[16:144], w_slots[at, :, 2].reshape(2048, 128), preferred_element_type=F32
        )
        tap = taps[t]
        conv = tap[2:3] * prod[16:144] + tap[1:2] * prod[15:143] + tap[0:1] * prod[14:142]
        gated[lax.rem(t, 2), t // 2] = (outer * conv).astype(BF16)

        @pl.when(t + 2 < NZ * 2)
        def _():
            fetch(t + 2).start()

        return 0
    steps = (1, NZ - 1)

    def place(way, m):
        if m == STEPS:
            return z, way
        return lax.rem(z + SCATTER_D[m] * steps[way], NZ), SCATTER_X[way][m]

    def across(way, m):
        return remote(
            c_out.at[way, m], c_in.at[way, m], c_send.at[way, m], c_recv.at[way, m],
            (ep, z, 1 - core),
        )

    def ring_copy(way, m):
        return remote(
            r_out.at[way, m], r_in.at[way, m], r_send.at[way, m], r_recv.at[way, m],
            (ep, lax.rem(z + steps[way], NZ), core),
        )

    def partial(at, at_core, x, add, out):
        def tile(j, _):
            cols = pl.ds(pl.multiple_of(j * 512, 512), 512)
            total = jnp.dot(hid[at, at_core, x], w_down[x, :, cols], preferred_element_type=F32)
            for ref in add:
                total = total + ref[:, cols].astype(F32)
            out[:, cols] = total.astype(BF16)
            return 0

        lax.fori_loop(0, 4, tile, 0)

    def help_other(m):
        for way in range(2):
            at, x = place(way, m)
            partial(at, 1 - core, x, (), c_out.at[way, m])
            across(way, m).start()

    help_other(0)
    help_other(1)
    for m in range(STEPS):
        for way in range(2):
            at, x = place(way, m)
            add = [c_in.at[way, m]]
            across(way, m).wait_recv()
            came = SCATTER_IN[way][m]
            if came is not None:
                ring_copy(way, came).wait_recv()
                add.append(r_in.at[way, came])
            partial(at, core, x, add, r_out.at[way, m])
            ring_copy(way, m).start()
        if m + 2 <= STEPS:
            help_other(m + 2)
        if m == 1:
            row = lax.broadcasted_iota(jnp.int32, spread.shape, 0)
            col = lax.broadcasted_iota(jnp.int32, spread.shape, 1)
            want = ((row % EIGHTS) // CAP) * ROWS + (row // EIGHTS) * CAP + row % CAP
            spread[...] = (want == col).astype(BF16)
        if m > 1:
            lax.fori_loop((m - 2) * 4, min((m - 1) * 4, NZ * 2), mix, 0)

    def exchange(x, k):
        to = lax.rem(ep + k, EP)
        return remote(
            b_out.at[x, to], back.at[x, ep], a_send.at[x, k], a_recv.at[x, k], (to, z, core)
        )

    for x in (1, 0):
        across(x, STEPS).wait_recv()
        for way in range(2):
            ring_copy(way, LAST_IN[x][way]).wait_recv()

        def tile(j, _, x=x):
            cols = pl.ds(pl.multiple_of(j * 256, 256), 256)
            total = jnp.dot(hid[z, core, x], w_down[x, :, cols], preferred_element_type=F32)
            for ref in (c_in.at[x, STEPS], r_in.at[0, LAST_IN[x][0]], r_in.at[1, LAST_IN[x][1]]):
                total = total + ref[:, cols].astype(F32)
            b_in[j] = total.astype(BF16)
            return 0

        lax.fori_loop(0, 8, tile, 0)

        def spread_out(j, _, x=x):
            rows = pl.ds(pl.multiple_of(j * (4 * EIGHTS), 4 * EIGHTS), 4 * EIGHTS)
            wide = jnp.dot(spread[rows, :], b_in[...].reshape(8 * ROWS, 256), preferred_element_type=F32)
            b_out[x, pl.ds(j * 4, 4)] = wide.astype(BF16).reshape(4, EIGHTS, 256)
            return 0

        lax.fori_loop(0, 4, spread_out, 0)

        def send_one(k, _, x=x):
            exchange(x, k).start()
            return 0

        lax.fori_loop(1, EP, send_one, 0)
        back[x, ep] = b_out[x, ep]
    for way in range(2):
        for m in range(STEPS):
            ring_copy(way, m).wait_send()
            across(way, m).wait_send()
        across(way, STEPS).wait_send()
    for x in (1, 0):

        def end_one(k, _, x=x):
            exchange(x, k).wait()
            return 0

        lax.fori_loop(1, EP, end_one, 0)


def last_product_kernel(gated, w_one, out):
    rows = jnp.concatenate([gated[i, j] for i in range(2) for j in range(NZ)], axis=1)
    pair = jnp.concatenate([w_one[i].reshape(2048, 128) for i in range(2)], axis=1)
    out[...] = jnp.dot(rows, pair, preferred_element_type=F32).astype(BF16)


def slot_places(route_ids):
    flat_ids = route_ids.reshape(-1)
    member = (flat_ids[:, None] == jnp.arange(EXPERTS, dtype=jnp.int32)[None, :]).astype(jnp.int32)
    earlier = jnp.cumsum(member, axis=0) - member
    place = jnp.sum(earlier * member, axis=1)
    shape = route_ids.shape
    return (flat_ids // LOCAL).reshape(shape), (flat_ids % LOCAL).reshape(shape), place.reshape(shape)


DMA = pltpu.SemaphoreType.DMA


def per_device(
    mixer_in, expert_in, mixer_gain, w_outer, w_inner, w_value, conv_taps, w_mix_out,
    expert_gain, w_gate, w_up, w_down, route_ids, route_weights,
):
    tok_count, width = expert_in.shape
    normed_mix = rms_scale(mixer_in, mixer_gain)
    normed_exp = rms_scale(expert_in, expert_gain)
    owner, which, place = slot_places(route_ids)

    out_row = owner * QUADS + which * CAP + place
    rows_out = jnp.arange(EP * QUADS, dtype=jnp.int32)[:, None]
    placing = jnp.concatenate(
        [
            (
                (rows_out == out_row[None, :, 0] + q * (LOCAL * CAP))
                | (rows_out == out_row[None, :, 1] + q * (LOCAL * CAP))
            ).astype(BF16)
            for q in range(4)
        ],
        axis=1,
    )
    stacked = jnp.concatenate([normed_exp[:, q * 512 : (q + 1) * 512] for q in range(4)], axis=0)
    slots = jnp.dot(placing, stacked, preferred_element_type=F32).astype(BF16)
    slots = slots.reshape(EP, QUADS, 512)
    taps = jnp.concatenate((conv_taps, jnp.zeros((5, 128), F32)), axis=0)

    vmem = pl.BlockSpec(memory_space=pltpu.VMEM)
    anywhere = pl.BlockSpec(memory_space=pl.ANY)
    unit, w_three, w_one, taps_all, halo = pl.pallas_call(
        exchange_kernel,
        out_shape=(
            jax.ShapeDtypeStruct((LOCAL, ROWS, width), BF16),
            jax.ShapeDtypeStruct((NZ, 3, 128, 128), BF16),
            jax.ShapeDtypeStruct((NZ, 128, 128), BF16),
            jax.ShapeDtypeStruct((NZ * 2, 8, 128), F32),
            jax.ShapeDtypeStruct((16, width), BF16),
        ),
        in_specs=[vmem] * 3 + [anywhere] * 4,
        out_specs=(vmem,) * 5,
        scratch_shapes=[
            pltpu.VMEM((EP, QUADS, 512), BF16),
            pltpu.VMEM((4, 128, 128), BF16),
            DMA((4,)), DMA((EP,)), DMA((EP,)), DMA((2, STEPS, 2)), DMA((2, STEPS, 2)),
            DMA((NZ * 2,)), DMA((NZ * 2,)), DMA((2,)),
        ],
        cost_estimate=pl.CostEstimate(flops=2 * 10**10, bytes_accessed=10**7, transcendentals=0),
        compiler_params=pltpu.CompilerParams(
            collective_id=0, has_side_effects=True, vmem_limit_bytes=24 * 2**20
        ),
        name="exchange",
    )(slots, normed_mix[tok_count - 16 :], taps, w_outer, w_inner, w_value, w_mix_out)

    w_three = lax.all_gather(w_three, ("ep", "tp_1"), axis=0, tiled=False)
    w_one = lax.all_gather(w_one, ("ep", "tp_1"), axis=0, tiled=False)
    w_three = w_three.reshape(EP, 2, NZ, 3, 128, 128)
    w_one = w_one.reshape(EP, 2, NZ, 128, 128)

    hid = pl.pallas_call(
        gather_kernel,
        out_shape=jax.ShapeDtypeStruct((NZ, 2, LOCAL, ROWS, 128), BF16),
        in_specs=[vmem, anywhere, anywhere],
        out_specs=vmem,
        scratch_shapes=[
            pltpu.VMEM((NZ, 2, LOCAL, ROWS, width), BF16),
            pltpu.VMEM((LOCAL, width, 256), BF16),
            DMA((LOCAL, 2)),
            DMA((2, STEPS)), DMA((2, STEPS)), DMA((2, STEPS + 1)), DMA((2, STEPS + 1)),
        ],
        cost_estimate=pl.CostEstimate(flops=10**11, bytes_accessed=3 * 10**8, transcendentals=0),
        compiler_params=pltpu.CompilerParams(
            collective_id=1, has_side_effects=True, vmem_limit_bytes=40 * 2**20
        ),
        name="gather_experts",
    )(unit, w_gate, w_up)

    ep, z, core = places()
    halo = jnp.where((ep == 0) & (z == 0) & (core == 0), jnp.zeros_like(halo), halo)
    mix_rows = jnp.concatenate((halo, normed_mix), axis=0)
    back, gated = pl.pallas_call(
        scatter_kernel,
        out_shape=(
            jax.ShapeDtypeStruct((LOCAL, EP, EIGHTS, 256), BF16),
            jax.ShapeDtypeStruct((2, NZ, tok_count, 128), BF16),
        ),
        in_specs=[vmem] * 4 + [anywhere],
        out_specs=(vmem, vmem),
        scratch_shapes=[
            pltpu.VMEM((2, STEPS + 1, ROWS, width), BF16),
            pltpu.VMEM((2, STEPS + 1, ROWS, width), BF16),
            pltpu.VMEM((2, STEPS, ROWS, width), BF16),
            pltpu.VMEM((2, STEPS, ROWS, width), BF16),
            pltpu.VMEM((8, ROWS, 256), BF16),
            pltpu.VMEM((LOCAL, EP, EIGHTS, 256), BF16),
            pltpu.VMEM((EP * EIGHTS, 8 * ROWS), BF16),
            pltpu.VMEM((2, EP, 3, 128, 128), BF16),
            DMA((2, STEPS + 1)), DMA((2, STEPS + 1)), DMA((2, STEPS)), DMA((2, STEPS)),
            DMA((LOCAL, EP)), DMA((LOCAL, EP)), DMA((2,)),
        ],
        cost_estimate=pl.CostEstimate(flops=10**11, bytes_accessed=3 * 10**8, transcendentals=0),
        compiler_params=pltpu.CompilerParams(
            collective_id=2, has_side_effects=True, vmem_limit_bytes=58 * 2**20
        ),
        name="scatter_experts",
    )(hid, w_down, mix_rows, taps_all, w_three)

    back_row = which * (EP * EIGHTS) + owner * EIGHTS + place
    rows_back = jnp.arange(LOCAL * EP * EIGHTS, dtype=jnp.int32)[None, :]
    back = back.reshape(LOCAL * EP * EIGHTS, 256)
    blocks = []
    for q in range(8):
        weights = sum(
            jnp.where(
                rows_back == back_row[:, k : k + 1] + q * CAP, route_weights[:, k : k + 1], 0.0
            )
            for k in range(2)
        )
        high = lax.reduce_precision(weights, 8, 7)
        low = lax.reduce_precision(weights - high, 8, 7)
        both = jnp.concatenate((high, low), axis=0).astype(BF16)
        sums = jnp.dot(both, back, preferred_element_type=F32)
        blocks.append((sums[:tok_count] + sums[tok_count:]).astype(BF16))
    expert_out = jnp.concatenate(blocks, axis=1)

    mixer_out = pl.pallas_call(
        last_product_kernel,
        grid=(EP // 2,),
        out_shape=jax.ShapeDtypeStruct((tok_count, width), BF16),
        in_specs=[
            pl.BlockSpec((2, NZ, tok_count, 128), lambda e: (0, 0, 0, 0)),
            pl.BlockSpec((2, 2, NZ, 128, 128), lambda e: (e, 0, 0, 0, 0)),
        ],
        out_specs=pl.BlockSpec((tok_count, 256), lambda e: (0, e)),
        cost_estimate=pl.CostEstimate(flops=10**9, bytes_accessed=9 * 10**6, transcendentals=0),
        compiler_params=pltpu.CompilerParams(vmem_limit_bytes=16 * 2**20),
        name="last_product",
    )(gated, w_one)
    return (mixer_out, expert_out)


def solution(mesh):
    finer = Mesh(mesh.devices.reshape(mesh.shape["ep"], 8, 2), EP_TP)
    return jax.shard_map(
        per_device,
        mesh=finer,
        in_specs=(
            P(EP_TP, None), P(EP_TP, None), P(), P(None, TP), P(None, TP), P(None, TP),
            P(None, TP), P(TP, None), P(), P("ep", None, TP), P("ep", None, TP),
            P("ep", TP, None), P(EP_TP, None), P(EP_TP, None),
        ),
        out_specs=(P(EP_TP, None), P(EP_TP, None)),
        check_vma=False,
    )
```

time: 379 us -> 318 us (0.84)
  waiting for transfers between devices: 38 us -> 0.55 us
  Pallas kernels: 291 us -> 270 us
  blocking collectives: 17 us -> 0 us
  other arithmetic: 3.18 us -> 12.7 us
  local copies, waits for them, and re-layouts: 3.76 us -> 12.1 us
  starting transfers between devices: 8.23 us -> 0.26 us
  matrix products: 3.08 us -> 7.5 us
    all_gather x2, waiting for transfers between devices: 37.9 us -> 0.01 us  [the longest x1 0.01 us: per_device(): w_three = lax.all_gather(w_three, ('ep', 'tp_1'), axis=0, tiled=False)]
    pallas_call x1, Pallas kernels: 139 us -> 107 us  [per_device(): pl.pallas_call(gather_kernel, out_shape=jax.ShapeDtypeStruct((NZ, 2, LOCA...]
    all_gather x1 -> x0, blocking collectives: 17 us -> none  [per_device(): taps = lax.all_gather(conv_taps, TP, axis=0, tiled=False)]
    pallas_call x2 -> x3, Pallas kernels: 151 us -> 163 us  [the longest x1 125 us: per_device(): pl.pallas_call(scatter_kernel, out_shape=(jax.ShapeDtypeStruct((LOCAL, EP...]
    unnamed x21 -> x62, local copies, waits for them, and re-layouts: 1.19 us -> 11.3 us
    ppermute x1 -> x0, starting transfers between devices: 8.15 us -> none  [per_device(): lax.ppermute(normed_mix[tok_count - 16:], EP_TP, [(i, i + 1) for i in ran...]
    another operation x4 -> x3, other arithmetic: 1.46 us -> 7.87 us
    dot_general x2 -> x9, matrix products: 3.08 us -> 7.5 us  [the longest x8 6.64 us: per_device(): sums = jnp.dot(both, back, preferred_element_type=F32)]
  transfers between devices with their start and end apart: 3 -> 2, of which waited for: 1 -> 0; matrix products, arithmetic and copies ran while one was open for 2% -> 5% of each run, Pallas kernels for 71% -> 73%
where the time goes in v2:
time: 318 us; the launch traced here: 317 us
  Pallas kernels  270 us (85%)
  between operations  14.5 us (5%)
  other arithmetic  12.7 us (4%)
  local copies, waits for them, and re-layouts  12.1 us (4%)
  matrix products  7.5 us (2%)
    pallas_call x1, Pallas kernels, per_device(): pl.pallas_call(scatter_kernel, out_shape=(jax.ShapeDtypeStruct((LOCAL, EP...  125 us
    pallas_call x1, Pallas kernels, per_device(): pl.pallas_call(gather_kernel, out_shape=jax.ShapeDtypeStruct((NZ, 2, LOCA...  107 us
    pallas_call x1, Pallas kernels, per_device(): pl.pallas_call(exchange_kernel, out_shape=(jax.ShapeDtypeStruct((LOCAL, R...  34.3 us
    unnamed x62, local copies, waits for them, and re-layouts  11.3 us
    another operation x3, other arithmetic  7.87 us
    dot_general x8, matrix products, per_device(): sums = jnp.dot(both, back, preferred_element_type=F32)  6.64 us
  transfers between devices with their start and end apart: 2, of which 0 were waited for; matrix products, arithmetic and copies ran while one was open for 5% of the time, Pallas kernels for 73%

profile of v2, /device:TPU:1, one launch (start us, length us, event | category | flops | bytes accessed | tf_op | source)
XLA Modules:
  0.0 317.1 jit_solution(8940962906236116407)
XLA Ops:
  7.2 0.8 copy.39
  8.2 0.1 eq.389
  8.3 0.7 broadcast_compare_fusion
  9.0 0.6 reduce-window.6
  9.6 0.2 slice_reduce_fusion.4
  10.0 0.1 reshape.102
  10.1 0.1 copy.44
  10.3 0.5 slice_reduce_fusion.1
  11.0 0.2 fusion.55
  11.2 0.2 fusion.57
  11.5 0.6 copy-done.12
  12.0 0.2 fusion.58
  12.2 0.2 fusion.60
  12.9 0.3 copy-done.10
  13.2 0.9 convolution_convert_fusion
  14.1 0.2 copy-done.4
  14.3 0.2 copy-done.5
  14.4 0.2 copy-done.6
  14.6 0.2 copy-done.7
  14.8 34.3 %exchange.1 = (bf16[2,160,2048]{2,1,0:T(8,128)(2,1)S(1)}, bf16[8,3,128,128]{3,2,1,0:T(8,128)(2,1)}, bf16[8,128,128]{2,1,0:T(8,128)(2,1)}, f32[16,8,128]{2,1,0:T(8,128)S(1)}, bf16[16,2048]{1,0:T(8,128)(2,1)S(1)}) custom-call(bf16[16,80,512]{2,1,0:T(8,128)(2,1)S(1)} %bitcast.36, bf16[16,2048]{1,0:T(8,128)(2,1)S(1)} %slice.157.tail, ...), custom_call_target="tpu_custom_call" | custom-call | flops 20000000000 | bytes 10000000 | tf_op jit(solution)/shard_map/exchange/pallas_call | solution.py:464
  49.1 0.6 copy-done.8
  49.7 0.2 all-gather.7.cloned.1.call-start
  50.0 0.5 all-gather.7.cloned.1.call-update
  50.5 106.7 %gather_experts.1.hid = bf16[8,2,2,160,128]{4,3,2,1,0:T(8,128)(2,1)S(1)} custom-call(bf16[2,160,2048]{2,1,0:T(8,128)(2,1)S(1)} %get-tuple-element.9.unit, bf16[2,2048,128]{2,1,0:T(8,128)(2,1)S(1)} %copy-done.2, bf16[2,2048,128]{2,1,0:T(8,128)(2,1)S(1)} %copy-done.3), custom_call_target="tpu_custom_call" | custom-call | flops 99999997952 | bytes 300000000 | tf_op jit(solution)/shard_map/gather_experts/pallas_call | solution.py:493
  157.2 1.1 copy-done.9
  158.3 1.9 pad_maximum_fusion.tok
  160.2 7.2 %reduce-precision_convert_fusion = (bf16[128,2560]{1,0:T(8,128)(2,1)S(1)}, bf16[128,2560]{1,0:T(8,128)(2,1)S(1)}, bf16[128,2560]{1,0:T(8,128)(2,1)}, bf16[128,25...) fusion(s32[128]{0:T(128)S(1)} %get-tuple-element.88, ...), kind=kLoop, calls=%fused_computation.9 | loop fusion | flops 26214400 | bytes 10494976 | tf_op jit(solution)/shard_map/convert.1
  167.5 124.5 %scatter_experts.1 = (bf16[2,16,80,256]{3,2,1,0:T(8,128)(2,1)}, bf16[2,8,128,128]{3,2,1,0:T(8,128)(2,1)}) custom-call(bf16[8,2,2,160,128]{4,3,2,1,0:T(8,128)(2,1)} %copy-done.9, bf16[2,128,2048]{2,1,0:T(8,128)(2,1)} %w_down.1, bf16[144,2048]{1,0:T(8,128)(2,1)} %pad_maximum_fusion.tok, f32[16,8,128]{2,1,0:T(8,128)} %copy-done.8, ...), custom_call_target="tpu_custom_call" | custom-call | flops 99999997952 | bytes 300000000 | tf_op jit(solution)/shard_map/scatter_experts/pallas_call | solution.py:514
  292.1 2.1 fusion.23
  294.2 0.7 fusion.27
  294.9 0.4 copy-done.20
  295.3 0.2 copy-done.21
  295.5 0.7 fusion.31
  296.2 0.4 copy-done.18
  296.6 0.2 copy-done.19
  296.8 0.7 fusion.35
  297.5 0.4 copy-done.16
  297.9 0.2 copy-done.17
  298.1 0.7 fusion.39
  298.8 0.4 copy-done.14
  299.2 0.2 copy-done.15
  299.4 0.7 fusion.43
  300.1 0.4 copy-done.13
  300.5 0.6 fusion.47
  301.1 0.6 fusion.51
  301.8 1.0 copy.49
  302.8 3.4 %copy-done = bf16[256,128,128]{2,1,0:T(8,128)(2,1)S(1)} copy-done((bf16[256,128,128]{2,1,0:T(8,128)(2,1)S(1)}, bf16[256,128,128]{2,1,0:T(8,128)(2,1)}, u32[]{:S(2)}) %copy-start) | copy-done | bytes 8388632
  306.2 4.1 %last_product.1 = bf16[128,2048]{1,0:T(8,128)(2,1)} custom-call(bf16[2,8,128,128]{3,2,1,0:T(8,128)(2,1)S(1)} %copy-done.1, bf16[16,2,8,128,128]{4,3,2,1,0:T(8,128)(2,1)S(1)} %bitcast.35), custom_call_target="tpu_custom_call" | custom-call | flops 1000000000 | bytes 9000000 | tf_op jit(solution)/shard_map/last_product/pallas_call | solution.py:559
  (73 shorter events, 1.3 us)
Async XLA Ops:
  7.2 3.8 %copy-start.11 = (bf16[128,2048]{1,0:T(8,128)(2,1)S(1)}, bf16[128,2048]{1,0:T(8,128)(2,1)}, u32[]{:S(2)}) copy-start(bf16[128,2048]{1,0:T(8,128)(2,1)} %param.15) | copy-start | bytes 1572868
  7.2 4.0 %copy-start.25 = (f32[2048]{0:T(1024)S(1)}, f32[2048]{0:T(1024)}, u32[]{:S(2)}) copy-start(f32[2048]{0:T(1024)} %param.22) | copy-start | bytes 24580
  7.2 160.3 %all-gather.5.cloned.1.call-start = ((), (), s32[]{:S(2)}) async-start(), calls=%async_computation | async-start | bytes 25952256 | tf_op jit(solution)/shard_map/all_gather | solution.py:488
  11.0 1.0 copy-start.12
  11.2 1.0 copy-start.26
  12.0 0.9 copy-start.27
  12.4 0.8 copy-start.10
  13.2 1.0 copy-start.4
  13.2 1.2 copy-start.5
  13.2 1.4 copy-start.6
  13.2 1.5 copy-start.7
  14.8 35.7 %copy-start.2 = (bf16[2,2048,128]{2,1,0:T(8,128)(2,1)S(1)}, bf16[2,2048,128]{2,1,0:T(8,128)(2,1)}, u32[]{:S(2)}) copy-start(bf16[2,2048,128]{2,1,0:T(8,128)(2,1)} %w_gate.1) | copy-start | bytes 3145732
  14.8 35.8 %copy-start.3 = (bf16[2,2048,128]{2,1,0:T(8,128)(2,1)S(1)}, bf16[2,2048,128]{2,1,0:T(8,128)(2,1)}, u32[]{:S(2)}) copy-start(bf16[2,2048,128]{2,1,0:T(8,128)(2,1)} %w_up.1) | copy-start | bytes 3145732
  49.1 0.6 copy-start.8
  49.7 253.1 %all-gather.7.cloned.1.call-start = ((), (), s32[]{:S(2)}) async-start(), calls=%async_computation.1 | async-start | bytes 8650752 | tf_op jit(solution)/shard_map/all_gather | solution.py:489
  50.5 107.8 %copy-start.28 = (f32[128,2]{0,1:T(2,128)S(1)}, f32[128,2]{0,1:T(2,128)}, u32[]{:S(2)}) copy-start(f32[128,2]{0,1:T(2,128)} %param.27) | copy-start | bytes 3076
  157.2 1.1 copy-start.9
  167.5 124.5 %copy-start.24 = (bf16[128,2560]{1,0:T(8,128)(2,1)S(1)}, bf16[128,2560]{1,0:T(8,128)(2,1)}, u32[]{:S(2)}) copy-start(bf16[128,2560]{1,0:T(8,128)(2,1)} %get-tuple-element.77) | copy-start | bytes 1966084
  292.0 2.2 copy-start.22
  292.1 2.2 copy-start.23
  292.1 2.2 copy-start.29
  294.2 1.1 copy-start.20
  294.2 1.3 copy-start.21
  295.5 1.1 copy-start.18
  295.5 1.3 copy-start.19
  296.8 1.1 copy-start.16
  296.8 1.3 copy-start.17
  298.1 1.1 copy-start.14
  298.1 1.3 copy-start.15
  299.4 1.1 copy-start.13
  301.8 1.1 copy-start.1
  302.8 3.4 %copy-start = (bf16[256,128,128]{2,1,0:T(8,128)(2,1)S(1)}, bf16[256,128,128]{2,1,0:T(8,128)(2,1)}, u32[]{:S(2)}) copy-start(bf16[256,128,128]{2,1,0:T(8,128)(2,1)} %all-gather.7.cloned.1.call-done) | copy-start | bytes 25165828
Sparse Core Ops, SparseCore 0:
  49.9 94.1 all-gather.4
  146.6 56.1 all-gather.6

commit v3 on v2

v3 whole, which is shorter than its diff:
```python
import functools

import jax
import jax.numpy as jnp
from jax import lax
from jax.experimental import pallas as pl
from jax.experimental.pallas import tpu as pltpu
from jax.sharding import Mesh
from jax.sharding import PartitionSpec as P

EXPERTS = 32
CAP = 10
QUADS = 80
EIGHTS = 80
EP = 16
NZ = 8
LOCAL = 2
ROWS = EP * CAP
TP = ("tp_0", "tp_1")
EP_TP = ("ep", "tp_0", "tp_1")
MESH = pl.DeviceIdType.MESH
F32 = jnp.float32
BF16 = jnp.bfloat16

norm_eps = 1e-06
clamp_limit = 7.0
gate_alpha = 1.702


def normed(values, gain):
    scaled = values * lax.rsqrt(jnp.mean(values * values, axis=-1, keepdims=True) + norm_eps)
    return (scaled * gain).astype(BF16)


def places():
    return lax.axis_index("ep"), lax.axis_index("tp_0"), lax.axis_index("tp_1")


def signal(where):
    pl.semaphore_signal(
        pltpu.get_barrier_semaphore(), inc=1, device_id=where, device_id_type=MESH
    )


def signal_all(count, where):
    def one(k, _):
        signal(where(k))
        return 0

    lax.fori_loop(1, count, one, 0)


def signal_ring(ep, z, core):
    for step in (1, NZ - 1):
        signal((ep, lax.rem(z + step, NZ), core))
    signal((ep, z, 1 - core))


def remote(src, dst, send, recv, where):
    return pltpu.make_async_remote_copy(
        src_ref=src, dst_ref=dst, send_sem=send, recv_sem=recv, device_id=where, device_id_type=MESH
    )


def each(count, act):
    def one(k, _):
        act(k)
        return 0

    lax.fori_loop(1, count, one, 0)


GATHER_D = (1, 1, 2, 2, 3, 3, 4)
GATHER_X = ((0, 1, 0, 1, 0, 1, 0), (0, 1, 0, 1, 0, 1, 1))
SCATTER_D = (4, 3, 3, 2, 2, 1, 1)
SCATTER_X = ((0, 1, 0, 1, 0, 1, 0), (1, 0, 1, 0, 1, 1, 0))
SCATTER_IN = ((None, None, 0, 1, 2, 3, 4), (None, None, 0, 1, 2, 4, 3))
LAST_IN = {1: (5, 5), 0: (6, 6)}
STEPS = 7


def forwards(way, n):
    nxt = 6 if (way, n) == (1, 5) else n + 2
    if nxt < STEPS and GATHER_X[way][nxt] == GATHER_X[way][n] and GATHER_D[nxt] == GATHER_D[n] + 1:
        return nxt
    return None


LINE = (0, 3, 1, 2)
KINDS = 10


def gather_kernel(
    mixer_in, expert_in, mixer_gain, expert_gain, ids, taps, w_outer, w_inner, w_value, w_mix, w_gate, w_up,
    hid, mix_rows, taps_all, wall,
    stacked, slots, landed, part, wz, tail, halo, unit, units, w_both,
    w_sem, g_sem, a_send, a_recv, z_send, z_recv, t_send, t_recv, h_sem,
    r_send, r_recv, c_send, c_recv, x_send, x_recv, d_send, d_recv, o_sem,
):
    ep, z, core = places()
    own = pl.ds(pl.multiple_of(ep * 128, 128), 128)
    loads = [
        pltpu.make_async_copy(w.at[own], part.at[i], w_sem.at[i])
        for i, w in enumerate((w_inner, w_value, w_outer))
    ]
    loads.append(pltpu.make_async_copy(w_mix.at[:, own], part.at[3], w_sem.at[3]))
    for load in loads:
        load.start()
    gate_loads = []
    for x in range(LOCAL):
        gate_loads.append(pltpu.make_async_copy(w_gate.at[x], w_both.at[x, :, 0:128], g_sem.at[x, 0]))
        gate_loads.append(pltpu.make_async_copy(w_up.at[x], w_both.at[x, :, 128:256], g_sem.at[x, 1]))
    for load in gate_loads:
        load.start()
    spot = z * 2 + core
    partner = (ep, z, 1 - core)

    def tp_peer(k):
        to = lax.rem(spot + k, NZ * 2)
        return ep, to // 2, lax.rem(to, 2)

    def in_order(step):
        to = lax.rem(ep * (NZ * 2) + spot + step, EP * NZ * 2)
        return to // (NZ * 2), lax.rem(to // 2, NZ), lax.rem(to, 2)

    def ep_peer(k):
        return lax.rem(ep + k, EP), z, core

    signal_all(EP, ep_peer)
    signal_all(NZ * 2, tp_peer)
    signal(in_order(1))
    signal(in_order(EP * NZ * 2 - 1))

    def exchange(k):
        where = ep_peer(k)
        return remote(slots.at[where[0]], landed.at[ep], a_send.at[k], a_recv.at[k], where)

    def tell_taps(k):
        return remote(taps, taps_all.at[spot], t_send.at[k], t_recv.at[k], tp_peer(k))

    def tell_tail():
        return remote(tail, halo, h_sem.at[0], h_sem.at[1], in_order(1))

    steps = (NZ - 1, 1)

    def spread_z(way, n):
        away = GATHER_D[n] - 1
        at = lax.rem(z + away * steps[way], NZ)
        there = (ep, lax.rem(z + (NZ - steps[way]), NZ), core)
        two = pl.ds(2 * GATHER_X[way][n], 2)
        return remote(
            part.at[two] if away == 0 else wz.at[at, two], wz.at[at, two],
            z_send.at[way, n], z_recv.at[way, n], there,
        )

    def ring_copy(way, n):
        away = GATHER_D[n] - 1
        at = lax.rem(z + away * steps[way], NZ)
        x = GATHER_X[way][n]
        there = lax.rem(z + (NZ - steps[way]), NZ)
        return remote(
            unit.at[x] if away == 0 else units.at[at, core, x], units.at[at, core, x],
            r_send.at[way, n], r_recv.at[way, n], (ep, there, core),
        )

    def across(way, n):
        mine = n == STEPS
        at = z if mine else lax.rem(z + GATHER_D[n] * steps[way], NZ)
        x = way if mine else GATHER_X[way][n]
        ref = units.at[at, core, x]
        copy = remote(unit.at[x] if mine else ref, ref, c_send.at[way, n], c_recv.at[way, n], partner)
        return copy, at, x

    at_x, at_y = lax.rem(ep, 4), ep // 4

    def off(half, du, dv):
        dx, dy = (du, dv) if half == 0 else (dv, du)
        return lax.rem(at_y + dy, 4) * 4 + lax.rem(at_x + dx, 4)

    def piece(half, way, kind, e, at_core):
        whole = kind == 0 or 2 <= kind < 6
        zs = pl.ds(4 * half, 4) if whole else pl.ds(4 * half + 2 * way, 2)
        return wall.at[e, at_core, zs]

    def plane(half, way, kind):
        step = 1 if way == 0 else 3
        if kind == 0:
            e, to = ep, off(half, step, 0)
        elif kind == 1:
            e, to = off(half, 4 - step, 0), off(half, step, 0)
        elif kind < 6:
            e, to = off(half, LINE[kind - 2], 0), off(half, 0, step)
        else:
            e, to = off(half, LINE[kind - 6], 4 - step), off(half, 0, step)
        ref = piece(half, way, kind, e, core)
        return remote(
            wz.at[pl.ds(4 * half, 4)] if kind in (0, 2) else ref, ref,
            x_send.at[half, way, kind], x_recv.at[half, way, kind], (to, z, core),
        )

    def plane_over(half, way, kind):
        step = 1 if way == 0 else 3
        if kind == 0:
            e = off(half, 4 - step, 0)
        elif kind == 1:
            e = off(half, 2, 0)
        elif kind < 6:
            e = off(half, LINE[kind - 2], 4 - step)
        else:
            e = off(half, LINE[kind - 6], 2)
        ref = piece(half, way, kind, e, core)
        return remote(ref, ref, d_send.at[half, way, kind], d_recv.at[half, way, kind], partner)

    both_halves = [(half, way) for half in range(2) for way in range(2)]

    def take(*kinds):
        for kind in kinds:
            for half, way in both_halves:
                plane(half, way, kind).wait_recv()
                plane_over(half, way, kind).start()

    def give(*kinds):
        for kind in kinds:
            for half, way in both_halves:
                plane(half, way, kind).start()

    def own_over():
        ref = wall.at[ep, core]
        return remote(wz, ref, o_sem.at[0], o_sem.at[1], partner)

    def own_keep():
        return pltpu.make_async_copy(wz, wall.at[ep, core], o_sem.at[2])

    def compute(tok, at_z, at_core, x):
        both = jnp.dot(tok, w_both[x], preferred_element_type=F32)
        gate_pre = jnp.minimum(both[:, 0:128], clamp_limit)
        up_pre = jnp.clip(both[:, 128:256], -clamp_limit, clamp_limit)
        hid[at_z, at_core, x] = (
            (up_pre + 1.0) * gate_pre * jax.nn.sigmoid(gate_alpha * gate_pre)
        ).astype(BF16)

    def pass_z(n):
        for way in range(2):
            spread_z(way, n).wait_recv()
            nxt = forwards(way, n)
            if nxt is not None:
                spread_z(way, nxt).start()

    pl.semaphore_wait(pltpu.get_barrier_semaphore(), EP + NZ * 2)
    for load in loads:
        load.wait()
    for n in range(LOCAL):
        for way in range(2):
            spread_z(way, n).start()
    each(NZ * 2, lambda k: tell_taps(k).start())
    rows = normed(expert_in[...].astype(F32), expert_gain[...])
    for q in range(4):
        stacked[q * 128 : (q + 1) * 128] = rows[:, q * 512 : (q + 1) * 512]

    experts = lax.broadcasted_iota(jnp.int32, (EXPERTS, 128), 0)
    hits = [experts == ids[k : k + 1, :] for k in range(2)]
    member = (hits[0] | hits[1]).astype(BF16)
    before = lax.broadcasted_iota(jnp.int32, (128, 128), 0) < lax.broadcasted_iota(jnp.int32, (128, 128), 1)
    earlier = jnp.dot(member, before.astype(BF16), preferred_element_type=F32)
    goes = []
    for k in range(2):
        place = jnp.sum(jnp.where(hits[k], earlier, 0.0), axis=0, keepdims=True).astype(jnp.int32)
        one = ids[k : k + 1, :]
        goes.append((one >> 1) * QUADS + (one & 1) * CAP + place)

    def fill(j, _):
        row = lax.broadcasted_iota(jnp.int32, (4 * QUADS, 128), 0) + j * (4 * QUADS)
        placing = jnp.concatenate(
            [
                ((row == goes[0] + q * (LOCAL * CAP)) | (row == goes[1] + q * (LOCAL * CAP))).astype(F32)
                for q in range(4)
            ],
            axis=1,
        ).astype(BF16)
        out = jnp.dot(placing, stacked[...], preferred_element_type=F32)
        slots[pl.ds(j * 4, 4)] = out.astype(BF16).reshape(4, QUADS, 512)
        return 0

    lax.fori_loop(0, 4, fill, 0)
    each(EP, lambda k: exchange(k).start())
    landed[ep] = slots[ep]
    pass_z(0)
    rows = normed(mixer_in[...].astype(F32), mixer_gain[...])
    mix_rows[16:144] = rows
    tail[...] = rows[112:128]
    tell_tail().start()
    wz[z] = part[...]
    taps_all[spot] = taps[...]
    for n in range(1, STEPS):
        pass_z(n)
    give(0)
    give(2)
    own_over().start()
    own_keep().start()
    row = lax.broadcasted_iota(jnp.int32, (LOCAL * ROWS, EP * QUADS), 0)
    col = lax.broadcasted_iota(jnp.int32, (LOCAL * ROWS, EP * QUADS), 1)
    x, src, slot = row // ROWS, (row % ROWS) // CAP, row % CAP
    first = src * QUADS + x * CAP + slot
    each(EP, lambda k: exchange(k).wait_recv())
    for block in range(4):
        picks = (first + block * (LOCAL * CAP) == col).astype(BF16)
        out = jnp.dot(picks, landed[...].reshape(EP * QUADS, 512), preferred_element_type=F32)
        unit[:, :, block * 512 : (block + 1) * 512] = out.astype(BF16).reshape(LOCAL, ROWS, 512)
    for n in range(LOCAL):
        for way in range(2):
            ring_copy(way, n).start()
    for way in range(2):
        across(way, STEPS)[0].start()
    tell_tail().wait()
    lone = (ep == 0) & (spot == 0)
    mix_rows[0:16] = jnp.where(lone, jnp.zeros_like(halo), halo[...])
    each(NZ * 2, lambda k: tell_taps(k).wait())
    for load in gate_loads:
        load.wait()
    for x in range(LOCAL):
        compute(unit[x], z, core, x)

    for n in range(STEPS):
        for way in range(2):
            ring_copy(way, n).wait_recv()
            nxt = forwards(way, n)
            if nxt is not None:
                ring_copy(way, nxt).start()
            across(way, n)[0].start()
        if n == 0:
            take(0)
            give(1, 3, 4)
        elif n == 1:
            take(2)
            give(6)
        elif n == 2:
            take(1)
            give(5)
        elif n == 3:
            take(3, 4)
            give(7, 8)
        elif n == 4:
            take(6)
        elif n == 5:
            take(5)
            give(9)
            take(7, 8)
        for way in range(2):
            at = lax.rem(z + GATHER_D[n] * steps[way], NZ)
            x = GATHER_X[way][n]
            compute(units[at, core, x], at, core, x)
        for way in range(2):
            copy, at, x = across(way, STEPS if n == 0 else n - 1)
            copy.wait_recv()
            compute(units[at, 1 - core, x], at, 1 - core, x)
    for way in range(2):
        copy, at, x = across(way, STEPS - 1)
        copy.wait_recv()
        compute(units[at, 1 - core, x], at, 1 - core, x)
    take(9)
    own_keep().wait()
    own_over().wait()
    for half, way in both_halves:
        for kind in range(KINDS):
            plane(half, way, kind).wait_send()
            plane_over(half, way, kind).wait()
    each(EP, lambda k: exchange(k).wait_send())
    for way in range(2):
        for n in range(STEPS):
            spread_z(way, n).wait_send()
            ring_copy(way, n).wait_send()
            across(way, n)[0].wait_send()
        across(way, STEPS)[0].wait_send()


def scatter_kernel(
    hid, w_down, tok, taps, ids, weights, wall,
    mixer_out, expert_out,
    c_out, c_in, r_out, r_in, b_in, b_out, back, spread, gather, shares, sums, gated, w_slots, l_slots,
    c_send, c_recv, r_send, r_recv, a_send, a_recv, w_sem, l_sem,
):
    ep, z, core = places()

    def fetch(t):
        return pltpu.make_async_copy(
            wall.at[:, lax.rem(t, 2), t // 2, 0:3], w_slots.at[lax.rem(t, 2)], w_sem.at[lax.rem(t, 2)]
        )

    def fetch_last(j):
        return pltpu.make_async_copy(
            wall.at[pl.ds(2 * j, 2), :, :, 3], l_slots.at[lax.rem(j, 2)], l_sem.at[lax.rem(j, 2)]
        )

    for t in range(2):
        fetch(t).start()
        fetch_last(t).start()
    signal_all(EP, lambda k: (lax.rem(ep + k, EP), z, core))
    signal_ring(ep, z, core)
    pl.semaphore_wait(pltpu.get_barrier_semaphore(), EP + 2)

    def mix(t, _):
        fetch(t).wait()
        at = lax.rem(t, 2)
        rows = tok[...]
        pair = jnp.concatenate([w_slots[at, :, i].reshape(2048, 128) for i in range(2)], axis=1)
        pair = jnp.dot(rows, pair, preferred_element_type=F32)
        prod = pair[:, 0:128] * pair[:, 128:256]
        outer = jnp.dot(
            rows[16:144], w_slots[at, :, 2].reshape(2048, 128), preferred_element_type=F32
        )
        tap = taps[t]
        conv = tap[2:3] * prod[16:144] + tap[1:2] * prod[15:143] + tap[0:1] * prod[14:142]
        gated[t] = (outer * conv).astype(BF16)

        @pl.when(t + 2 < NZ * 2)
        def _():
            fetch(t + 2).start()

        return 0

    def last(j, _):
        fetch_last(j).wait()
        at = lax.rem(j, 2)
        rows = jnp.concatenate([gated[i * 2 + c] for c in range(2) for i in range(NZ)], axis=1)
        pair = jnp.concatenate([l_slots[at, i].reshape(2048, 128) for i in range(2)], axis=1)
        cols = pl.ds(pl.multiple_of(j * 256, 256), 256)
        mixer_out[:, cols] = jnp.dot(rows, pair, preferred_element_type=F32).astype(BF16)

        @pl.when(j + 2 < EP // 2)
        def _():
            fetch_last(j + 2).start()

        return 0

    def tables():
        def fill(j, _):
            rows = pl.ds(pl.multiple_of(j * 320, 320), 320)
            row = lax.broadcasted_iota(jnp.int32, (320, spread.shape[1]), 0) + j * 320
            col = lax.broadcasted_iota(jnp.int32, (320, spread.shape[1]), 1)
            slot = lax.rem(row, CAP)
            to = lax.rem(row, EIGHTS) // CAP * ROWS + row // EIGHTS * CAP + slot
            spread[rows] = (to == col).astype(BF16)
            to = lax.rem(row, ROWS) // CAP * EIGHTS + row // ROWS * CAP + slot
            gather[rows] = (to == col).astype(BF16)
            return 0

        lax.fori_loop(0, 4, fill, 0)

    def split_weights():
        experts = lax.broadcasted_iota(jnp.int32, (128, EXPERTS), 1)
        hits = [experts == ids[:, k : k + 1] for k in range(2)]
        member = (hits[0] | hits[1]).astype(BF16)
        before = lax.broadcasted_iota(jnp.int32, (128, 128), 1) < lax.broadcasted_iota(jnp.int32, (128, 128), 0)
        earlier = jnp.dot(before.astype(BF16), member, preferred_element_type=F32)
        col = lax.broadcasted_iota(jnp.int32, (128, ROWS), 1)
        for x in range(LOCAL):
            total = jnp.zeros((128, ROWS), F32)
            for k in range(2):
                place = jnp.sum(jnp.where(hits[k], earlier, 0.0), axis=1, keepdims=True).astype(jnp.int32)
                one = ids[:, k : k + 1]
                here = (one & 1 == x) & ((one >> 1) * CAP + place == col)
                total = total + jnp.where(here, weights[:, k : k + 1], 0.0)
            high = total.astype(BF16)
            shares[x, 0:128] = high
            shares[x, 128:256] = (total - high.astype(F32)).astype(BF16)
    steps = (1, NZ - 1)

    def place(way, m):
        if m == STEPS:
            return z, way
        return lax.rem(z + SCATTER_D[m] * steps[way], NZ), SCATTER_X[way][m]

    def across(way, m):
        return remote(
            c_out.at[way, m], c_in.at[way, m], c_send.at[way, m], c_recv.at[way, m],
            (ep, z, 1 - core),
        )

    def ring_copy(way, m):
        return remote(
            r_out.at[way, m], r_in.at[way, m], r_send.at[way, m], r_recv.at[way, m],
            (ep, lax.rem(z + steps[way], NZ), core),
        )

    def partial(at, at_core, x, add, out):
        def tile(j, _):
            cols = pl.ds(pl.multiple_of(j * 512, 512), 512)
            total = jnp.dot(hid[at, at_core, x], w_down[x, :, cols], preferred_element_type=F32)
            for ref in add:
                total = total + ref[:, cols].astype(F32)
            out[:, cols] = total.astype(BF16)
            return 0

        lax.fori_loop(0, 4, tile, 0)

    def help_other(m):
        for way in range(2):
            at, x = place(way, m)
            partial(at, 1 - core, x, (), c_out.at[way, m])
            across(way, m).start()

    help_other(0)
    help_other(1)
    for m in range(STEPS):
        for way in range(2):
            at, x = place(way, m)
            add = [c_in.at[way, m]]
            across(way, m).wait_recv()
            came = SCATTER_IN[way][m]
            if came is not None:
                ring_copy(way, came).wait_recv()
                add.append(r_in.at[way, came])
            partial(at, core, x, add, r_out.at[way, m])
            ring_copy(way, m).start()
        if m + 2 <= STEPS:
            help_other(m + 2)
        if m == 0:
            split_weights()
        elif m == 1:
            tables()
        elif m < 5:
            lax.fori_loop((m - 2) * 5, (5, 10, 16)[m - 2], mix, 0)
        elif m == 6:
            lax.fori_loop(0, EP // 2, last, 0)

    def exchange(x, k):
        to = lax.rem(ep + k, EP)
        return remote(
            b_out.at[x, to], back.at[x, ep], a_send.at[x, k], a_recv.at[x, k], (to, z, core)
        )

    for x in (1, 0):
        across(x, STEPS).wait_recv()
        for way in range(2):
            ring_copy(way, LAST_IN[x][way]).wait_recv()

        def tile(j, _, x=x):
            cols = pl.ds(pl.multiple_of(j * 256, 256), 256)
            total = jnp.dot(hid[z, core, x], w_down[x, :, cols], preferred_element_type=F32)
            for ref in (c_in.at[x, STEPS], r_in.at[0, LAST_IN[x][0]], r_in.at[1, LAST_IN[x][1]]):
                total = total + ref[:, cols].astype(F32)
            b_in[j] = total.astype(BF16)
            return 0

        lax.fori_loop(0, 8, tile, 0)

        def spread_out(j, _, x=x):
            rows = pl.ds(pl.multiple_of(j * (4 * EIGHTS), 4 * EIGHTS), 4 * EIGHTS)
            wide = jnp.dot(spread[rows, :], b_in[...].reshape(8 * ROWS, 256), preferred_element_type=F32)
            b_out[x, pl.ds(j * 4, 4)] = wide.astype(BF16).reshape(4, EIGHTS, 256)
            return 0

        lax.fori_loop(0, 4, spread_out, 0)

        def send_one(k, _, x=x):
            exchange(x, k).start()
            return 0

        lax.fori_loop(1, EP, send_one, 0)
        back[x, ep] = b_out[x, ep]
    for x in (1, 0):

        def came_one(k, _, x=x):
            exchange(x, k).wait_recv()
            return 0

        lax.fori_loop(1, EP, came_one, 0)

        def combine(j, _, x=x):
            rows = pl.ds(pl.multiple_of(j * ROWS, ROWS), ROWS)
            part = jnp.dot(
                gather[rows], back[x].reshape(EP * EIGHTS, 256), preferred_element_type=F32
            ).astype(BF16)
            both = jnp.dot(shares[x], part, preferred_element_type=F32)
            both = both[0:128] + both[128:256]
            if x == 1:
                sums[j] = both
            else:
                cols = pl.ds(pl.multiple_of(j * 256, 256), 256)
                expert_out[:, cols] = (sums[j] + both).astype(BF16)
            return 0

        lax.fori_loop(0, 8, combine, 0)
    for way in range(2):
        for m in range(STEPS):
            ring_copy(way, m).wait_send()
            across(way, m).wait_send()
        across(way, STEPS).wait_send()
    for x in (1, 0):

        def end_one(k, _, x=x):
            exchange(x, k).wait_send()
            return 0

        lax.fori_loop(1, EP, end_one, 0)


DMA = pltpu.SemaphoreType.DMA


def per_device(
    mixer_in, expert_in, mixer_gain, w_outer, w_inner, w_value, conv_taps, w_mix_out,
    expert_gain, w_gate, w_up, w_down, route_ids, route_weights,
):
    tok_count, width = expert_in.shape
    taps = jnp.concatenate((conv_taps, jnp.zeros((5, 128), F32)), axis=0)
    vmem = pl.BlockSpec(memory_space=pltpu.VMEM)
    anywhere = pl.BlockSpec(memory_space=pl.ANY)
    hid, mix_rows, taps_all, wall = pl.pallas_call(
        gather_kernel,
        out_shape=(
            jax.ShapeDtypeStruct((NZ, 2, LOCAL, ROWS, 128), BF16),
            jax.ShapeDtypeStruct((tok_count + 16, width), BF16),
            jax.ShapeDtypeStruct((NZ * 2, 8, 128), F32),
            jax.ShapeDtypeStruct((EP, 2, NZ, 4, 128, 128), BF16),
        ),
        in_specs=[vmem] * 6 + [anywhere] * 6,
        out_specs=(vmem, vmem, vmem, anywhere),
        scratch_shapes=[
            pltpu.VMEM((512, 512), BF16),
            pltpu.VMEM((EP, QUADS, 512), BF16),
            pltpu.VMEM((EP, QUADS, 512), BF16),
            pltpu.VMEM((4, 128, 128), BF16),
            pltpu.VMEM((NZ, 4, 128, 128), BF16),
            pltpu.VMEM((16, width), BF16),
            pltpu.VMEM((16, width), BF16),
            pltpu.VMEM((LOCAL, ROWS, width), BF16),
            pltpu.VMEM((NZ, 2, LOCAL, ROWS, width), BF16),
            pltpu.VMEM((LOCAL, width, 256), BF16),
            DMA((4,)), DMA((LOCAL, 2)), DMA((EP,)), DMA((EP,)), DMA((2, STEPS)), DMA((2, STEPS)),
            DMA((NZ * 2,)), DMA((NZ * 2,)), DMA((2,)),
            DMA((2, STEPS)), DMA((2, STEPS)), DMA((2, STEPS + 1)), DMA((2, STEPS + 1)),
            DMA((2, 2, KINDS)), DMA((2, 2, KINDS)), DMA((2, 2, KINDS)), DMA((2, 2, KINDS)), DMA((3,)),
        ],
        cost_estimate=pl.CostEstimate(flops=10**11, bytes_accessed=3 * 10**8, transcendentals=0),
        compiler_params=pltpu.CompilerParams(
            collective_id=0, has_side_effects=True, vmem_limit_bytes=60 * 2**20
        ),
        name="gather_experts",
    )(
        mixer_in, expert_in, mixer_gain[None, :], expert_gain[None, :], route_ids.T, taps,
        w_outer, w_inner, w_value, w_mix_out, w_gate, w_up,
    )
    return pl.pallas_call(
        scatter_kernel,
        out_shape=(
            jax.ShapeDtypeStruct((tok_count, width), BF16),
            jax.ShapeDtypeStruct((tok_count, width), BF16),
        ),
        in_specs=[vmem] * 6 + [anywhere],
        out_specs=(vmem, vmem),
        scratch_shapes=[
            pltpu.VMEM((2, STEPS + 1, ROWS, width), BF16),
            pltpu.VMEM((2, STEPS + 1, ROWS, width), BF16),
            pltpu.VMEM((2, STEPS, ROWS, width), BF16),
            pltpu.VMEM((2, STEPS, ROWS, width), BF16),
            pltpu.VMEM((8, ROWS, 256), BF16),
            pltpu.VMEM((LOCAL, EP, EIGHTS, 256), BF16),
            pltpu.VMEM((LOCAL, EP, EIGHTS, 256), BF16),
            pltpu.VMEM((EP * EIGHTS, 8 * ROWS), BF16),
            pltpu.VMEM((8 * ROWS, EP * EIGHTS), BF16),
            pltpu.VMEM((LOCAL, 256, ROWS), BF16),
            pltpu.VMEM((8, 128, 256), F32),
            pltpu.VMEM((NZ * 2, 128, 128), BF16),
            pltpu.VMEM((2, EP, 3, 128, 128), BF16),
            pltpu.VMEM((2, 2, 2, NZ, 128, 128), BF16),
            DMA((2, STEPS + 1)), DMA((2, STEPS + 1)), DMA((2, STEPS)), DMA((2, STEPS)),
            DMA((LOCAL, EP)), DMA((LOCAL, EP)), DMA((2,)), DMA((2,)),
        ],
        cost_estimate=pl.CostEstimate(flops=10**11, bytes_accessed=3 * 10**8, transcendentals=0),
        compiler_params=pltpu.CompilerParams(
            collective_id=1, has_side_effects=True, vmem_limit_bytes=62 * 2**20
        ),
        name="scatter_experts",
    )(hid, w_down, mix_rows, taps_all, route_ids, route_weights, wall)


def solution(mesh):
    finer = Mesh(mesh.devices.reshape(mesh.shape["ep"], 8, 2), EP_TP)
    return jax.shard_map(
        per_device,
        mesh=finer,
        in_specs=(
            P(EP_TP, None), P(EP_TP, None), P(), P(None, TP), P(None, TP), P(None, TP),
            P(None, TP), P(TP, None), P(), P("ep", None, TP), P("ep", None, TP),
            P("ep", TP, None), P(EP_TP, None), P(EP_TP, None),
        ),
        out_specs=(P(EP_TP, None), P(EP_TP, None)),
        check_vma=False,
    )
```

time: 318 us -> 284 us (0.89)
  between operations: 14.5 us -> 0.65 us
  other arithmetic: 12.7 us -> 0 us
  matrix products: 7.5 us -> 0 us
  Pallas kernels: 270 us -> 275 us
  local copies, waits for them, and re-layouts: 12.1 us -> 7.86 us
    another operation x3 -> x0, other arithmetic: 7.87 us -> none
    dot_general x9 -> x0, matrix products: 7.5 us -> none  [the longest x8 6.64 us: per_device(): sums = jnp.dot(both, back, preferred_element_type=F32)]
    pallas_call x4 -> x2, Pallas kernels: 270 us -> 275 us  [the longest x1 145 us: per_device(): pl.pallas_call(gather_kernel, out_shape=(jax.ShapeDtypeStruct((NZ, 2, LOC...]
    unnamed x62 -> x4, local copies, waits for them, and re-layouts: 11.3 us -> 6.59 us
  transfers between devices with their start and end apart: 2 -> 0, of which waited for: 0 -> 0; matrix products, arithmetic and copies ran while one was open for 5% -> 0% of each run, Pallas kernels for 73% -> 0%
where the time goes in v3:
time: 284 us
  Pallas kernels  275 us (97%)
  local copies, waits for them, and re-layouts  7.86 us (3%)
    pallas_call x1, Pallas kernels, per_device(): pl.pallas_call(gather_kernel, out_shape=(jax.ShapeDtypeStruct((NZ, 2, LOC...  145 us
    pallas_call x1, Pallas kernels, per_device(): pl.pallas_call(scatter_kernel, out_shape=(jax.ShapeDtypeStruct((tok_count...  130 us
    unnamed x4, local copies, waits for them, and re-layouts  6.59 us

profile of v3, /device:TPU:1, one launch (start us, length us, event | category | flops | bytes accessed | tf_op | source)
XLA Modules:
  0.0 283.5 jit_solution(11119446723525296323)
XLA Ops:
  0.6 1.3 concatenate.3.taps
  1.9 1.4 copy.17.weights
  3.3 1.4 copy.16.ids
  4.7 145.3 %gather_experts.1 = (bf16[8,2,2,160,128]{4,3,2,1,0:T(8,128)(2,1)}, bf16[144,2048]{1,0:T(8,128)(2,1)}, f32[16,8,128]{2,1,0:T(8,128)}, bf16[16,2,8,4,128,128]{5,4,3,2,1,0:T(8,128)(2,1)}) custom-call(bf16[128,2048]{1,0:T(8,128)(2,1)} %mixer_in.1, bf16[128,2048]{1,0:T(8,128)(2,1)} %expert_in.1, f32[1,2048]{1,0:T(1,128)} %bitcast.4, f32[1,2048]{1,0:T(1,128)} %bitcast.5, ...), custom_call_target="tpu_custom_call" | custom-call | flops 99999997952 | bytes 300000000 | tf_op jit(solution)/shard_map/gather_experts/pallas_call | solution.py:609
  150.0 129.8 %scatter_experts.1 = (bf16[128,2048]{1,0:T(8,128)(2,1)}, bf16[128,2048]{1,0:T(8,128)(2,1)}) custom-call(bf16[8,2,2,160,128]{4,3,2,1,0:T(8,128)(2,1)} %get-tuple-element.6.hid, bf16[2,128,2048]{2,1,0:T(8,128)(2,1)} %w_down.1, bf16[144,2048]{1,0:T(8,128)(2,1)} %get-tuple-element.7.tok, f32[16,8,128]{2,1,0:T(8,128)} %get-tuple-element.8.taps, ...), custom_call_target="tpu_custom_call" | custom-call | flops 99999997952 | bytes 300000000 | tf_op jit(solution)/shard_map/scatter_experts/pallas_call | solution.py:644
  279.8 1.9 copy.20
  281.7 1.9 copy.21

commit v4 on v0

v4 whole, which is shorter than its diff:
```python
import functools

import jax
import jax.numpy as jnp
from jax import lax
from jax.experimental import pallas as pl
from jax.experimental.pallas import tpu as pltpu
from jax.sharding import Mesh
from jax.sharding import PartitionSpec as P

EXPERTS = 32
CAP = 10
EIGHTS = 80
EP = 16
NZ = 8
LOCAL = 2
ROWS = EP * CAP
TP = ("tp_0", "tp_1")
EP_TP = ("ep", "tp_0", "tp_1")
MESH = pl.DeviceIdType.MESH
F32 = jnp.float32
BF16 = jnp.bfloat16

norm_eps = 1e-06
clamp_limit = 7.0
gate_alpha = 1.702


def normed(values, gain):
    scaled = values * lax.rsqrt(jnp.mean(values * values, axis=-1, keepdims=True) + norm_eps)
    return (scaled * gain).astype(BF16)


def places():
    return lax.axis_index("ep"), lax.axis_index("tp_0"), lax.axis_index("tp_1")


def signal(where):
    pl.semaphore_signal(
        pltpu.get_barrier_semaphore(), inc=1, device_id=where, device_id_type=MESH
    )


def signal_all(count, where):
    def one(k, _):
        signal(where(k))
        return 0

    lax.fori_loop(1, count, one, 0)


def signal_ring(ep, z, core):
    for step in (1, NZ - 1):
        signal((ep, lax.rem(z + step, NZ), core))
    signal((ep, z, 1 - core))


def remote(src, dst, send, recv, where):
    return pltpu.make_async_remote_copy(
        src_ref=src, dst_ref=dst, send_sem=send, recv_sem=recv, device_id=where, device_id_type=MESH
    )


def each(count, act):
    def one(k, _):
        act(k)
        return 0

    lax.fori_loop(1, count, one, 0)


GATHER_D = (1, 1, 2, 2, 3, 3, 4)
GATHER_X = ((0, 1, 0, 1, 0, 1, 0), (0, 1, 0, 1, 0, 1, 1))
SCATTER_D = ((3, 4, 2, 3, 1, 2, 1), (3, 4, 3, 2, 2, 1, 1))
SCATTER_X = ((1, 0, 1, 0, 1, 0, 0), (0, 1, 1, 0, 1, 1, 0))
SCATTER_IN = ((None, None, 0, 1, 2, 3, 5), (None, None, 1, 0, 2, 4, 3))
LAST_IN = {1: (4, 5), 0: (6, 6)}
STEPS = 7
C_IN = 3
C_OUT = 2
R_OUT = 3
LINE = (0, 3, 1, 2)
KINDS = 10


def forwards(way, n):
    nxt = 6 if (way, n) == (1, 5) else n + 2
    if nxt < STEPS and GATHER_X[way][nxt] == GATHER_X[way][n] and GATHER_D[nxt] == GATHER_D[n] + 1:
        return nxt
    return None


def whole_kernel(
    mixer_in, expert_in, mixer_gain, expert_gain, ids, weights, taps, w_down,
    w_outer, w_inner, w_value, w_mix, w_gate, w_up,
    mixer_out, expert_out, wall,
    tap, slots, landed, back, b_in, wz, halo, mix_rows, taps_all, units, w_both, hid,
    c_out, c_in, r_out, r_in, spread, gather, shares, sums, gated, w_slots,
    w_sem, g_sem, a_send, a_recv, b_send, b_recv, z_send, z_recv, t_send, t_recv, h_sem,
    r_send, r_recv, c_send, c_recv, x_send, x_recv, d_send, d_recv, o_sem,
    s_send, s_recv, p_send, p_recv, m_sem, free_sem,
):
    ep, z, core = places()
    own = pl.ds(pl.multiple_of(ep * 128, 128), 128)
    loads = [
        pltpu.make_async_copy(w.at[own], wz.at[z, i], w_sem.at[i])
        for i, w in enumerate((w_inner, w_value, w_outer))
    ]
    loads.append(pltpu.make_async_copy(w_mix.at[:, own], wz.at[z, 3], w_sem.at[3]))
    for load in loads:
        load.start()
    gate_loads = []
    for x in range(LOCAL):
        gate_loads.append(pltpu.make_async_copy(w_gate.at[x], w_both.at[x, :, 0:128], g_sem.at[x, 0]))
        gate_loads.append(pltpu.make_async_copy(w_up.at[x], w_both.at[x, :, 128:256], g_sem.at[x, 1]))
    for load in gate_loads:
        load.start()
    spot = z * 2 + core
    partner = (ep, z, 1 - core)

    def tp_peer(k):
        to = lax.rem(spot + k, NZ * 2)
        return ep, to // 2, lax.rem(to, 2)

    def in_order(step):
        to = lax.rem(ep * (NZ * 2) + spot + step, EP * NZ * 2)
        return to // (NZ * 2), lax.rem(to // 2, NZ), lax.rem(to, 2)

    def ep_peer(k):
        return lax.rem(ep + k, EP), z, core

    signal_all(EP, ep_peer)
    signal_all(NZ * 2, tp_peer)
    signal(in_order(1))
    signal(in_order(EP * NZ * 2 - 1))

    def exchange(x, k):
        where = ep_peer(k)
        return remote(
            slots.at[x, where[0]], landed.at[x, ep], a_send.at[x, k], a_recv.at[x, k], where
        )

    def hand_back(x, k):
        where = ep_peer(k)
        return remote(
            slots.at[x, where[0]], back.at[x, ep], b_send.at[x, k], b_recv.at[x, k], where
        )

    def tell_taps(k):
        return remote(tap, taps_all.at[spot], t_send.at[k], t_recv.at[k], tp_peer(k))

    def tell_tail():
        return remote(mix_rows.at[128:144], halo, h_sem.at[0], h_sem.at[1], in_order(1))

    steps = (NZ - 1, 1)

    def spread_z(way, n):
        away = GATHER_D[n] - 1
        at = lax.rem(z + away * steps[way], NZ)
        there = (ep, lax.rem(z + (NZ - steps[way]), NZ), core)
        two = pl.ds(2 * GATHER_X[way][n], 2)
        return remote(
            wz.at[at, two], wz.at[at, two], z_send.at[way, n], z_recv.at[way, n], there
        )

    def ring_copy(way, n):
        at = lax.rem(z + (GATHER_D[n] - 1) * steps[way], NZ)
        x = GATHER_X[way][n]
        there = lax.rem(z + (NZ - steps[way]), NZ)
        ref = units.at[at, core, x]
        return remote(ref, ref, r_send.at[way, n], r_recv.at[way, n], (ep, there, core))

    def across(way, n):
        mine = n == STEPS
        at = z if mine else lax.rem(z + GATHER_D[n] * steps[way], NZ)
        x = way if mine else GATHER_X[way][n]
        ref = units.at[at, core, x]
        return remote(ref, ref, c_send.at[way, n], c_recv.at[way, n], partner), at, x

    at_x, at_y = lax.rem(ep, 4), ep // 4

    def off(half, du, dv):
        dx, dy = (du, dv) if half == 0 else (dv, du)
        return lax.rem(at_y + dy, 4) * 4 + lax.rem(at_x + dx, 4)

    def piece(half, way, kind, e, at_core):
        zs = pl.ds(at_core * NZ + 4 * half, 4)
        if kind == 1 or kind >= 6:
            zs = pl.ds(at_core * NZ + 4 * half + 2 * way, 2)
        return wall.at[e, zs]

    def plane(half, way, kind):
        step = 1 if way == 0 else 3
        if kind == 0:
            e, to = ep, off(half, step, 0)
        elif kind == 1:
            e, to = off(half, 4 - step, 0), off(half, step, 0)
        elif kind < 6:
            e, to = off(half, LINE[kind - 2], 0), off(half, 0, step)
        else:
            e, to = off(half, LINE[kind - 6], 4 - step), off(half, 0, step)
        ref = piece(half, way, kind, e, core)
        return remote(
            wz.at[pl.ds(4 * half, 4)] if kind in (0, 2) else ref, ref,
            x_send.at[half, way, kind], x_recv.at[half, way, kind], (to, z, core),
        )

    def plane_over(half, way, kind):
        step = 1 if way == 0 else 3
        if kind == 0:
            e = off(half, 4 - step, 0)
        elif kind == 1:
            e = off(half, 2, 0)
        elif kind < 6:
            e = off(half, LINE[kind - 2], 4 - step)
        else:
            e = off(half, LINE[kind - 6], 2)
        ref = piece(half, way, kind, e, core)
        return remote(ref, ref, d_send.at[half, way, kind], d_recv.at[half, way, kind], partner)

    both_halves = [(half, way) for half in range(2) for way in range(2)]

    def take(*kinds):
        for kind in kinds:
            for half, way in both_halves:
                plane(half, way, kind).wait_recv()
                plane_over(half, way, kind).start()

    def give(*kinds):
        for kind in kinds:
            for half, way in both_halves:
                plane(half, way, kind).start()

    own_wall = wall.at[ep, pl.ds(core * NZ, NZ)]

    def own_over():
        return remote(wz, own_wall, o_sem.at[0], o_sem.at[1], partner)

    def own_keep():
        return pltpu.make_async_copy(wz, own_wall, o_sem.at[2])

    def compute(at_z, at_core, x):
        both = jnp.dot(units[at_z, at_core, x], w_both[x], preferred_element_type=F32)
        gate_pre = jnp.minimum(both[:, 0:128], clamp_limit)
        up_pre = jnp.clip(both[:, 128:256], -clamp_limit, clamp_limit)
        hid[at_z, at_core, x] = (
            (up_pre + 1.0) * gate_pre * jax.nn.sigmoid(gate_alpha * gate_pre)
        ).astype(BF16)

    def pass_z(n):
        for way in range(2):
            spread_z(way, n).wait_recv()
            nxt = forwards(way, n)
            if nxt is not None:
                spread_z(way, nxt).start()

    go = (1, NZ - 1)

    def place(way, m):
        if m == STEPS:
            return z, way
        return lax.rem(z + SCATTER_D[way][m] * go[way], NZ), SCATTER_X[way][m]

    def help_copy(way, m):
        return remote(
            c_out.at[way, m % C_OUT], c_in.at[way, m % C_IN], p_send.at[way, m], p_recv.at[way, m], partner
        )

    def sum_copy(way, m):
        return remote(
            r_out.at[way, m % R_OUT], r_in.at[way, m], s_send.at[way, m], s_recv.at[way, m],
            (ep, lax.rem(z + go[way], NZ), core),
        )

    def partial(at, at_core, x, add, out):
        def tile(j, _):
            cols = pl.ds(pl.multiple_of(j * 512, 512), 512)
            total = jnp.dot(hid[at, at_core, x], w_down[x, :, cols], preferred_element_type=F32)
            for ref in add:
                total = total + ref[:, cols].astype(F32)
            out[:, cols] = total.astype(BF16)
            return 0

        lax.fori_loop(0, 4, tile, 0)

    def help_other(m):
        for way in range(2):
            at, x = place(way, m)
            if m >= C_OUT:
                help_copy(way, m - C_OUT).wait_send()
            partial(at, 1 - core, x, (), c_out.at[way, m % C_OUT])
            if m >= C_IN:
                pl.semaphore_wait(free_sem.at[way], 1)
            help_copy(way, m).start()

    def used(way, m):
        if m + C_IN <= STEPS:
            pl.semaphore_signal(free_sem.at[way], inc=1, device_id=partner, device_id_type=MESH)

    def send_sums(m):
        for way in range(2):
            at, x = place(way, m)
            add = [c_in.at[way, m % C_IN]]
            help_copy(way, m).wait_recv()
            came = SCATTER_IN[way][m]
            if came is not None:
                sum_copy(way, came).wait_recv()
                add.append(r_in.at[way, came])
            if m >= R_OUT:
                sum_copy(way, m - R_OUT).wait_send()
            partial(at, core, x, add, r_out.at[way, m % R_OUT])
            sum_copy(way, m).start()
            used(way, m)

    def fetch(t):
        at = lax.rem(t, 2)
        return pltpu.make_async_copy(wall.at[:, t, 0:3], w_slots.at[at], m_sem.at[at, 0])

    def fetch_last(j):
        at = lax.rem(j, 2)
        return [
            pltpu.make_async_copy(wall.at[2 * j + i, :, 3], w_slots.at[at, :, i], m_sem.at[at, i])
            for i in range(2)
        ]

    def mix(t, _):
        fetch(t).wait()
        at = lax.rem(t, 2)
        rows = mix_rows[...]
        pair = jnp.concatenate([w_slots[at, :, i].reshape(2048, 128) for i in range(2)], axis=1)
        pair = jnp.dot(rows, pair, preferred_element_type=F32)
        prod = pair[:, 0:128] * pair[:, 128:256]
        outer = jnp.dot(
            rows[16:144], w_slots[at, :, 2].reshape(2048, 128), preferred_element_type=F32
        )
        tap_at = taps_all[lax.rem(t, NZ) * 2 + t // NZ]
        conv = tap_at[2:3] * prod[16:144] + tap_at[1:2] * prod[15:143] + tap_at[0:1] * prod[14:142]
        gated[t] = (outer * conv).astype(BF16)

        @pl.when(t + 2 < NZ * 2)
        def _():
            fetch(t + 2).start()

        return 0

    def last(j, _):
        for copy in fetch_last(j):
            copy.wait()
        at = lax.rem(j, 2)
        rows = jnp.concatenate([gated[t] for t in range(NZ * 2)], axis=1)
        pair = jnp.concatenate([w_slots[at, :, i].reshape(2048, 128) for i in range(2)], axis=1)
        cols = pl.ds(pl.multiple_of(j * 256, 256), 256)
        mixer_out[:, cols] = jnp.dot(rows, pair, preferred_element_type=F32).astype(BF16)

        @pl.when(j + 2 < EP // 2)
        def _():
            for copy in fetch_last(j + 2):
                copy.start()

        return 0

    def fill_tables(j, _):
        rows = pl.ds(pl.multiple_of(j * 320, 320), 320)
        row = lax.broadcasted_iota(jnp.int32, (320, 1), 0) + j * 320
        col = lax.broadcasted_iota(jnp.int32, (320, spread.shape[1]), 1)
        slot = lax.rem(row, CAP)
        to = lax.rem(row, EIGHTS) // CAP * ROWS + row // EIGHTS * CAP + slot
        spread[rows] = (to == col).astype(F32).astype(BF16)
        to = lax.rem(row, ROWS) // CAP * EIGHTS + row // ROWS * CAP + slot
        gather[rows] = (to == col).astype(F32).astype(BF16)
        return 0

    def spread_rows(x):
        def one(j, _):
            rows = pl.ds(pl.multiple_of(j * (4 * EIGHTS), 4 * EIGHTS), 4 * EIGHTS)
            wide = jnp.dot(spread[rows], b_in[...].reshape(8 * ROWS, 256), preferred_element_type=F32)
            slots[x, pl.ds(j * 4, 4)] = wide.astype(BF16).reshape(4, EIGHTS, 256)
            return 0

        lax.fori_loop(0, 4, one, 0)

    lax.fori_loop(0, 4, fill_tables, 0)
    experts = lax.broadcasted_iota(jnp.int32, (EXPERTS, 128), 0)
    hits = [experts == ids[k : k + 1, :] for k in range(2)]
    member = (hits[0] | hits[1]).astype(F32).astype(BF16)
    before = lax.broadcasted_iota(jnp.int32, (128, 128), 0) < lax.broadcasted_iota(jnp.int32, (128, 128), 1)
    earlier = jnp.dot(member, before.astype(F32).astype(BF16), preferred_element_type=F32)
    goes = []
    for k in range(2):
        slot = jnp.sum(jnp.where(hits[k], earlier, 0.0), axis=0, keepdims=True).astype(jnp.int32)
        one = ids[k : k + 1, :]
        goes.append((one & 1) * ROWS + (one >> 1) * CAP + slot)
    rows = normed(expert_in[...].astype(F32), expert_gain[...])
    slot_row = lax.broadcasted_iota(jnp.int32, (ROWS, 128), 0)
    for x in range(LOCAL):
        placing = (slot_row + x * ROWS == goes[0]) | (slot_row + x * ROWS == goes[1])
        placing = placing.astype(F32).astype(BF16)
        for j in range(8):
            cols = slice(j * 256, (j + 1) * 256)
            b_in[j] = jnp.dot(placing, rows[:, cols], preferred_element_type=F32).astype(BF16)
        spread_rows(x)
    pl.semaphore_wait(pltpu.get_barrier_semaphore(), EP + NZ * 2)
    each(EP, lambda k: exchange(0, k).start())
    for load in loads:
        load.wait()
    for n in range(LOCAL):
        for way in range(2):
            spread_z(way, n).start()
    each(EP, lambda k: exchange(1, k).start())
    tap[0:3] = taps[...]
    tap[3:8] = jnp.zeros((5, 128), F32)
    each(NZ * 2, lambda k: tell_taps(k).start())
    for x in range(LOCAL):
        landed[x, ep] = slots[x, ep]
    rows = normed(mixer_in[...].astype(F32), mixer_gain[...])
    mix_rows[16:144] = rows
    tell_tail().start()
    pass_z(0)
    taps_all[spot] = tap[...]
    slot_row = lax.broadcasted_iota(jnp.int32, (LOCAL * ROWS, 128), 0)
    held = jnp.zeros((LOCAL * ROWS, 128), F32)
    for k in range(2):
        held = held + jnp.where(slot_row == goes[k], weights[k : k + 1, :], 0.0)
    for x in range(LOCAL):
        total = held[x * ROWS : (x + 1) * ROWS].T
        high = total.astype(BF16)
        shares[x, 0:128] = high
        shares[x, 128:256] = (total - high.astype(F32)).astype(BF16)
    for n in range(1, 4):
        pass_z(n)

    def pack(x):
        def one(j, _):
            rows = pl.ds(pl.multiple_of(j * ROWS, ROWS), ROWS)
            cols = pl.ds(pl.multiple_of(j * 256, 256), 256)
            out = jnp.dot(
                gather[rows], landed[x].reshape(EP * EIGHTS, 256), preferred_element_type=F32
            )
            units[z, core, x, :, cols] = out.astype(BF16)
            return 0

        each(EP, lambda k: exchange(x, k).wait_recv())
        lax.fori_loop(0, 8, one, 0)
        for way in range(2):
            ring_copy(way, x).start()
        across(x, STEPS)[0].start()

    pack(0)
    for load in gate_loads:
        load.wait()
    compute(z, core, 0)
    for n in range(4, STEPS):
        pass_z(n)
    pack(1)
    give(0)
    give(2)
    own_over().start()
    own_keep().start()
    compute(z, core, 1)
    tell_tail().wait()
    lone = (ep == 0) & (spot == 0)
    mix_rows[0:16] = jnp.where(lone, jnp.zeros_like(halo), halo[...])
    each(NZ * 2, lambda k: tell_taps(k).wait())
    for x in range(LOCAL):
        copy, at, _ = across(x, STEPS)
        copy.wait_recv()
        compute(z, 1 - core, x)

    for n in range(STEPS):
        for way in range(2):
            ring_copy(way, n).wait_recv()
            nxt = forwards(way, n)
            if nxt is not None:
                ring_copy(way, nxt).start()
            across(way, n)[0].start()
        if n == 1:
            take(0)
            give(1, 3, 4)
        elif n == 2:
            take(2)
            give(6)
            take(1)
            give(5)
        elif n == 3:
            take(3)
            give(7)
        elif n == 4:
            take(4)
            give(8)
            take(6)
        for way in range(2):
            at = lax.rem(z + GATHER_D[n] * steps[way], NZ)
            compute(at, core, GATHER_X[way][n])
        for way in range(2):
            copy, at, x = across(way, n)
            copy.wait_recv()
            compute(at, 1 - core, x)
        if n == 4:
            each(EP, lambda k: exchange(0, k).wait_send())
            each(EP, lambda k: exchange(1, k).wait_send())
        elif n == 5:
            help_other(0)
            send_sums(0)
            take(5)
            give(9)
        elif n == 6:
            help_other(1)
            send_sums(1)
            help_other(2)
            take(7, 8)
    for m in range(2, STEPS):
        send_sums(m)
        help_other(m + 1)
        if m == 2:
            take(9)
            own_keep().wait()
            own_over().wait()
            for half, way in both_halves:
                for kind in range(KINDS):
                    plane(half, way, kind).wait_send()
                    plane_over(half, way, kind).wait()
            fetch(0).start()
            fetch(1).start()
            lax.fori_loop(0, 4, mix, 0)
        elif m == 3:
            lax.fori_loop(4, 10, mix, 0)
        elif m == 4:
            lax.fori_loop(10, NZ * 2, mix, 0)
            for j in range(2):
                for copy in fetch_last(j):
                    copy.start()
        elif m == 6:
            lax.fori_loop(0, EP // 2, last, 0)

    for x in (1, 0):
        help_copy(x, STEPS).wait_recv()
        for way in range(2):
            sum_copy(way, LAST_IN[x][way]).wait_recv()

        def tile(j, _, x=x):
            cols = pl.ds(pl.multiple_of(j * 256, 256), 256)
            total = jnp.dot(hid[z, core, x], w_down[x, :, cols], preferred_element_type=F32)
            for ref in (
                c_in.at[x, STEPS % C_IN], r_in.at[0, LAST_IN[x][0]], r_in.at[1, LAST_IN[x][1]]
            ):
                total = total + ref[:, cols].astype(F32)
            b_in[j] = total.astype(BF16)
            return 0

        lax.fori_loop(0, 8, tile, 0)
        spread_rows(x)
        each(EP, lambda k, x=x: hand_back(x, k).start())
        back[x, ep] = slots[x, ep]

    for x in (1, 0):
        each(EP, lambda k, x=x: hand_back(x, k).wait_recv())

        def combine(j, _, x=x):
            rows = pl.ds(pl.multiple_of(j * ROWS, ROWS), ROWS)
            values = jnp.dot(
                gather[rows], back[x].reshape(EP * EIGHTS, 256), preferred_element_type=F32
            ).astype(BF16)
            both = jnp.dot(shares[x], values, preferred_element_type=F32)
            both = both[0:128] + both[128:256]
            if x == 1:
                sums[j] = both
            else:
                cols = pl.ds(pl.multiple_of(j * 256, 256), 256)
                expert_out[:, cols] = (sums[j] + both).astype(BF16)
            return 0

        lax.fori_loop(0, 8, combine, 0)
    for way in range(2):
        for n in range(STEPS):
            spread_z(way, n).wait_send()
            ring_copy(way, n).wait_send()
            across(way, n)[0].wait_send()
        across(way, STEPS)[0].wait_send()
        for m in range(STEPS + 1 - C_OUT, STEPS + 1):
            help_copy(way, m).wait_send()
        for m in range(STEPS - R_OUT, STEPS):
            sum_copy(way, m).wait_send()
    for x in (1, 0):
        each(EP, lambda k, x=x: hand_back(x, k).wait_send())


DMA = pltpu.SemaphoreType.DMA


def per_device(
    mixer_in, expert_in, mixer_gain, w_outer, w_inner, w_value, conv_taps, w_mix_out,
    expert_gain, w_gate, w_up, w_down, route_ids, route_weights,
):
    tok_count, width = expert_in.shape
    vmem = pl.BlockSpec(memory_space=pltpu.VMEM)
    anywhere = pl.BlockSpec(memory_space=pl.ANY)
    out = jax.ShapeDtypeStruct((tok_count, width), BF16)
    mixer_out, expert_out, _ = pl.pallas_call(
        whole_kernel,
        out_shape=(out, out, jax.ShapeDtypeStruct((EP, 2 * NZ, 4, 128, 128), BF16)),
        in_specs=[vmem] * 8 + [anywhere] * 6,
        out_specs=(vmem, vmem, anywhere),
        scratch_shapes=[
            pltpu.VMEM((8, 128), F32),
            pltpu.VMEM((LOCAL, EP, EIGHTS, 256), BF16),
            pltpu.VMEM((LOCAL, EP, EIGHTS, 256), BF16),
            pltpu.VMEM((LOCAL, EP, EIGHTS, 256), BF16),
            pltpu.VMEM((8, ROWS, 256), BF16),
            pltpu.VMEM((NZ, 4, 128, 128), BF16),
            pltpu.VMEM((16, width), BF16),
            pltpu.VMEM((tok_count + 16, width), BF16),
            pltpu.VMEM((NZ * 2, 8, 128), F32),
            pltpu.VMEM((NZ, 2, LOCAL, ROWS, width), BF16),
            pltpu.VMEM((LOCAL, width, 256), BF16),
            pltpu.VMEM((NZ, 2, LOCAL, ROWS, 128), BF16),
            pltpu.VMEM((2, C_OUT, ROWS, width), BF16),
            pltpu.VMEM((2, C_IN, ROWS, width), BF16),
            pltpu.VMEM((2, R_OUT, ROWS, width), BF16),
            pltpu.VMEM((2, STEPS, ROWS, width), BF16),
            pltpu.VMEM((EP * EIGHTS, 8 * ROWS), BF16),
            pltpu.VMEM((8 * ROWS, EP * EIGHTS), BF16),
            pltpu.VMEM((LOCAL, 256, ROWS), BF16),
            pltpu.VMEM((8, 128, 256), F32),
            pltpu.VMEM((NZ * 2, 128, 128), BF16),
            pltpu.VMEM((2, EP, 3, 128, 128), BF16),
            DMA((4,)), DMA((LOCAL, 2)), DMA((LOCAL, EP)), DMA((LOCAL, EP)), DMA((LOCAL, EP)), DMA((LOCAL, EP)),
            DMA((2, STEPS)), DMA((2, STEPS)), DMA((NZ * 2,)), DMA((NZ * 2,)), DMA((2,)),
            DMA((2, STEPS)), DMA((2, STEPS)), DMA((2, STEPS + 1)), DMA((2, STEPS + 1)),
            DMA((2, 2, KINDS)), DMA((2, 2, KINDS)), DMA((2, 2, KINDS)), DMA((2, 2, KINDS)), DMA((3,)),
            DMA((2, STEPS)), DMA((2, STEPS)), DMA((2, STEPS + 1)), DMA((2, STEPS + 1)), DMA((2, 2)),
            pltpu.SemaphoreType.REGULAR((2,)),
        ],
        cost_estimate=pl.CostEstimate(flops=10**11, bytes_accessed=3 * 10**8, transcendentals=0),
        compiler_params=pltpu.CompilerParams(
            collective_id=0, has_side_effects=True, vmem_limit_bytes=67043328
        ),
        name="whole_block",
    )(
        mixer_in, expert_in, mixer_gain[None, :], expert_gain[None, :], route_ids.T, route_weights.T,
        conv_taps, w_down, w_outer, w_inner, w_value, w_mix_out, w_gate, w_up,
    )
    return mixer_out, expert_out


def solution(mesh):
    finer = Mesh(mesh.devices.reshape(mesh.shape["ep"], 8, 2), EP_TP)
    return jax.shard_map(
        per_device,
        mesh=finer,
        in_specs=(
            P(EP_TP, None), P(EP_TP, None), P(), P(None, TP), P(None, TP), P(None, TP),
            P(None, TP), P(TP, None), P(), P("ep", None, TP), P("ep", None, TP),
            P("ep", TP, None), P(EP_TP, None), P(EP_TP, None),
        ),
        out_specs=(P(EP_TP, None), P(EP_TP, None)),
        check_vma=False,
    )
```

time: 402 us -> 263 us (0.65)
  waiting for transfers between devices: 261 us -> 0 us
  Pallas kernels: 0 us -> 259 us
  matrix products: 56 us -> 0 us
  blocking collectives: 29 us -> 0 us
  local copies, waits for them, and re-layouts: 22.2 us -> 3.76 us
  between operations: 14 us -> 0.64 us
  starting transfers between devices: 10.1 us -> 0 us
  other arithmetic: 9.98 us -> 0 us
    pallas_call x0 -> x1, Pallas kernels: none -> 259 us  [per_device(): pl.pallas_call(whole_kernel, out_shape=(out, out, jax.ShapeDtypeStruct((E...]
    reduce_scatter x3 -> x0, waiting for transfers between devices: 136 us -> none  [the longest x1 118 us: per_device(): lax.psum_scatter(down_rows(hidden_all, w_down).astype(jnp.bfloat16), TP,...]
    all_gather x2 -> x0, waiting for transfers between devices: 104 us -> none  [the longest x1 81.4 us: per_device(): lax.all_gather(arrived, TP, axis=0, tiled=True)]
    dot_general x7 -> x0, matrix products: 56 us -> none  [the longest x1 13.1 us: per_device(): jnp.dot(gated_rows, w_mix_out, preferred_element_type=jnp.float32)]
    all_to_all x1 -> x0, blocking collectives: 29 us -> none  [per_device(): lax.all_to_all(packed, 'ep', split_axis=0, concat_axis=0, tiled=True)]
    all_to_all x1 -> x0, waiting for transfers between devices: 20.1 us -> none  [per_device(): lax.all_to_all(expert_value, 'ep', split_axis=0, concat_axis=0, tiled=True)]
    transpose x1 -> x0, local copies, waits for them, and re-layouts: 8.54 us -> none  [summed_rows_2(): pieces = pieces.reshape(*sizes, *inside).swapaxes(0, 1).reshape(-1, *inside)]
    reshape x3 -> x0, local copies, waits for them, and re-layouts: 7.73 us -> none  [the longest x1 3.22 us: per_device(): expert_sum.reshape(ep_count, slot_total // ep_count, model_width)]
  transfers between devices with their start and end apart: 7 -> 0, of which waited for: 6 -> 0; matrix products, arithmetic and copies ran while one was open for 21% -> 0% of each run, Pallas kernels for 0% -> 0%
where the time goes in v4:
time: 263 us
  Pallas kernels  259 us (98%)
  local copies, waits for them, and re-layouts  3.76 us (1%)
    pallas_call x1, Pallas kernels, per_device(): pl.pallas_call(whole_kernel, out_shape=(out, out, jax.ShapeDtypeStruct((E...  259 us

profile of v4, /device:TPU:1, one launch (start us, length us, event | category | flops | bytes accessed | tf_op | source)
XLA Modules:
  0.0 263.1 jit_solution(7611453887659829750)
XLA Ops:
  0.6 258.7 %whole_block.1 = (bf16[128,2048]{1,0:T(8,128)(2,1)}, bf16[128,2048]{1,0:T(8,128)(2,1)}, bf16[16,16,4,128,128]{4,3,2,1,0:T(8,128)(2,1)}) custom-call(bf16[128,2048]{1,0:T(8,128)(2,1)} %mixer_in.1, bf16[128,2048]{1,0:T(8,128)(2,1)} %expert_in.1, f32[1,2048]{1,0:T(1,128)} %bitcast.4, f32[1,2048]{1,0:T(1,128)} %bitcast.5, s32[2,128]{1,0:T(2,128)} %bitcast.6, ...), custom_call_target="tpu_custom_call" | custom-call | flops 99999997952 | bytes 300000000 | tf_op jit(solution)/shard_map/whole_block/pallas_call | solution.py:598
  259.3 1.9 copy.18
  261.2 1.9 copy.19

commit v5 on v4

--- a/solution.py
+++ b/solution.py
@@ -77,6 +77,7 @@
 LAST_IN = {1: (4, 5), 0: (6, 6)}
 STEPS = 7
 C_IN = 3
+SWAP = 8 * EIGHTS
 C_OUT = 2
 R_OUT = 3
 LINE = (0, 3, 1, 2)
@@ -91,14 +92,14 @@
 
 
 def whole_kernel(
-    mixer_in, expert_in, mixer_gain, expert_gain, ids, weights, taps, w_down,
-    w_outer, w_inner, w_value, w_mix, w_gate, w_up,
+    expert_in, mixer_gain, expert_gain, ids, weights, taps,
+    mixer_hbm, down_hbm, w_outer, w_inner, w_value, w_mix, w_gate, w_up,
     mixer_out, expert_out, wall,
     tap, slots, landed, back, b_in, wz, halo, mix_rows, taps_all, units, w_both, hid,
-    c_out, c_in, r_out, r_in, spread, gather, shares, sums, gated, w_slots,
+    mixer_in, w_down, c_out, c_in, r_out, r_in, swap, shares, sums, gated, w_slots,
     w_sem, g_sem, a_send, a_recv, b_send, b_recv, z_send, z_recv, t_send, t_recv, h_sem,
     r_send, r_recv, c_send, c_recv, x_send, x_recv, d_send, d_recv, o_sem,
-    s_send, s_recv, p_send, p_recv, m_sem, free_sem,
+    s_send, s_recv, p_send, p_recv, m_sem, i_sem, free_sem,
 ):
     ep, z, core = places()
     own = pl.ds(pl.multiple_of(ep * 128, 128), 128)
@@ -113,7 +114,11 @@
     for x in range(LOCAL):
         gate_loads.append(pltpu.make_async_copy(w_gate.at[x], w_both.at[x, :, 0:128], g_sem.at[x, 0]))
         gate_loads.append(pltpu.make_async_copy(w_up.at[x], w_both.at[x, :, 128:256], g_sem.at[x, 1]))
-    for load in gate_loads:
+    inputs = [
+        pltpu.make_async_copy(mixer_hbm, mixer_in, i_sem.at[0]),
+        pltpu.make_async_copy(down_hbm, w_down, i_sem.at[1]),
+    ]
+    for load in inputs + gate_loads:
         load.start()
     spot = z * 2 + core
     partner = (ep, z, 1 - core)
@@ -297,20 +302,19 @@
         if m + C_IN <= STEPS:
             pl.semaphore_signal(free_sem.at[way], inc=1, device_id=partner, device_id_type=MESH)
 
-    def send_sums(m):
-        for way in range(2):
-            at, x = place(way, m)
-            add = [c_in.at[way, m % C_IN]]
-            help_copy(way, m).wait_recv()
-            came = SCATTER_IN[way][m]
-            if came is not None:
-                sum_copy(way, came).wait_recv()
-                add.append(r_in.at[way, came])
-            if m >= R_OUT:
-                sum_copy(way, m - R_OUT).wait_send()
-            partial(at, core, x, add, r_out.at[way, m % R_OUT])
-            sum_copy(way, m).start()
-            used(way, m)
+    def send_sum(way, m):
+        at, x = place(way, m)
+        add = [c_in.at[way, m % C_IN]]
+        help_copy(way, m).wait_recv()
+        came = SCATTER_IN[way][m]
+        if came is not None:
+            sum_copy(way, came).wait_recv()
+            add.append(r_in.at[way, came])
+        if m >= R_OUT:
+            sum_copy(way, m - R_OUT).wait_send()
+        partial(at, core, x, add, r_out.at[way, m % R_OUT])
+        sum_copy(way, m).start()
+        used(way, m)
 
     def fetch(t):
         at = lax.rem(t, 2)
@@ -359,27 +363,33 @@
 
         return 0
 
-    def fill_tables(j, _):
+    def fill_swap(j, _):
         rows = pl.ds(pl.multiple_of(j * 320, 320), 320)
         row = lax.broadcasted_iota(jnp.int32, (320, 1), 0) + j * 320
-        col = lax.broadcasted_iota(jnp.int32, (320, spread.shape[1]), 1)
-        slot = lax.rem(row, CAP)
-        to = lax.rem(row, EIGHTS) // CAP * ROWS + row // EIGHTS * CAP + slot
-        spread[rows] = (to == col).astype(F32).astype(BF16)
-        to = lax.rem(row, ROWS) // CAP * EIGHTS + row // ROWS * CAP + slot
-        gather[rows] = (to == col).astype(F32).astype(BF16)
+        col = lax.broadcasted_iota(jnp.int32, (320, SWAP), 1)
+        to = lax.rem(row, EIGHTS) // CAP * EIGHTS + row // EIGHTS * CAP + lax.rem(row, CAP)
+        swap[rows] = (to == col).astype(F32).astype(BF16)
         return 0
 
     def spread_rows(x):
         def one(j, _):
-            rows = pl.ds(pl.multiple_of(j * (4 * EIGHTS), 4 * EIGHTS), 4 * EIGHTS)
-            wide = jnp.dot(spread[rows], b_in[...].reshape(8 * ROWS, 256), preferred_element_type=F32)
-            slots[x, pl.ds(j * 4, 4)] = wide.astype(BF16).reshape(4, EIGHTS, 256)
+            rows = pl.ds(pl.multiple_of(j * EIGHTS, EIGHTS), EIGHTS)
+            wide = jnp.dot(swap[...], b_in[:, rows].reshape(SWAP, 256), preferred_element_type=F32)
+            slots[x, pl.ds(j * 8, 8)] = wide.astype(BF16).reshape(8, EIGHTS, 256)
             return 0
 
-        lax.fori_loop(0, 4, one, 0)
-
-    lax.fori_loop(0, 4, fill_tables, 0)
+        lax.fori_loop(0, 2, one, 0)
+
+    def gather_rows(got):
+        def one(j, _):
+            rows = pl.ds(pl.multiple_of(j * EIGHTS, EIGHTS), EIGHTS)
+            out = jnp.dot(swap[...], got[pl.ds(j * 8, 8)].reshape(SWAP, 256), preferred_element_type=F32)
+            b_in[:, rows] = out.astype(BF16).reshape(8, EIGHTS, 256)
+            return 0
+
+        lax.fori_loop(0, 2, one, 0)
+
+    rows = normed(expert_in[...].astype(F32), expert_gain[...])
     experts = lax.broadcasted_iota(jnp.int32, (EXPERTS, 128), 0)
     hits = [experts == ids[k : k + 1, :] for k in range(2)]
     member = (hits[0] | hits[1]).astype(F32).astype(BF16)
@@ -390,67 +400,66 @@
         slot = jnp.sum(jnp.where(hits[k], earlier, 0.0), axis=0, keepdims=True).astype(jnp.int32)
         one = ids[k : k + 1, :]
         goes.append((one & 1) * ROWS + (one >> 1) * CAP + slot)
-    rows = normed(expert_in[...].astype(F32), expert_gain[...])
     slot_row = lax.broadcasted_iota(jnp.int32, (ROWS, 128), 0)
-    for x in range(LOCAL):
+
+    def fill_slots(x):
         placing = (slot_row + x * ROWS == goes[0]) | (slot_row + x * ROWS == goes[1])
-        placing = placing.astype(F32).astype(BF16)
+        out = jnp.dot(placing.astype(F32).astype(BF16), rows, preferred_element_type=F32).astype(BF16)
         for j in range(8):
-            cols = slice(j * 256, (j + 1) * 256)
-            b_in[j] = jnp.dot(placing, rows[:, cols], preferred_element_type=F32).astype(BF16)
+            b_in[j] = out[:, j * 256 : (j + 1) * 256]
         spread_rows(x)
+
     pl.semaphore_wait(pltpu.get_barrier_semaphore(), EP + NZ * 2)
-    each(EP, lambda k: exchange(0, k).start())
     for load in loads:
         load.wait()
     for n in range(LOCAL):
         for way in range(2):
             spread_z(way, n).start()
+    lax.fori_loop(0, 2, fill_swap, 0)
+    fill_slots(0)
+    each(EP, lambda k: exchange(0, k).start())
+    pass_z(0)
+    fill_slots(1)
     each(EP, lambda k: exchange(1, k).start())
+    pass_z(1)
+    for x in range(LOCAL):
+        landed[x, ep] = slots[x, ep]
     tap[0:3] = taps[...]
     tap[3:8] = jnp.zeros((5, 128), F32)
     each(NZ * 2, lambda k: tell_taps(k).start())
-    for x in range(LOCAL):
-        landed[x, ep] = slots[x, ep]
-    rows = normed(mixer_in[...].astype(F32), mixer_gain[...])
-    mix_rows[16:144] = rows
+    for load in inputs:
+        load.wait()
+    mixed = normed(mixer_in[...].astype(F32), mixer_gain[...])
+    mix_rows[16:144] = mixed
+    pass_z(2)
     tell_tail().start()
-    pass_z(0)
     taps_all[spot] = tap[...]
     slot_row = lax.broadcasted_iota(jnp.int32, (LOCAL * ROWS, 128), 0)
     held = jnp.zeros((LOCAL * ROWS, 128), F32)
     for k in range(2):
         held = held + jnp.where(slot_row == goes[k], weights[k : k + 1, :], 0.0)
+    pass_z(3)
     for x in range(LOCAL):
         total = held[x * ROWS : (x + 1) * ROWS].T
         high = total.astype(BF16)
         shares[x, 0:128] = high
         shares[x, 128:256] = (total - high.astype(F32)).astype(BF16)
-    for n in range(1, 4):
+    for load in gate_loads:
+        load.wait()
+    for n in range(4, STEPS):
         pass_z(n)
 
     def pack(x):
-        def one(j, _):
-            rows = pl.ds(pl.multiple_of(j * ROWS, ROWS), ROWS)
-            cols = pl.ds(pl.multiple_of(j * 256, 256), 256)
-            out = jnp.dot(
-                gather[rows], landed[x].reshape(EP * EIGHTS, 256), preferred_element_type=F32
-            )
-            units[z, core, x, :, cols] = out.astype(BF16)
-            return 0
-
         each(EP, lambda k: exchange(x, k).wait_recv())
-        lax.fori_loop(0, 8, one, 0)
+        gather_rows(landed.at[x])
+        for j in range(8):
+            units[z, core, x, :, j * 256 : (j + 1) * 256] = b_in[j]
         for way in range(2):
             ring_copy(way, x).start()
         across(x, STEPS)[0].start()
 
     pack(0)
-    for load in gate_loads:
-        load.wait()
     compute(z, core, 0)
-    for n in range(4, STEPS):
-        pass_z(n)
     pack(1)
     give(0)
     give(2)
@@ -500,37 +509,47 @@
             each(EP, lambda k: exchange(1, k).wait_send())
         elif n == 5:
             help_other(0)
-            send_sums(0)
+            send_sum(1, 0)
+            send_sum(0, 0)
             take(5)
             give(9)
         elif n == 6:
             help_other(1)
-            send_sums(1)
+            send_sum(0, 1)
+            send_sum(1, 1)
             help_other(2)
             take(7, 8)
-    for m in range(2, STEPS):
-        send_sums(m)
-        help_other(m + 1)
-        if m == 2:
-            take(9)
-            own_keep().wait()
-            own_over().wait()
-            for half, way in both_halves:
-                for kind in range(KINDS):
-                    plane(half, way, kind).wait_send()
-                    plane_over(half, way, kind).wait()
-            fetch(0).start()
-            fetch(1).start()
-            lax.fori_loop(0, 4, mix, 0)
-        elif m == 3:
-            lax.fori_loop(4, 10, mix, 0)
-        elif m == 4:
-            lax.fori_loop(10, NZ * 2, mix, 0)
-            for j in range(2):
-                for copy in fetch_last(j):
-                    copy.start()
-        elif m == 6:
-            lax.fori_loop(0, EP // 2, last, 0)
+    take(9)
+    own_keep().wait()
+    own_over().wait()
+    for half, way in both_halves:
+        for kind in range(KINDS):
+            plane(half, way, kind).wait_send()
+            plane_over(half, way, kind).wait()
+    fetch(0).start()
+    fetch(1).start()
+    send_sum(0, 2)
+    lax.fori_loop(0, 6, mix, 0)
+    help_other(3)
+    send_sum(1, 2)
+    send_sum(0, 3)
+    send_sum(1, 3)
+    help_other(4)
+    lax.fori_loop(6, 11, mix, 0)
+    send_sum(0, 4)
+    send_sum(1, 4)
+    help_other(5)
+    lax.fori_loop(11, NZ * 2, mix, 0)
+    for j in range(2):
+        for copy in fetch_last(j):
+            copy.start()
+    send_sum(0, 5)
+    help_other(6)
+    lax.fori_loop(0, EP // 2, last, 0)
+    send_sum(1, 5)
+    send_sum(0, 6)
+    send_sum(1, 6)
+    help_other(7)
 
     for x in (1, 0):
         help_copy(x, STEPS).wait_recv()
@@ -555,11 +574,10 @@
     for x in (1, 0):
         each(EP, lambda k, x=x: hand_back(x, k).wait_recv())
 
+        gather_rows(back.at[x])
+
         def combine(j, _, x=x):
-            rows = pl.ds(pl.multiple_of(j * ROWS, ROWS), ROWS)
-            values = jnp.dot(
-                gather[rows], back[x].reshape(EP * EIGHTS, 256), preferred_element_type=F32
-            ).astype(BF16)
+            values = b_in[j]
             both = jnp.dot(shares[x], values, preferred_element_type=F32)
             both = both[0:128] + both[128:256]
             if x == 1:
@@ -598,7 +616,7 @@
     mixer_out, expert_out, _ = pl.pallas_call(
         whole_kernel,
         out_shape=(out, out, jax.ShapeDtypeStruct((EP, 2 * NZ, 4, 128, 128), BF16)),
-        in_specs=[vmem] * 8 + [anywhere] * 6,
+        in_specs=[vmem] * 6 + [anywhere] * 8,
         out_specs=(vmem, vmem, anywhere),
         scratch_shapes=[
             pltpu.VMEM((8, 128), F32),
@@ -613,12 +631,13 @@
             pltpu.VMEM((NZ, 2, LOCAL, ROWS, width), BF16),
             pltpu.VMEM((LOCAL, width, 256), BF16),
             pltpu.VMEM((NZ, 2, LOCAL, ROWS, 128), BF16),
+            pltpu.VMEM((tok_count, width), BF16),
+            pltpu.VMEM(w_down.shape, BF16),
             pltpu.VMEM((2, C_OUT, ROWS, width), BF16),
             pltpu.VMEM((2, C_IN, ROWS, width), BF16),
             pltpu.VMEM((2, R_OUT, ROWS, width), BF16),
             pltpu.VMEM((2, STEPS, ROWS, width), BF16),
-            pltpu.VMEM((EP * EIGHTS, 8 * ROWS), BF16),
-            pltpu.VMEM((8 * ROWS, EP * EIGHTS), BF16),
+            pltpu.VMEM((SWAP, SWAP), BF16),
             pltpu.VMEM((LOCAL, 256, ROWS), BF16),
             pltpu.VMEM((8, 128, 256), F32),
             pltpu.VMEM((NZ * 2, 128, 128), BF16),
@@ -627,7 +646,7 @@
             DMA((2, STEPS)), DMA((2, STEPS)), DMA((NZ * 2,)), DMA((NZ * 2,)), DMA((2,)),
             DMA((2, STEPS)), DMA((2, STEPS)), DMA((2, STEPS + 1)), DMA((2, STEPS + 1)),
             DMA((2, 2, KINDS)), DMA((2, 2, KINDS)), DMA((2, 2, KINDS)), DMA((2, 2, KINDS)), DMA((3,)),
-            DMA((2, STEPS)), DMA((2, STEPS)), DMA((2, STEPS + 1)), DMA((2, STEPS + 1)), DMA((2, 2)),
+            DMA((2, STEPS)), DMA((2, STEPS)), DMA((2, STEPS + 1)), DMA((2, STEPS + 1)), DMA((2, 2)), DMA((2,)),
             pltpu.SemaphoreType.REGULAR((2,)),
         ],
         cost_estimate=pl.CostEstimate(flops=10**11, bytes_accessed=3 * 10**8, transcendentals=0),
@@ -636,8 +655,8 @@
         ),
         name="whole_block",
     )(
-        mixer_in, expert_in, mixer_gain[None, :], expert_gain[None, :], route_ids.T, route_weights.T,
-        conv_taps, w_down, w_outer, w_inner, w_value, w_mix_out, w_gate, w_up,
+        expert_in, mixer_gain[None, :], expert_gain[None, :], route_ids.T, route_weights.T, conv_taps,
+        mixer_in, w_down, w_outer, w_inner, w_value, w_mix_out, w_gate, w_up,
     )
     return mixer_out, expert_out
 

time: 263 us -> 253 us (0.962)
  Pallas kernels: 259 us -> 246 us
    pallas_call x1, Pallas kernels: 259 us -> 246 us  [per_device(): pl.pallas_call(whole_kernel, out_shape=(out, out, jax.ShapeDtypeStruct((E...]
where the time goes in v5:
time: 253 us; the launch traced here: 250 us
  Pallas kernels  246 us (97%)
  local copies, waits for them, and re-layouts  3.76 us (1%)
    pallas_call x1, Pallas kernels, per_device(): pl.pallas_call(whole_kernel, out_shape=(out, out, jax.ShapeDtypeStruct((E...  246 us

profile of v5, /device:TPU:1, one launch (start us, length us, event | category | flops | bytes accessed | tf_op | source)
XLA Modules:
  0.0 250.5 jit_solution(11899012025786222529)
XLA Ops:
  0.6 246.1 %whole_block.1 = (bf16[128,2048]{1,0:T(8,128)(2,1)}, bf16[128,2048]{1,0:T(8,128)(2,1)}, bf16[16,16,4,128,128]{4,3,2,1,0:T(8,128)(2,1)}) custom-call(bf16[128,2048]{1,0:T(8,128)(2,1)} %expert_in.1, f32[1,2048]{1,0:T(1,128)} %bitcast.4, f32[1,2048]{1,0:T(1,128)} %bitcast.5, s32[2,128]{1,0:T(2,128)} %bitcast.6, f32[2,128]{1,0:T(2,128)} %bitcast.7, ...), custom_call_target="tpu_custom_call" | custom-call | flops 99999997952 | bytes 300000000 | tf_op jit(solution)/shard_map/whole_block/pallas_call | solution.py:616
  246.7 1.9 copy.18
  248.6 1.9 copy.19

commit v6 on v5

--- a/solution.py
+++ b/solution.py
@@ -61,6 +61,10 @@
     )
 
 
+def drain(ref, sem):
+    pltpu.make_async_copy(ref, ref, sem).wait()
+
+
 def each(count, act):
     def one(k, _):
         act(k)
@@ -74,7 +78,7 @@
 SCATTER_D = ((3, 4, 2, 3, 1, 2, 1), (3, 4, 3, 2, 2, 1, 1))
 SCATTER_X = ((1, 0, 1, 0, 1, 0, 0), (0, 1, 1, 0, 1, 1, 0))
 SCATTER_IN = ((None, None, 0, 1, 2, 3, 5), (None, None, 1, 0, 2, 4, 3))
-LAST_IN = {1: (4, 5), 0: (6, 6)}
+LAST_IN = {(1, 0): (4, 5), (1, 1): (4, 5), (0, 0): (6, 6), (0, 1): (7, 7)}
 STEPS = 7
 C_IN = 3
 SWAP = 8 * EIGHTS
@@ -92,34 +96,32 @@
 
 
 def whole_kernel(
-    expert_in, mixer_gain, expert_gain, ids, weights, taps,
+    expert_hbm, mixer_gain_hbm, expert_gain_hbm, ids_hbm, weights_hbm, taps_hbm,
     mixer_hbm, down_hbm, w_outer, w_inner, w_value, w_mix, w_gate, w_up,
     mixer_out, expert_out, wall,
-    tap, slots, landed, back, b_in, wz, halo, mix_rows, taps_all, units, w_both, hid,
-    mixer_in, w_down, c_out, c_in, r_out, r_in, swap, shares, sums, gated, w_slots,
+    expert_in, mixer_gain, expert_gain, ids, weights, tap, mixer_in, w_down,
+    slots, landed, b_slots, back, b_in, b_half, wz, halo, mix_rows, taps_all, units, w_both, hid,
+    c_out, c_in, r_out, r_in, swap, shares, sums, gated, w_slots,
     w_sem, g_sem, a_send, a_recv, b_send, b_recv, z_send, z_recv, t_send, t_recv, h_sem,
     r_send, r_recv, c_send, c_recv, x_send, x_recv, d_send, d_recv, o_sem,
     s_send, s_recv, p_send, p_recv, m_sem, i_sem, free_sem,
 ):
     ep, z, core = places()
     own = pl.ds(pl.multiple_of(ep * 128, 128), 128)
-    loads = [
-        pltpu.make_async_copy(w.at[own], wz.at[z, i], w_sem.at[i])
-        for i, w in enumerate((w_inner, w_value, w_outer))
-    ]
-    loads.append(pltpu.make_async_copy(w_mix.at[:, own], wz.at[z, 3], w_sem.at[3]))
-    for load in loads:
+    for i, w in enumerate((w_inner, w_value, w_outer)):
+        pltpu.make_async_copy(w.at[own], wz.at[z, i], w_sem.at[0]).start()
+    pltpu.make_async_copy(w_mix.at[:, own], wz.at[z, 3], w_sem.at[0]).start()
+    pairs = (
+        (expert_hbm, expert_in), (expert_gain_hbm, expert_gain), (ids_hbm, ids),
+        (weights_hbm, weights), (taps_hbm, tap.at[0:3]), (mixer_gain_hbm, mixer_gain),
+        (mixer_hbm, mixer_in), (down_hbm, w_down),
+    )
+    inputs = [pltpu.make_async_copy(src, dst, i_sem.at[i]) for i, (src, dst) in enumerate(pairs)]
+    for load in inputs:
         load.start()
-    gate_loads = []
     for x in range(LOCAL):
-        gate_loads.append(pltpu.make_async_copy(w_gate.at[x], w_both.at[x, :, 0:128], g_sem.at[x, 0]))
-        gate_loads.append(pltpu.make_async_copy(w_up.at[x], w_both.at[x, :, 128:256], g_sem.at[x, 1]))
-    inputs = [
-        pltpu.make_async_copy(mixer_hbm, mixer_in, i_sem.at[0]),
-        pltpu.make_async_copy(down_hbm, w_down, i_sem.at[1]),
-    ]
-    for load in inputs + gate_loads:
-        load.start()
+        pltpu.make_async_copy(w_gate.at[x], w_both.at[x, :, 0:128], g_sem.at[0]).start()
+        pltpu.make_async_copy(w_up.at[x], w_both.at[x, :, 128:256], g_sem.at[0]).start()
     spot = z * 2 + core
     partner = (ep, z, 1 - core)
 
@@ -142,17 +144,18 @@
     def exchange(x, k):
         where = ep_peer(k)
         return remote(
-            slots.at[x, where[0]], landed.at[x, ep], a_send.at[x, k], a_recv.at[x, k], where
+            slots.at[x, where[0]], landed.at[x, ep], a_send.at[x], a_recv.at[x], where
         )
 
-    def hand_back(x, k):
+    def hand_back(x, part, k):
         where = ep_peer(k)
         return remote(
-            slots.at[x, where[0]], back.at[x, ep], b_send.at[x, k], b_recv.at[x, k], where
+            b_slots.at[x, part, where[0]], back.at[x, part, ep],
+            b_send.at[x, part], b_recv.at[x, part], where,
         )
 
     def tell_taps(k):
-        return remote(tap, taps_all.at[spot], t_send.at[k], t_recv.at[k], tp_peer(k))
+        return remote(tap, taps_all.at[spot], t_send.at[0], t_recv.at[0], tp_peer(k))
 
     def tell_tail():
         return remote(mix_rows.at[128:144], halo, h_sem.at[0], h_sem.at[1], in_order(1))
@@ -165,7 +168,7 @@
         there = (ep, lax.rem(z + (NZ - steps[way]), NZ), core)
         two = pl.ds(2 * GATHER_X[way][n], 2)
         return remote(
-            wz.at[at, two], wz.at[at, two], z_send.at[way, n], z_recv.at[way, n], there
+            wz.at[at, two], wz.at[at, two], z_send.at[way], z_recv.at[way, n], there
         )
 
     def ring_copy(way, n):
@@ -173,14 +176,14 @@
         x = GATHER_X[way][n]
         there = lax.rem(z + (NZ - steps[way]), NZ)
         ref = units.at[at, core, x]
-        return remote(ref, ref, r_send.at[way, n], r_recv.at[way, n], (ep, there, core))
+        return remote(ref, ref, r_send.at[way], r_recv.at[way, n], (ep, there, core))
 
     def across(way, n):
         mine = n == STEPS
         at = z if mine else lax.rem(z + GATHER_D[n] * steps[way], NZ)
         x = way if mine else GATHER_X[way][n]
         ref = units.at[at, core, x]
-        return remote(ref, ref, c_send.at[way, n], c_recv.at[way, n], partner), at, x
+        return remote(ref, ref, c_send.at[way], c_recv.at[way, n], partner), at, x
 
     at_x, at_y = lax.rem(ep, 4), ep // 4
 
@@ -207,7 +210,7 @@
         ref = piece(half, way, kind, e, core)
         return remote(
             wz.at[pl.ds(4 * half, 4)] if kind in (0, 2) else ref, ref,
-            x_send.at[half, way, kind], x_recv.at[half, way, kind], (to, z, core),
+            x_send.at[kind], x_recv.at[kind], (to, z, core),
         )
 
     def plane_over(half, way, kind):
@@ -221,14 +224,17 @@
         else:
             e = off(half, LINE[kind - 6], 2)
         ref = piece(half, way, kind, e, core)
-        return remote(ref, ref, d_send.at[half, way, kind], d_recv.at[half, way, kind], partner)
+        return remote(ref, ref, d_send.at[kind], d_recv.at[kind], partner)
 
     both_halves = [(half, way) for half in range(2) for way in range(2)]
+
+    def four(kind):
+        return wall.at[0, 0 : (NZ if kind == 1 or kind >= 6 else 2 * NZ)]
 
     def take(*kinds):
         for kind in kinds:
+            drain(four(kind), x_recv.at[kind])
             for half, way in both_halves:
-                plane(half, way, kind).wait_recv()
                 plane_over(half, way, kind).start()
 
     def give(*kinds):
@@ -272,12 +278,14 @@
         )
 
     def sum_copy(way, m):
+        cols = slice(0, 2048) if m < 6 else slice(1024 * (m - 6), 1024 * (m - 5))
+        step = min(m, 6)
         return remote(
-            r_out.at[way, m % R_OUT], r_in.at[way, m], s_send.at[way, m], s_recv.at[way, m],
-            (ep, lax.rem(z + go[way], NZ), core),
+            r_out.at[way, step % R_OUT, :, cols], r_in.at[way, step, :, cols],
+            s_send.at[way, m], s_recv.at[way, m], (ep, lax.rem(z + go[way], NZ), core),
         )
 
-    def partial(at, at_core, x, add, out):
+    def partial(at, at_core, x, add, out, tiles=(0, 4)):
         def tile(j, _):
             cols = pl.ds(pl.multiple_of(j * 512, 512), 512)
             total = jnp.dot(hid[at, at_core, x], w_down[x, :, cols], preferred_element_type=F32)
@@ -286,7 +294,7 @@
             out[:, cols] = total.astype(BF16)
             return 0
 
-        lax.fori_loop(0, 4, tile, 0)
+        lax.fori_loop(*tiles, tile, 0)
 
     def help_other(m):
         for way in range(2):
@@ -312,8 +320,13 @@
             add.append(r_in.at[way, came])
         if m >= R_OUT:
             sum_copy(way, m - R_OUT).wait_send()
-        partial(at, core, x, add, r_out.at[way, m % R_OUT])
-        sum_copy(way, m).start()
+        if m < 6:
+            partial(at, core, x, add, r_out.at[way, m % R_OUT])
+            sum_copy(way, m).start()
+        else:
+            for part in range(2):
+                partial(at, core, x, add, r_out.at[way, m % R_OUT], (2 * part, 2 * part + 2))
+                sum_copy(way, 6 + part).start()
         used(way, m)
 
     def fetch(t):
@@ -389,6 +402,10 @@
 
         lax.fori_loop(0, 2, one, 0)
 
+    tap[3:8] = jnp.zeros((5, 128), F32)
+    lax.fori_loop(0, 2, fill_swap, 0)
+    for load in inputs[0:3]:
+        load.wait()
     rows = normed(expert_in[...].astype(F32), expert_gain[...])
     experts = lax.broadcasted_iota(jnp.int32, (EXPERTS, 128), 0)
     hits = [experts == ids[k : k + 1, :] for k in range(2)]
@@ -410,12 +427,10 @@
         spread_rows(x)
 
     pl.semaphore_wait(pltpu.get_barrier_semaphore(), EP + NZ * 2)
-    for load in loads:
-        load.wait()
+    drain(wz.at[z], w_sem.at[0])
     for n in range(LOCAL):
         for way in range(2):
             spread_z(way, n).start()
-    lax.fori_loop(0, 2, fill_swap, 0)
     fill_slots(0)
     each(EP, lambda k: exchange(0, k).start())
     pass_z(0)
@@ -424,11 +439,9 @@
     pass_z(1)
     for x in range(LOCAL):
         landed[x, ep] = slots[x, ep]
-    tap[0:3] = taps[...]
-    tap[3:8] = jnp.zeros((5, 128), F32)
+    for load in inputs[3:]:
+        load.wait()
     each(NZ * 2, lambda k: tell_taps(k).start())
-    for load in inputs:
-        load.wait()
     mixed = normed(mixer_in[...].astype(F32), mixer_gain[...])
     mix_rows[16:144] = mixed
     pass_z(2)
@@ -444,13 +457,12 @@
         high = total.astype(BF16)
         shares[x, 0:128] = high
         shares[x, 128:256] = (total - high.astype(F32)).astype(BF16)
-    for load in gate_loads:
-        load.wait()
+    drain(w_both, g_sem.at[0])
     for n in range(4, STEPS):
         pass_z(n)
 
     def pack(x):
-        each(EP, lambda k: exchange(x, k).wait_recv())
+        drain(landed.at[x, 0 : EP - 1], a_recv.at[x])
         gather_rows(landed.at[x])
         for j in range(8):
             units[z, core, x, :, j * 256 : (j + 1) * 256] = b_in[j]
@@ -469,7 +481,8 @@
     tell_tail().wait()
     lone = (ep == 0) & (spot == 0)
     mix_rows[0:16] = jnp.where(lone, jnp.zeros_like(halo), halo[...])
-    each(NZ * 2, lambda k: tell_taps(k).wait())
+    drain(taps_all.at[0 : NZ * 2 - 1], t_recv.at[0])
+    drain(taps_all.at[0 : NZ * 2 - 1], t_send.at[0])
     for x in range(LOCAL):
         copy, at, _ = across(x, STEPS)
         copy.wait_recv()
@@ -504,10 +517,7 @@
             copy, at, x = across(way, n)
             copy.wait_recv()
             compute(at, 1 - core, x)
-        if n == 4:
-            each(EP, lambda k: exchange(0, k).wait_send())
-            each(EP, lambda k: exchange(1, k).wait_send())
-        elif n == 5:
+        if n == 5:
             help_other(0)
             send_sum(1, 0)
             send_sum(0, 0)
@@ -522,10 +532,9 @@
     take(9)
     own_keep().wait()
     own_over().wait()
-    for half, way in both_halves:
-        for kind in range(KINDS):
-            plane(half, way, kind).wait_send()
-            plane_over(half, way, kind).wait()
+    for kind in range(KINDS):
+        for sem in (d_recv, d_send, x_send):
+            drain(four(kind), sem.at[kind])
     fetch(0).start()
     fetch(1).start()
     send_sum(0, 2)
@@ -551,55 +560,81 @@
     send_sum(1, 6)
     help_other(7)
 
-    for x in (1, 0):
-        help_copy(x, STEPS).wait_recv()
-        for way in range(2):
-            sum_copy(way, LAST_IN[x][way]).wait_recv()
-
-        def tile(j, _, x=x):
-            cols = pl.ds(pl.multiple_of(j * 256, 256), 256)
+    for x, part in ((1, 0), (1, 1), (0, 0), (0, 1)):
+        if part == 0:
+            help_copy(x, STEPS).wait_recv()
+        if part == 0 or x == 0:
+            for way in range(2):
+                sum_copy(way, LAST_IN[x, part][way]).wait_recv()
+
+        def tile(j, _, x=x, part=part):
+            cols = pl.ds(pl.multiple_of(part * 1024 + j * 256, 256), 256)
             total = jnp.dot(hid[z, core, x], w_down[x, :, cols], preferred_element_type=F32)
             for ref in (
-                c_in.at[x, STEPS % C_IN], r_in.at[0, LAST_IN[x][0]], r_in.at[1, LAST_IN[x][1]]
+                c_in.at[x, STEPS % C_IN],
+                r_in.at[0, min(LAST_IN[x, part][0], 6)],
+                r_in.at[1, min(LAST_IN[x, part][1], 6)],
             ):
                 total = total + ref[:, cols].astype(F32)
-            b_in[j] = total.astype(BF16)
+            total = total.astype(BF16)
+            b_half[2 * j] = total[:, 0:128]
+            b_half[2 * j + 1] = total[:, 128:256]
             return 0
 
-        lax.fori_loop(0, 8, tile, 0)
-        spread_rows(x)
-        each(EP, lambda k, x=x: hand_back(x, k).start())
-        back[x, ep] = slots[x, ep]
-
-    for x in (1, 0):
-        each(EP, lambda k, x=x: hand_back(x, k).wait_recv())
-
-        gather_rows(back.at[x])
-
-        def combine(j, _, x=x):
-            values = b_in[j]
-            both = jnp.dot(shares[x], values, preferred_element_type=F32)
+        lax.fori_loop(0, 4, tile, 0)
+
+        def swap_out(j, _, x=x, part=part):
+            rows = pl.ds(pl.multiple_of(j * EIGHTS, EIGHTS), EIGHTS)
+            wide = jnp.dot(swap[...], b_half[:, rows].reshape(SWAP, 128), preferred_element_type=F32)
+            b_slots[x, part, pl.ds(j * 8, 8)] = wide.astype(BF16).reshape(8, EIGHTS, 128)
+            return 0
+
+        lax.fori_loop(0, 2, swap_out, 0)
+        each(EP, lambda k, x=x, part=part: hand_back(x, part, k).start())
+        back[x, part, ep] = b_slots[x, part, ep]
+
+    for x, part in ((1, 0), (1, 1), (0, 0), (0, 1)):
+        drain(back.at[x, part, 0 : EP - 1], b_recv.at[x, part])
+
+        def swap_in(j, _, x=x, part=part):
+            rows = pl.ds(pl.multiple_of(j * EIGHTS, EIGHTS), EIGHTS)
+            out = jnp.dot(
+                swap[...], back[x, part, pl.ds(j * 8, 8)].reshape(SWAP, 128), preferred_element_type=F32
+            )
+            b_half[:, rows] = out.astype(BF16).reshape(8, EIGHTS, 128)
+            return 0
+
+        lax.fori_loop(0, 2, swap_in, 0)
+
+        def combine(j, _, x=x, part=part):
+            pair = jnp.concatenate((b_half[2 * j], b_half[2 * j + 1]), axis=1)
+            both = jnp.dot(shares[x], pair, preferred_element_type=F32)
             both = both[0:128] + both[128:256]
             if x == 1:
-                sums[j] = both
+                sums[part * 4 + j] = both
             else:
-                cols = pl.ds(pl.multiple_of(j * 256, 256), 256)
-                expert_out[:, cols] = (sums[j] + both).astype(BF16)
+                cols = pl.ds(pl.multiple_of(part * 1024 + j * 256, 256), 256)
+                expert_out[:, cols] = (sums[part * 4 + j] + both).astype(BF16)
             return 0
 
-        lax.fori_loop(0, 8, combine, 0)
+        lax.fori_loop(0, 4, combine, 0)
+    for x in range(LOCAL):
+        drain(slots.at[x, 0 : EP - 1], a_send.at[x])
+        for part in range(2):
+            drain(b_slots.at[x, part, 0 : EP - 1], b_send.at[x, part])
     for way in range(2):
-        for n in range(STEPS):
-            spread_z(way, n).wait_send()
-            ring_copy(way, n).wait_send()
-            across(way, n)[0].wait_send()
-        across(way, STEPS)[0].wait_send()
+        drain(wz.at[0:STEPS, 0:2], z_send.at[way])
+        drain(units.at[0:STEPS, 0, 0], r_send.at[way])
+        drain(units.at[:, 0, 0], c_send.at[way])
         for m in range(STEPS + 1 - C_OUT, STEPS + 1):
             help_copy(way, m).wait_send()
-        for m in range(STEPS - R_OUT, STEPS):
+        for m in range(STEPS - R_OUT, STEPS + 1):
             sum_copy(way, m).wait_send()
-    for x in (1, 0):
-        each(EP, lambda k, x=x: hand_back(x, k).wait_send())
+
+
+def hand_out_kernel(mixer_in, expert_in, mixer_out, expert_out):
+    mixer_out[...] = mixer_in[...]
+    expert_out[...] = expert_in[...]
 
 
 DMA = pltpu.SemaphoreType.DMA
@@ -616,14 +651,23 @@
     mixer_out, expert_out, _ = pl.pallas_call(
         whole_kernel,
         out_shape=(out, out, jax.ShapeDtypeStruct((EP, 2 * NZ, 4, 128, 128), BF16)),
-        in_specs=[vmem] * 6 + [anywhere] * 8,
+        in_specs=[anywhere] * 14,
         out_specs=(vmem, vmem, anywhere),
         scratch_shapes=[
+            pltpu.VMEM((tok_count, width), BF16),
+            pltpu.VMEM((1, width), F32),
+            pltpu.VMEM((1, width), F32),
+            pltpu.VMEM((2, tok_count), jnp.int32),
+            pltpu.VMEM((2, tok_count), F32),
             pltpu.VMEM((8, 128), F32),
+            pltpu.VMEM((tok_count, width), BF16),
+            pltpu.VMEM(w_down.shape, BF16),
             pltpu.VMEM((LOCAL, EP, EIGHTS, 256), BF16),
             pltpu.VMEM((LOCAL, EP, EIGHTS, 256), BF16),
-            pltpu.VMEM((LOCAL, EP, EIGHTS, 256), BF16),
+            pltpu.VMEM((LOCAL, 2, EP, EIGHTS, 128), BF16),
+            pltpu.VMEM((LOCAL, 2, EP, EIGHTS, 128), BF16),
             pltpu.VMEM((8, ROWS, 256), BF16),
+            pltpu.VMEM((8, ROWS, 128), BF16),
             pltpu.VMEM((NZ, 4, 128, 128), BF16),
             pltpu.VMEM((16, width), BF16),
             pltpu.VMEM((tok_count + 16, width), BF16),
@@ -631,8 +675,6 @@
             pltpu.VMEM((NZ, 2, LOCAL, ROWS, width), BF16),
             pltpu.VMEM((LOCAL, width, 256), BF16),
             pltpu.VMEM((NZ, 2, LOCAL, ROWS, 128), BF16),
-            pltpu.VMEM((tok_count, width), BF16),
-            pltpu.VMEM(w_down.shape, BF16),
             pltpu.VMEM((2, C_OUT, ROWS, width), BF16),
             pltpu.VMEM((2, C_IN, ROWS, width), BF16),
             pltpu.VMEM((2, R_OUT, ROWS, width), BF16),
@@ -642,11 +684,12 @@
             pltpu.VMEM((8, 128, 256), F32),
             pltpu.VMEM((NZ * 2, 128, 128), BF16),
             pltpu.VMEM((2, EP, 3, 128, 128), BF16),
-            DMA((4,)), DMA((LOCAL, 2)), DMA((LOCAL, EP)), DMA((LOCAL, EP)), DMA((LOCAL, EP)), DMA((LOCAL, EP)),
-            DMA((2, STEPS)), DMA((2, STEPS)), DMA((NZ * 2,)), DMA((NZ * 2,)), DMA((2,)),
-            DMA((2, STEPS)), DMA((2, STEPS)), DMA((2, STEPS + 1)), DMA((2, STEPS + 1)),
-            DMA((2, 2, KINDS)), DMA((2, 2, KINDS)), DMA((2, 2, KINDS)), DMA((2, 2, KINDS)), DMA((3,)),
-            DMA((2, STEPS)), DMA((2, STEPS)), DMA((2, STEPS + 1)), DMA((2, STEPS + 1)), DMA((2, 2)), DMA((2,)),
+            DMA((1,)), DMA((1,)), DMA((LOCAL,)), DMA((LOCAL,)), DMA((LOCAL, 2)), DMA((LOCAL, 2)),
+            DMA((2,)), DMA((2, STEPS)), DMA((1,)), DMA((1,)), DMA((2,)),
+            DMA((2,)), DMA((2, STEPS)), DMA((2,)), DMA((2, STEPS + 1)),
+            DMA((KINDS,)), DMA((KINDS,)), DMA((KINDS,)), DMA((KINDS,)), DMA((3,)),
+            DMA((2, STEPS + 1)), DMA((2, STEPS + 1)), DMA((2, STEPS + 1)), DMA((2, STEPS + 1)),
+            DMA((2, 2)), DMA((8,)),
             pltpu.SemaphoreType.REGULAR((2,)),
         ],
         cost_estimate=pl.CostEstimate(flops=10**11, bytes_accessed=3 * 10**8, transcendentals=0),
@@ -658,7 +701,13 @@
         expert_in, mixer_gain[None, :], expert_gain[None, :], route_ids.T, route_weights.T, conv_taps,
         mixer_in, w_down, w_outer, w_inner, w_value, w_mix_out, w_gate, w_up,
     )
-    return mixer_out, expert_out
+    return pl.pallas_call(
+        hand_out_kernel,
+        out_shape=(out, out),
+        in_specs=[vmem, vmem],
+        out_specs=(vmem, vmem),
+        name="hand_out",
+    )(mixer_out, expert_out)
 
 
 def solution(mesh):

time: 253 us -> 244 us (0.964)
  local copies, waits for them, and re-layouts: 3.76 us -> 0 us
  Pallas kernels: 246 us -> 243 us
    pallas_call x1, Pallas kernels: 246 us -> 241 us  [per_device(): pl.pallas_call(whole_kernel, out_shape=(out, out, jax.ShapeDtypeStruct((E...]
    unnamed x2 -> x0, local copies, waits for them, and re-layouts: 3.76 us -> none
where the time goes in v6:
time: 244 us
  Pallas kernels  243 us (100%)
    pallas_call x1, Pallas kernels, per_device(): pl.pallas_call(whole_kernel, out_shape=(out, out, jax.ShapeDtypeStruct((E...  241 us

profile of v6, /device:TPU:1, one launch (start us, length us, event | category | flops | bytes accessed | tf_op | source)
XLA Modules:
  0.0 243.9 jit_solution(16565593528422130132)
XLA Ops:
  0.6 241.0 %whole_block.1 = (bf16[128,2048]{1,0:T(8,128)(2,1)}, bf16[128,2048]{1,0:T(8,128)(2,1)}, bf16[16,16,4,128,128]{4,3,2,1,0:T(8,128)(2,1)}) custom-call(bf16[128,2048]{1,0:T(8,128)(2,1)} %expert_hbm.1, f32[1,2048]{1,0:T(1,128)} %bitcast.4, f32[1,2048]{1,0:T(1,128)} %bitcast.5, s32[2,128]{1,0:T(2,128)} %bitcast.6, f32[2,128]{1,0:T(2,128)} %bitcast.7, ...), custom_call_target="tpu_custom_call" | custom-call | flops 99999997952 | bytes 300000000 | tf_op jit(solution)/shard_map/whole_block/pallas_call | solution.py:651
  241.7 2.2 hand_out.1

commit v7 on v6

--- a/solution.py
+++ b/solution.py
@@ -163,9 +163,9 @@
     steps = (NZ - 1, 1)
 
     def spread_z(way, n):
-        away = GATHER_D[n] - 1
-        at = lax.rem(z + away * steps[way], NZ)
-        there = (ep, lax.rem(z + (NZ - steps[way]), NZ), core)
+        hops = 2 if n == STEPS - 1 else 1
+        at = lax.rem(z + (GATHER_D[n] - hops) * steps[way], NZ)
+        there = (ep, lax.rem(z + hops * (NZ - steps[way]), NZ), core)
         two = pl.ds(2 * GATHER_X[way][n], 2)
         return remote(
             wz.at[at, two], wz.at[at, two], z_send.at[way], z_recv.at[way, n], there
@@ -261,9 +261,11 @@
     def pass_z(n):
         for way in range(2):
             spread_z(way, n).wait_recv()
-            nxt = forwards(way, n)
-            if nxt is not None:
-                spread_z(way, nxt).start()
+            for nxt in (n + 2, STEPS - 1):
+                hops = 2 if nxt == STEPS - 1 else 1
+                if nxt < STEPS and nxt > n and (nxt == n + 2 or n in (2, 3)):
+                    if (GATHER_X[way][nxt], GATHER_D[nxt]) == (GATHER_X[way][n], GATHER_D[n] + hops):
+                        spread_z(way, nxt).start()
 
     go = (1, NZ - 1)
 
@@ -426,12 +428,12 @@
             b_in[j] = out[:, j * 256 : (j + 1) * 256]
         spread_rows(x)
 
+    fill_slots(0)
     pl.semaphore_wait(pltpu.get_barrier_semaphore(), EP + NZ * 2)
     drain(wz.at[z], w_sem.at[0])
     for n in range(LOCAL):
         for way in range(2):
             spread_z(way, n).start()
-    fill_slots(0)
     each(EP, lambda k: exchange(0, k).start())
     pass_z(0)
     fill_slots(1)
@@ -458,8 +460,6 @@
         shares[x, 0:128] = high
         shares[x, 128:256] = (total - high.astype(F32)).astype(BF16)
     drain(w_both, g_sem.at[0])
-    for n in range(4, STEPS):
-        pass_z(n)
 
     def pack(x):
         drain(landed.at[x, 0 : EP - 1], a_recv.at[x])
@@ -473,6 +473,8 @@
     pack(0)
     compute(z, core, 0)
     pack(1)
+    for n in range(4, STEPS):
+        pass_z(n)
     give(0)
     give(2)
     own_over().start()

time: 244 us -> 242 us (level)
  Pallas kernels: 243 us -> 240 us
    pallas_call x1, Pallas kernels: 241 us -> 237 us  [per_device(): pl.pallas_call(whole_kernel, out_shape=(out, out, jax.ShapeDtypeStruct((E...]
where the time goes in v7:
time: 242 us; the launch traced here: 240 us
  Pallas kernels  240 us (99%)
    pallas_call x1, Pallas kernels, per_device(): pl.pallas_call(whole_kernel, out_shape=(out, out, jax.ShapeDtypeStruct((E...  237 us

profile of v7, /device:TPU:1, one launch (start us, length us, event | category | flops | bytes accessed | tf_op | source)
XLA Modules:
  0.0 240.2 jit_solution(8683945243262852398)
XLA Ops:
  0.6 237.3 %whole_block.1 = (bf16[128,2048]{1,0:T(8,128)(2,1)}, bf16[128,2048]{1,0:T(8,128)(2,1)}, bf16[16,16,4,128,128]{4,3,2,1,0:T(8,128)(2,1)}) custom-call(bf16[128,2048]{1,0:T(8,128)(2,1)} %expert_hbm.1, f32[1,2048]{1,0:T(1,128)} %bitcast.4, f32[1,2048]{1,0:T(1,128)} %bitcast.5, s32[2,128]{1,0:T(2,128)} %bitcast.6, f32[2,128]{1,0:T(2,128)} %bitcast.7, ...), custom_call_target="tpu_custom_call" | custom-call | flops 99999997952 | bytes 300000000 | tf_op jit(solution)/shard_map/whole_block/pallas_call | solution.py:653
  238.0 2.2 hand_out.1
